TPU v7x, 32 devices: a whole 2x2x4 slice. The times are simulated.
32 devices in a mesh: rep: 2 (over x), fs: 8 (over z, y), tp: 2 (over core).
Axes of the slice: x: 2, y: 2, z: 4, core: 2. Of those that a mesh axis runs over, the one named last changes fastest.
Arguments:
- tokens: bfloat16 [16, 512, 2048], P(('rep', 'fs')), may hold values from -6 to 6
- gain_mix_pre: float32 [2048], P('fs'), may hold values from 0.1 to 1.9
- gain_mix_post: float32 [2048], P('fs'), may hold values from 0.1 to 1.9
- gain_mlp_pre: float32 [2048], P('fs'), may hold values from 0.1 to 1.9
- gain_mlp_post: float32 [2048], P('fs'), may hold values from 0.1 to 1.9
- x_weight: float32 [2048, 2048], P('fs', 'tp'), may hold values from -0.125 to 0.125
- gate_weight: float32 [2048, 2048], P('fs', 'tp'), may hold values from -0.125 to 0.125
- x_scale: float32 [2048], P('tp'), may hold values from 0.5 to 2
- gate_scale: float32 [2048], P('tp'), may hold values from 0.5 to 2
- conv_weight: float32 [4, 2048], P(None, 'tp'), may hold values from -3 to 3
- recur_map: bfloat16 [2048, 32], P('tp'), may hold values from -1 to 1
- input_map: bfloat16 [2048, 32], P('tp'), may hold values from -1 to 1
- decay_param: float32 [2048], P('tp'), may hold values from 3.9 to 10
- out_weight: float32 [2048, 2048], P('tp', 'fs'), may hold values from -0.125 to 0.125
- out_scale: float32 [2048], P('fs'), may hold values from 0.5 to 2
- up_weight: float32 [2048, 6144], P('fs', 'tp'), may hold values from -0.125 to 0.125
- up_scale: float32 [6144], P('tp'), may hold values from 0.5 to 2
- down_weight: float32 [6144, 2048], P('tp', 'fs'), may hold values from -0.078125 to 0.078125
- down_scale: float32 [2048], P('fs'), may hold values from 0.5 to 2
Outputs:
- layer_out: bfloat16 [16, 512, 2048], P(('rep', 'fs'), 'tp')
All inputs are finite; a program needn't handle non-finite values.
Results may differ from a plain program's by a relative error of at most 0.025.
Values may be sent and summed in bfloat16 or wider, within the bound.
No kernel may reach another device: no remote copies, remote signals or barrier semaphores. Data moves between devices by JAX's collectives and lax.ppermute only.
A program may use at most 128 MiB of HBM per device.

v0:
```python
import functools

import jax
import jax.numpy as jnp
import numpy as np
from jax import lax
from jax.experimental import pallas as pl
from jax.experimental.pallas import tpu as pltpu
from jax.sharding import PartitionSpec as P


BLOCK = 32
EPSILON = 1e-06
DECAY_SCALE = 8.0
BF16 = jnp.bfloat16
F32 = jnp.float32
LANES = 128
TIME_PAD = 8
VMEM_LIMIT = 56 * 1024 * 1024


def rms_rows(values, gain_vector):
    return (
        values
        * lax.rsqrt(jnp.mean(values * values, axis=-1, keepdims=True) + EPSILON)
        * gain_vector
    )


def params(**kw):
    return pltpu.CompilerParams(vmem_limit_bytes=VMEM_LIMIT, **kw)


def cost(flops, bytes_accessed, transcendentals=0):
    return pl.CostEstimate(
        flops=int(flops), bytes_accessed=int(bytes_accessed), transcendentals=int(transcendentals)
    )


def whole_spec(shape):
    zeros = (0,) * len(shape)
    return pl.BlockSpec(shape, lambda *_: zeros)


def ring_order(count):
    return list(range(0, count, 2)) + [i for i in range(count - 1, 0, -1) if i % 2]


def arrival(count):
    offsets = [0]
    for k in range(1, count // 2):
        offsets += [-k, k]
    return offsets + [count // 2]


def order_table(count):
    ring = ring_order(count)
    place = {dev: i for i, dev in enumerate(ring)}
    rows = [[ring[(place[m] + off) % count] for off in arrival(count)] for m in range(count)]
    return np.asarray(rows, np.int32)


def ring_gather(first, second, count):
    ring = ring_order(count)
    fwd = [(ring[i], ring[(i + 1) % count]) for i in range(count)]
    bwd = [(b, a) for a, b in fwd]
    far = count // 2
    ahead, behind = [first, second], [first, second]
    held = [(first, second)]
    for k in range(1, far + 1):
        for h in range(2):
            if k < far or h == 0:
                ahead[h] = lax.ppermute(ahead[h], "fs", fwd)
            if k < far or h == 1:
                behind[h] = lax.ppermute(behind[h], "fs", bwd)
        if k < far:
            held += [tuple(ahead), tuple(behind)]
    return held + [(ahead[0], behind[1])]


def shift(value, axis, count, by):
    return lax.ppermute(value, axis, [((i + by) % count, i) for i in range(count)])


def exchange_small(value, axis, count):
    got = [value]
    for by in range(1, count):
        got.append(shift(value, axis, count, by))
    return got


def fetch(order, chunks, weights, first, cols, sems):
    copies = []
    for s, chunk in enumerate(chunks):
        rows = chunk.shape[0]
        at = pl.multiple_of(order[s] * rows, rows)
        copies.append(
            pltpu.make_async_copy(
                chunk.at[:, 0:cols], weights.at[pl.ds(at, rows), first : first + cols], sems.at[s]
            )
        )
    for copy in copies:
        copy.start()
    return copies


def wait_all(copies):
    for copy in copies:
        copy.wait()


def norm_kernel(count, tp, *refs):
    out = refs[-1]
    for i in range(count):

        @pl.when(pl.program_id(0) == i)
        def _():
            v = refs[i][...].astype(F32)
            scale = lax.rsqrt(jnp.mean(v * v, axis=-1, keepdims=True) + EPSILON)
            out[...] = (v * scale).astype(BF16)


def normalize(tp, pieces):
    rows, width = pieces[0].shape
    count = len(pieces)
    return pl.pallas_call(
        functools.partial(norm_kernel, count),
        grid_spec=pltpu.PrefetchScalarGridSpec(
            num_scalar_prefetch=1,
            grid=(count,),
            in_specs=[whole_spec((rows, width))] * count,
            out_specs=pl.BlockSpec((rows, width), lambda i, tp: ((tp[0] + i) % count, 0)),
        ),
        out_shape=jax.ShapeDtypeStruct((count * rows, width), BF16),
        compiler_params=params(),
        cost_estimate=cost(1e9, 4 * count * rows * width),
        name="normalize",
    )(tp, *pieces)


def project_kernel(steps, order, normed, scale, *refs):
    xs, gs = refs[:steps], refs[steps : 2 * steps]
    x_out, gate_out, x_full, gate_full, sems = refs[2 * steps :]
    cols = x_out.shape[1]
    x_copies = fetch(order, xs, x_full, 0, cols, sems.at[0])
    gate_copies = fetch(order, gs, gate_full, 0, cols, sems.at[1])
    wait_all(x_copies)
    total = jnp.dot(normed[...], x_full[...], preferred_element_type=F32)
    x_out[...] = (total * scale[:, :cols]).astype(BF16)
    wait_all(gate_copies)
    total = jnp.dot(normed[...], gate_full[...], preferred_element_type=F32)
    gate_out[...] = (total * scale[:, cols:]).astype(BF16)


def project(order, normed, scale, held):
    steps = len(held)
    length, width = normed.shape
    cols = scale.shape[1] // 2
    out = jax.ShapeDtypeStruct((length, cols), BF16)
    vmem = pl.BlockSpec(memory_space=pltpu.VMEM)
    hbm = pl.BlockSpec(memory_space=pltpu.HBM)
    return pl.pallas_call(
        functools.partial(project_kernel, steps),
        grid_spec=pltpu.PrefetchScalarGridSpec(
            num_scalar_prefetch=1,
            grid=(),
            in_specs=[vmem, vmem] + [hbm] * (2 * steps),
            out_specs=[vmem, vmem],
            scratch_shapes=[
                pltpu.VMEM((width, cols), BF16),
                pltpu.VMEM((width, cols), BF16),
                pltpu.SemaphoreType.DMA((2, steps)),
            ],
        ),
        out_shape=[out, out],
        compiler_params=params(),
        cost_estimate=cost(4 * length * width * cols, 2 * (length + 2 * cols) * width),
        name="project",
    )(order, normed, scale, *[h[0] for h in held], *[h[1] for h in held])


def recur_kernel(x_ref, gate_ref, conv_ref, maps_ref, rate_ref, out_ref, pad, decay, state):
    seqs, length, width = x_ref.shape
    blocks = width // LANES
    lines = seqs * blocks
    stride = length + TIME_PAD
    taps = conv_ref.shape[0]
    pad[0:TIME_PAD, :] = jnp.zeros((TIME_PAD, LANES), F32)
    for q in range(seqs):
        for b in range(blocks):
            cols = slice(b * LANES, (b + 1) * LANES)
            base = (q * blocks + b) * stride
            pad[TIME_PAD:, :] = x_ref[q, :, cols].astype(F32)
            total = None
            for k in range(taps):
                at = TIME_PAD - (taps - 1) + k
                part = conv_ref[k : k + 1, cols] * pad[at : at + length, :]
                total = part if total is None else total + part
            conv = total.astype(BF16)
            logits = jnp.dot(conv, maps_ref[b], preferred_element_type=F32)
            log_decay = rate_ref[:, cols] * jax.nn.sigmoid(logits[:, :LANES])
            a = jnp.exp(log_decay)
            y = 2.0 * log_decay
            series = -y * (
                1.0
                + y * (1 / 2 + y * (1 / 6 + y * (1 / 24 + y * (1 / 120 + y * (1 / 720)))))
            )
            loss = jnp.where(y > -0.4, series, 1.0 - a * a)
            decay[base : base + length, :] = a
            state[base : base + length, :] = (
                jnp.sqrt(loss) * jax.nn.sigmoid(logits[:, LANES:]) * conv.astype(F32)
            )

    def advance(t, h):
        at = pl.ds(t, lines, stride=stride)
        h = decay[at, :] * h + state[at, :]
        state[at, :] = h
        return h

    lax.fori_loop(0, length, advance, jnp.zeros((lines, LANES), F32), unroll=16)
    for q in range(seqs):
        for b in range(blocks):
            cols = slice(b * LANES, (b + 1) * LANES)
            base = (q * blocks + b) * stride
            g = gate_ref[q, :, cols].astype(F32)
            out_ref[q, :, cols] = (
                state[base : base + length, :] * jax.nn.gelu(g)
            ).astype(BF16)


def recur(x_branch, gate_branch, conv_weight, maps, rate):
    seqs, length, width = x_branch.shape
    lines = seqs * (width // LANES)
    rows = lines * (length + TIME_PAD)
    vmem = pl.BlockSpec(memory_space=pltpu.VMEM)
    return pl.pallas_call(
        recur_kernel,
        in_specs=[vmem] * 5,
        out_specs=vmem,
        out_shape=jax.ShapeDtypeStruct(x_branch.shape, BF16),
        scratch_shapes=[
            pltpu.VMEM((length + TIME_PAD, LANES), F32),
            pltpu.VMEM((rows, LANES), F32),
            pltpu.VMEM((rows, LANES), F32),
        ],
        compiler_params=params(),
        cost_estimate=cost(3e9, 6 * x_branch.size, 10 * x_branch.size),
        name="recur",
    )(x_branch, gate_branch, conv_weight, maps, rate)


def out_kernel(steps, order, mixed, *refs):
    top, low = refs[:steps], refs[steps : 2 * steps]
    outs = refs[2 * steps :]
    tps, share = len(outs), outs[0].shape[1]
    half, cols = top[0].shape
    pieces = []
    for j in range(tps):
        at = pl.multiple_of((order[steps] + j) % tps * share, share)
        pieces.append(mixed[0, pl.ds(at, share), :])
    m = jnp.concatenate(pieces, axis=0)
    for s in range(steps):
        at = pl.multiple_of(order[s] * cols, cols)
        part = jnp.dot(m[:, :half], top[s][...], preferred_element_type=F32)
        part = part + jnp.dot(m[:, half:], low[s][...], preferred_element_type=F32)
        for j, out in enumerate(outs):
            out[0, :, pl.ds(at, cols)] = part[j * share : (j + 1) * share].astype(BF16)


def out_project(order, tp, tps, mixed, held, cols):
    steps = len(held)
    seqs, length, width = mixed.shape
    share = length // tps
    scalars = jnp.concatenate([order, tp.astype(jnp.int32).reshape(1)])
    chunk = pl.BlockSpec((width // 2, cols), lambda *_: (0, width // cols))
    row = lambda rows, n: pl.BlockSpec((1, rows, n), lambda i, *_: (i, 0, 0))
    return pl.pallas_call(
        functools.partial(out_kernel, steps),
        grid_spec=pltpu.PrefetchScalarGridSpec(
            num_scalar_prefetch=1,
            grid=(seqs,),
            in_specs=[row(length, width)] + [chunk] * (2 * steps),
            out_specs=[row(share, steps * cols)] * tps,
        ),
        out_shape=[jax.ShapeDtypeStruct((seqs, share, steps * cols), BF16)] * tps,
        compiler_params=params(),
        cost_estimate=cost(
            2 * seqs * length * width * steps * cols,
            2 * (width * steps * cols + seqs * length * (width + steps * cols)),
        ),
        name="out_project",
    )(scalars, mixed, *[h[0] for h in held], *[h[1] for h in held])


def place_gains(me, pieces, gains):
    count, cols = len(pieces), pieces[0].shape[1]
    for i, piece in enumerate(pieces):
        at = pl.multiple_of((me + i) % count * cols, cols)
        gains[:, pl.ds(at, cols)] = piece[...]


def mid_kernel(count, me, tokens, *refs):
    parts, pieces = refs[: -3 - count], refs[-3 - count : -3]
    hidden, normed, gains = refs[-3:]
    place_gains(me[0], pieces, gains)
    total = parts[0][0].astype(F32)
    for part in parts[1:]:
        total = total + part[0].astype(F32)
    h = (
        tokens[...].astype(F32)
        + total
        * lax.rsqrt(jnp.mean(total * total, axis=-1, keepdims=True) + EPSILON)
        * gains[0:1, :]
    ).astype(BF16)
    hidden[...] = h
    v = h.astype(F32)
    normed[...] = (
        v * lax.rsqrt(jnp.mean(v * v, axis=-1, keepdims=True) + EPSILON)
    ).astype(BF16)


def mid(me, tokens, parts, gains):
    rows, width = tokens.shape
    tile = rows // 2
    row = pl.BlockSpec((tile, width), lambda i, *_: (i, 0))
    part = pl.BlockSpec((1, tile, width), lambda i, *_: (0, i, 0))
    out = jax.ShapeDtypeStruct((rows, width), BF16)
    return pl.pallas_call(
        functools.partial(mid_kernel, len(gains)),
        grid_spec=pltpu.PrefetchScalarGridSpec(
            num_scalar_prefetch=1,
            grid=(rows // tile,),
            in_specs=[row] + [part] * len(parts) + [whole_spec(g.shape) for g in gains],
            out_specs=[row, row],
            scratch_shapes=[pltpu.VMEM((2, width), F32)],
        ),
        out_shape=[out, out],
        compiler_params=params(),
        cost_estimate=cost(2e9, 2 * rows * width * (3 + len(parts))),
        name="mid",
    )(me, tokens, *parts, *gains)


def up_kernel(steps, blocks, order, scale, *refs):
    first, second = refs[:steps], refs[steps : 2 * steps]
    xs = refs[2 * steps : 2 * steps + blocks]
    out, first_full, second_full, sems = refs[2 * steps + blocks :]
    cols = first[0].shape[1]
    x = jnp.concatenate([ref[...] for ref in xs], axis=0)
    ready = [fetch(order, first, first_full, 0, cols, sems.at[0])]
    ready.append(fetch(order, second, second_full, 0, cols, sems.at[1]))
    for w, full in enumerate((first_full, second_full)):
        wait_all(ready[w])
        span = slice(w * cols, (w + 1) * cols)
        total = jnp.dot(x, full[...], preferred_element_type=F32)
        total = jnp.maximum(total * scale[:, span], 0.0)
        out[:, span] = (total * total).astype(BF16)


def up_project(order, scale, held, xs):
    steps = len(held)
    rows, width = xs[0].shape
    cols = held[0][0].shape[1]
    vmem = pl.BlockSpec(memory_space=pltpu.VMEM)
    hbm = pl.BlockSpec(memory_space=pltpu.HBM)
    return pl.pallas_call(
        functools.partial(up_kernel, steps, len(xs)),
        grid_spec=pltpu.PrefetchScalarGridSpec(
            num_scalar_prefetch=1,
            grid=(),
            in_specs=[vmem] + [hbm] * (2 * steps) + [vmem] * len(xs),
            out_specs=vmem,
            scratch_shapes=[
                pltpu.VMEM((width, cols), BF16),
                pltpu.VMEM((width, cols), BF16),
                pltpu.SemaphoreType.DMA((2, steps)),
            ],
        ),
        out_shape=jax.ShapeDtypeStruct((len(xs) * rows, 2 * cols), BF16),
        compiler_params=params(),
        cost_estimate=cost(
            4 * len(xs) * rows * width * cols,
            2 * (2 * width * cols + len(xs) * rows * (width + 2 * cols)),
        ),
        name="up_project",
    )(order, scale, *[h[0] for h in held], *[h[1] for h in held], *xs)


def down_kernel(steps, acts, *refs):
    a, chunks, outs = refs[:acts], refs[acts : acts + 2 * steps], refs[acts + 2 * steps :]
    half, cols = chunks[0].shape
    rows = outs[0].shape[1]
    for s in range(steps):
        for d, act in enumerate(a):
            total = jnp.dot(act[:, :half], chunks[2 * s][...], preferred_element_type=F32)
            total = total + jnp.dot(
                act[:, half:], chunks[2 * s + 1][...], preferred_element_type=F32
            )
            for i, out in enumerate(outs):
                out[d, :, s * cols : (s + 1) * cols] = total[i * rows : (i + 1) * rows].astype(
                    BF16
                )


def down_project(blocks, acts, held):
    rows, hidden = acts[0].shape
    rows = rows // blocks
    flat = [c for pair in held for c in pair]
    cols = flat[0].shape[1] * len(held)
    vmem = pl.BlockSpec(memory_space=pltpu.VMEM)
    return pl.pallas_call(
        functools.partial(down_kernel, len(held), len(acts)),
        in_specs=[vmem] * (len(acts) + len(flat)),
        out_specs=[vmem] * blocks,
        out_shape=[jax.ShapeDtypeStruct((len(acts), rows, cols), BF16)] * blocks,
        compiler_params=params(),
        cost_estimate=cost(
            2 * len(acts) * blocks * rows * hidden * cols,
            2 * (hidden * cols + len(acts) * blocks * rows * (hidden + cols)),
        ),
        name="down_project",
    )(*acts, *flat)


def last_kernel(streams, count, scalars, hidden, *refs):
    pieces = refs[-3 - count : -3]
    out, total, gains = refs[-3:]
    place_gains(scalars[count], pieces, gains)
    cols = hidden.shape[1] // count
    where = []
    first = 0
    for groups in streams:
        where.append([(first + g, s) for g, steps in enumerate(groups) for s in range(steps)])
        first += len(groups)
    for step in range(count):
        value = None
        for places in where:
            g, s = places[step]
            part = refs[g][0, :, s * cols : (s + 1) * cols].astype(F32)
            value = part if value is None else value + part
        to = pl.multiple_of(scalars[step] * cols, cols)
        total[:, pl.ds(to, cols)] = value
    v = total[...]
    out[...] = (
        hidden[...].astype(F32)
        + v * lax.rsqrt(jnp.mean(v * v, axis=-1, keepdims=True) + EPSILON) * gains[1:2, :]
    ).astype(BF16)


def last(scalars, hidden, streams, parts, gains):
    rows, width = hidden.shape
    tile = rows // 2
    flat = [p for stream in parts for p in stream]
    row = pl.BlockSpec((tile, width), lambda i, *_: (i, 0))
    part = lambda p: pl.BlockSpec((1, tile, p.shape[2]), lambda i, *_: (p.shape[0] - 1, i, 0))
    return pl.pallas_call(
        functools.partial(last_kernel, streams, len(gains)),
        grid_spec=pltpu.PrefetchScalarGridSpec(
            num_scalar_prefetch=1,
            grid=(rows // tile,),
            in_specs=[row] + [part(p) for p in flat] + [whole_spec(g.shape) for g in gains],
            out_specs=row,
            scratch_shapes=[pltpu.VMEM((tile, width), F32), pltpu.VMEM((2, width), F32)],
        ),
        out_shape=jax.ShapeDtypeStruct((rows, width), BF16),
        compiler_params=params(),
        cost_estimate=cost(1e9, 2 * rows * width * (2 + len(streams))),
        name="last",
    )(scalars, hidden, *flat, *gains)


def group_sizes(count):
    far = (3,) + (2,) * (count // 2 - 2) + (1,) if count > 2 else (1, 1)
    return far, (count - 1, 1)


def ring_device(
    reps,
    count,
    tps,
    tokens,
    gain_mix_pre,
    gain_mix_post,
    gain_mlp_pre,
    gain_mlp_post,
    x_weight,
    gate_weight,
    x_scale,
    gate_scale,
    conv_weight,
    recur_map,
    input_map,
    decay_param,
    out_weight,
    out_scale,
    up_weight,
    up_scale,
    down_weight,
    down_scale,
):
    rep, me, tp = (lax.axis_index(a) for a in ("rep", "fs", "tp"))
    length, width = tokens.shape[1:]
    share = length // tps
    chan = x_weight.shape[1] // reps
    hid = up_weight.shape[1] // reps

    def rep_part(value, size, axis):
        return lax.dynamic_slice_in_dim(value, rep * size, size, axis)

    pre = gain_mix_pre[:, None]
    out_mine = rep_part(out_weight, chan, 0) * out_scale
    mixer = ring_gather(
        jnp.concatenate(
            [rep_part(x_weight, chan, 1) * pre, out_mine[: chan // 2]], axis=1
        ).astype(BF16),
        jnp.concatenate(
            [rep_part(gate_weight, chan, 1) * pre, out_mine[chan // 2 :]], axis=1
        ).astype(BF16),
        count,
    )
    up_mine = (rep_part(up_weight, hid, 1) * gain_mlp_pre[:, None]).astype(BF16)
    ups = ring_gather(up_mine[:, : hid // 2], up_mine[:, hid // 2 :], count)
    down_mine = (rep_part(down_weight, hid, 0) * down_scale).astype(BF16)
    downs = ring_gather(down_mine[: hid // 2], down_mine[hid // 2 :], count)
    order = lax.dynamic_slice_in_dim(jnp.asarray(order_table(count)), me, 1, 0)[0]

    mine = lax.dynamic_slice_in_dim(tokens[0], tp * share, share, 0)
    seqs = [[tokens[0]]]
    for dr in range(1, reps):
        seqs.append([shift(mine, "rep", reps, dr)])
        for dt in range(1, tps):
            seqs[dr].append(shift(seqs[dr][0], "tp", tps, dt))
    tp_scalar = tp.astype(jnp.int32).reshape(1)
    normed_in = []
    for dr, pieces in enumerate(seqs):
        normed_in.append(normalize(tp_scalar if dr else 0 * tp_scalar, pieces))
    gains = exchange_small(jnp.stack([gain_mix_post, gain_mlp_post]), "fs", count)
    scales = jnp.concatenate([rep_part(x_scale, chan, 0), rep_part(gate_scale, chan, 0)])[None]
    same = jnp.asarray(
        (np.arange(LANES)[:, None] // BLOCK == np.arange(LANES)[None] // BLOCK), BF16
    )

    def dense_map(value):
        blocks = rep_part(value, chan, 0).reshape(chan // LANES, LANES, BLOCK)
        return jnp.tile(blocks, (1, 1, LANES // BLOCK)) * same

    maps = jnp.concatenate([dense_map(recur_map), dense_map(input_map)], axis=2)
    rate = -DECAY_SCALE * jax.nn.softplus(-rep_part(decay_param, chan, 0))[None]
    taps = rep_part(conv_weight, chan, 1)

    def over_tp(parts):
        got = [parts[0]]
        for dt in range(1, tps):
            got.append(shift(parts[dt], "tp", tps, tps - dt))
        return got

    def over_rep(summands, dr):
        total = sum(x.astype(F32) for x in summands).astype(BF16)
        return shift(total, "rep", reps, reps - dr)

    far_first = list(range(1, reps)) + [0]
    pieces = []
    for dr in far_first:
        x_branch, gate_branch = project(order, normed_in[dr], scales, mixer)
        mixed = recur(x_branch[None], gate_branch[None], taps, maps, rate)
        parts = out_project(order, tp, tps, mixed, mixer, width // count)
        summands = over_tp(parts)
        pieces += [over_rep(summands, dr)] if dr else summands
    hidden, normed = mid(me.astype(jnp.int32).reshape(1), mine, pieces, gains)

    scale = rep_part(up_scale, hid, 0)[None]
    acts = []
    for dr in range(reps):
        base = normed
        if dr:
            base = shift(normed, "rep", reps, dr)
        blocks = [base]
        for dt in range(1, tps):
            blocks.append(shift(base, "tp", tps, dt))
        acts.append(up_project(order, scale, ups, blocks))

    rows_of = {dr: [] for dr in far_first}
    for dr in far_first:
        groups = group_sizes(count)[0 if dr else 1]
        at = 0
        for steps in groups[:-1]:
            parts = down_project(tps, [acts[dr]], downs[at : at + steps])
            at += steps
            summands = over_tp(parts)
            rows_of[dr].append([over_rep(summands, dr)] if dr else summands)
    parts = down_project(tps, [acts[dr] for dr in far_first], downs[-1:])
    summands = over_tp(parts)
    for i, dr in enumerate(far_first):
        if dr:
            own = [x[i : i + 1] for x in summands]
            rows_of[dr].append([over_rep(own, dr)])
        else:
            rows_of[dr].append(summands)
    streams, arrays = [], []
    for dr in far_first:
        for i in range(len(rows_of[dr][0])):
            streams.append(group_sizes(count)[0 if dr else 1])
            arrays.append([group[i] for group in rows_of[dr]])
    scalars = jnp.concatenate([order, me.astype(jnp.int32).reshape(1)])
    return last(scalars, hidden, tuple(streams), arrays, gains)[None]


def link_states(earlier, later):
    return (earlier[0] * later[0], later[0] * earlier[1] + later[1])


def plain_device(
    tokens,
    gain_mix_pre,
    gain_mix_post,
    gain_mlp_pre,
    gain_mlp_post,
    x_weight,
    gate_weight,
    x_scale,
    gate_scale,
    conv_weight,
    recur_map,
    input_map,
    decay_param,
    out_weight,
    out_scale,
    up_weight,
    up_scale,
    down_weight,
    down_scale,
):
    resid_in = tokens[0].astype(F32)
    length = resid_in.shape[0]
    local_width = x_weight.shape[1]
    gains = lax.all_gather(
        jnp.stack(
            [gain_mix_pre, gain_mix_post, gain_mlp_pre, gain_mlp_post, out_scale, down_scale]
        ),
        "fs",
        axis=1,
        tiled=True,
    )
    gather = lambda w, axis: lax.all_gather(w.astype(BF16), "fs", axis=axis, tiled=True)
    normed = rms_rows(resid_in, gains[0]).astype(BF16)
    x_proj = jnp.dot(normed, gather(x_weight, 0), preferred_element_type=F32)
    gate_proj = jnp.dot(normed, gather(gate_weight, 0), preferred_element_type=F32)
    out_cols = gather(out_weight, 1)
    down_full = gather(down_weight, 1)
    x_branch = (x_proj * x_scale).astype(BF16)
    gate_branch = (gate_proj * gate_scale).astype(BF16)
    taps = conv_weight.shape[0]
    padded = jnp.concatenate([jnp.zeros((taps - 1, local_width), BF16), x_branch], axis=0)
    conv_sum = conv_weight[0] * padded[0:length].astype(F32)
    for k in range(1, taps):
        conv_sum = conv_sum + conv_weight[k] * padded[k : k + length].astype(F32)
    conv_out = lax.optimization_barrier(conv_sum.astype(BF16))
    blocks = local_width // BLOCK
    conv_blocks = conv_out.reshape(length, blocks, BLOCK)

    def logits(value):
        return jnp.einsum(
            "tnc,ncd->tnd",
            conv_blocks,
            value.reshape(blocks, BLOCK, BLOCK),
            preferred_element_type=F32,
        ).reshape(length, local_width)

    log_decay = (
        -DECAY_SCALE * jax.nn.sigmoid(logits(recur_map)) * jax.nn.softplus(-decay_param)
    )
    drive = (
        jnp.sqrt(-jnp.expm1(2.0 * log_decay))
        * jax.nn.sigmoid(logits(input_map))
        * conv_out.astype(F32)
    )
    _, states = lax.associative_scan(link_states, (jnp.exp(log_decay), drive), axis=0)
    mixed = (states * jax.nn.gelu(gate_branch.astype(F32))).astype(BF16)
    share_rows = length // lax.axis_size("tp")

    def scatter(left, right, scale):
        part = (jnp.dot(left, right, preferred_element_type=F32) * scale).astype(BF16)
        return lax.psum_scatter(part, "tp", scatter_dimension=0, tiled=True).astype(F32)

    mix_share = scatter(mixed, out_cols, gains[4])
    resid_share = lax.dynamic_slice_in_dim(
        resid_in, lax.axis_index("tp") * share_rows, share_rows, 0
    )
    hidden_state = (resid_share + rms_rows(mix_share, gains[1])).astype(BF16)
    normed_mlp = rms_rows(hidden_state.astype(F32), gains[2]).astype(BF16)
    mlp_input = lax.all_gather(normed_mlp, "tp", axis=0, tiled=True)
    up_proj = jnp.dot(mlp_input, gather(up_weight, 0), preferred_element_type=F32)
    activated = jnp.square(jax.nn.relu(up_proj * up_scale)).astype(BF16)
    mlp_share = scatter(activated, down_full, gains[5])
    out_share = hidden_state.astype(F32) + rms_rows(mlp_share, gains[3])
    return out_share.astype(BF16)[None]


def solution(mesh):
    in_specs = (
        P(("rep", "fs"), None, None),
        P("fs"),
        P("fs"),
        P("fs"),
        P("fs"),
        P("fs", "tp"),
        P("fs", "tp"),
        P("tp"),
        P("tp"),
        P(None, "tp"),
        P("tp", None),
        P("tp", None),
        P("tp"),
        P("tp", "fs"),
        P("fs"),
        P("fs", "tp"),
        P("tp"),
        P("tp", "fs"),
        P("fs"),
    )
    reps, count, tps = (mesh.shape[a] for a in ("rep", "fs", "tp"))

    def on_device(*args):
        tokens, x_weight, up_weight = args[0], args[5], args[15]
        (length, width), rows = tokens.shape[1:], x_weight.shape[0]
        chan, hid = x_weight.shape[1] // reps, up_weight.shape[1] // reps
        fits = (
            count % 2 == 0
            and rows % (2 * LANES) == 0
            and chan % (2 * LANES) == 0
            and chan == 2 * rows
            and chan % (width // count) == 0
            and hid % (2 * LANES) == 0
            and length % (32 * tps) == 0
            and reps * (chan // LANES) <= 8
        )
        if fits:
            return ring_device(reps, count, tps, *args)
        return plain_device(*args)

    return jax.shard_map(
        on_device,
        mesh=mesh,
        in_specs=in_specs,
        out_specs=P(("rep", "fs"), "tp", None),
        check_vma=False,
    )
```

profile of v0, /device:TPU:0, one launch (start us, length us, event | category | flops | bytes accessed | tf_op | source)
XLA Modules:
  0.0 303.3 jit_solution(9247164674960419689)
XLA Ops:
  11.9 6.0 %collective-permute-done.2.refs_1_ = bf16[256,768]{1,0:T(8,128)(2,1)S(1)} collective-permute-done((bf16[256,768]{1,0:T(8,128)(2,1)S(1)}, bf16[256,768]{1,0:T(8,128)(2,1)S(1)}, u32[]{:S(2)}, u32[]{:S(2)}) %collective-permute-start.2) | collective-permute-done | bytes 393248 | tf_op jit(solution)/shard_map/ppermute | solution.py:73
  19.5 6.7 %collective-permute-done.10.refs_10_ = bf16[256,768]{1,0:T(8,128)(2,1)S(1)} collective-permute-done((bf16[256,768]{1,0:T(8,128)(2,1)S(1)}, bf16[256,768]{1,0:T(8,128)(2,1)S(1)}, u32[]{:S(2)}, u32[]{:S(2)}) %collective-permute-start.10) | collective-permute-done | bytes 393248 | tf_op jit(solution)/shard_map/ppermute | solution.py:75
  39.7 6.7 %collective-permute-done.5.refs_4_ = bf16[256,768]{1,0:T(8,128)(2,1)S(1)} collective-permute-done((bf16[256,768]{1,0:T(8,128)(2,1)S(1)}, bf16[256,768]{1,0:T(8,128)(2,1)S(1)}, u32[]{:S(2)}, u32[]{:S(2)}) %collective-permute-start.5) | collective-permute-done | bytes 393248 | tf_op jit(solution)/shard_map/ppermute | solution.py:75
  48.4 4.1 %collective-permute-done.6.refs_5_ = bf16[256,768]{1,0:T(8,128)(2,1)S(1)} collective-permute-done((bf16[256,768]{1,0:T(8,128)(2,1)S(1)}, bf16[256,768]{1,0:T(8,128)(2,1)S(1)}, u32[]{:S(2)}, u32[]{:S(2)}) %collective-permute-start.6) | collective-permute-done | bytes 393248 | tf_op jit(solution)/shard_map/ppermute | solution.py:73
  54.8 3.7 %normalize.3.normed = bf16[512,2048]{1,0:T(8,128)(2,1)} custom-call(s32[1]{0:T(128)} %constant.35.clone.1.tp, bf16[512,2048]{1,0:T(8,128)(2,1)} %bitcast.28), custom_call_target="tpu_custom_call" | custom-call | flops 1000000000 | bytes 4194304 | tf_op jit(solution)/shard_map/normalize/pallas_call | solution.py:126
  59.5 4.6 %collective-permute-start.19 = (f32[2,256]{1,0:T(2,128)S(1)}, f32[2,256]{1,0:T(2,128)S(1)}, u32[]{:S(2)}, u32[]{:S(2)}) collective-permute-start(f32[2,256]{1,0:T(2,128)S(1)} %pad_maximum_fusion.4.refs_3_.refs_8_), channel_id=1, source_target_pairs={{2,0},{4,2},{6,4},{8,6},{10,8},{12,10},{14,12},{0,14},{3,1},{5,3},... | collective-permute-start | bytes 6152 | tf_op jit(solution)/shard_map/ppermute | solution.py:82
  71.7 7.3 %project.2 = (bf16[512,512]{1,0:T(8,128)(2,1)}, bf16[512,512]{1,0:T(8,128)(2,1)}) custom-call(s32[8]{0:T(128)} %copy-done.52, bf16[512,2048]{1,0:T(8,128)(2,1)} %normalize.2.normed, f32[1,1024]{1,0:T(1,128)} %bitcast.33, bf16[256,768]{1,0:T(8,128)(2,1)} %copy-done.2, bf16[256,768]{1,0:T(8,128)(2,1)} %copy-done.4, bf16[256,768]{1,0:T(8,128)(2,1)} %copy-done.5, ...), custom_call_target="tpu_custom_call" | custom-call | flops 2147483648 | bytes 6291456 | tf_op jit(solution)/shard_map/project/pallas_call | solution.py:162
  78.9 5.3 %recur.2.mixed = bf16[1,512,512]{2,1,0:T(8,128)(2,1)} custom-call(bf16[1,512,512]{2,1,0:T(8,128)(2,1)} %bitcast.41, bf16[1,512,512]{2,1,0:T(8,128)(2,1)} %bitcast.42, f32[4,512]{1,0:T(4,128)} %constant_dynamic-slice_fusion.conv_ref, bf16[4,128,256]{2,1,0:T(8,128)(2,1)} %pad_maximum_fusion.2.maps_ref, f32[1,512]{1,0:T(1,128)} %bitcast.35), custom_call_target="tpu_custom_call" | custom-call | flops 3000000000 | bytes 1572864 | tf_op jit(solution)/shard_map/recur/pallas_call | solution.py:236
  84.3 5.5 %out_project.2 = (bf16[1,256,2048]{2,1,0:T(8,128)(2,1)}, bf16[1,256,2048]{2,1,0:T(8,128)(2,1)}) custom-call(s32[9]{0:T(128)} %get-tuple-element.55.order, bf16[1,512,512]{2,1,0:T(8,128)(2,1)} %recur.2.mixed, bf16[256,768]{1,0:T(8,128)(2,1)} %copy-done.2, bf16[256,768]{1,0:T(8,128)(2,1)} %copy-done.4, bf16[256,768]{1,0:T(8,128)(2,1)} %copy-done.5, ...), custom_call_target="tpu_custom_call" | custom-call | flops 1073741824 | bytes 4718592 | tf_op jit(solution)/shard_map/out_project/pallas_call | solution.py:277
  89.9 7.3 %project.3 = (bf16[512,512]{1,0:T(8,128)(2,1)}, bf16[512,512]{1,0:T(8,128)(2,1)}) custom-call(s32[8]{0:T(128)} %copy-done.52, bf16[512,2048]{1,0:T(8,128)(2,1)} %normalize.3.normed, f32[1,1024]{1,0:T(1,128)} %bitcast.34, bf16[256,768]{1,0:T(8,128)(2,1)} %copy-done.2, bf16[256,768]{1,0:T(8,128)(2,1)} %copy-done.4, bf16[256,768]{1,0:T(8,128)(2,1)} %copy-done.5, ...), custom_call_target="tpu_custom_call" | custom-call | flops 2147483648 | bytes 6291456 | tf_op jit(solution)/shard_map/project/pallas_call | solution.py:162
  97.2 5.3 %recur.3.mixed = bf16[1,512,512]{2,1,0:T(8,128)(2,1)} custom-call(bf16[1,512,512]{2,1,0:T(8,128)(2,1)} %bitcast.39, bf16[1,512,512]{2,1,0:T(8,128)(2,1)} %bitcast.40, f32[4,512]{1,0:T(4,128)} %constant_dynamic-slice_fusion.conv_ref, bf16[4,128,256]{2,1,0:T(8,128)(2,1)} %pad_maximum_fusion.2.maps_ref, f32[1,512]{1,0:T(1,128)} %bitcast.36), custom_call_target="tpu_custom_call" | custom-call | flops 3000000000 | bytes 1572864 | tf_op jit(solution)/shard_map/recur/pallas_call | solution.py:236
  104.5 5.1 %out_project.3 = (bf16[1,256,2048]{2,1,0:T(8,128)(2,1)}, bf16[1,256,2048]{2,1,0:T(8,128)(2,1)}) custom-call(s32[9]{0:T(128)} %get-tuple-element.55.order, bf16[1,512,512]{2,1,0:T(8,128)(2,1)} %recur.3.mixed, bf16[256,768]{1,0:T(8,128)(2,1)} %copy-done.2, bf16[256,768]{1,0:T(8,128)(2,1)} %copy-done.4, bf16[256,768]{1,0:T(8,128)(2,1)} %copy-done.5, ...), custom_call_target="tpu_custom_call" | custom-call | flops 1073741824 | bytes 4718592 | tf_op jit(solution)/shard_map/out_project/pallas_call | solution.py:277
  116.7 7.4 %collective-permute-done.26.refs_1_ = bf16[256,768]{1,0:T(8,128)(2,1)S(1)} collective-permute-done((bf16[256,768]{1,0:T(8,128)(2,1)S(1)}, bf16[256,768]{1,0:T(8,128)(2,1)S(1)}, u32[]{:S(2)}, u32[]{:S(2)}) %collective-permute-start.26) | collective-permute-done | bytes 393248 | tf_op jit(solution)/shard_map/ppermute | solution.py:73
  126.3 6.2 %collective-permute-done.33.refs_9_ = bf16[256,768]{1,0:T(8,128)(2,1)S(1)} collective-permute-done((bf16[256,768]{1,0:T(8,128)(2,1)S(1)}, bf16[256,768]{1,0:T(8,128)(2,1)S(1)}, u32[]{:S(2)}, u32[]{:S(2)}) %collective-permute-start.33) | collective-permute-done | bytes 393248 | tf_op jit(solution)/shard_map/ppermute | solution.py:73
  134.6 6.4 %collective-permute-done.42.refs_3_ = bf16[768,256]{1,0:T(8,128)(2,1)S(1)} collective-permute-done((bf16[768,256]{1,0:T(8,128)(2,1)S(1)}, bf16[768,256]{1,0:T(8,128)(2,1)S(1)}, u32[]{:S(2)}, u32[]{:S(2)}) %collective-permute-start.42) | collective-permute-done | bytes 393248 | tf_op jit(solution)/shard_map/ppermute | solution.py:73
  142.5 5.5 %collective-permute-done.43.refs_4_ = bf16[768,256]{1,0:T(8,128)(2,1)S(1)} collective-permute-done((bf16[768,256]{1,0:T(8,128)(2,1)S(1)}, bf16[768,256]{1,0:T(8,128)(2,1)S(1)}, u32[]{:S(2)}, u32[]{:S(2)}) %collective-permute-start.43) | collective-permute-done | bytes 393248 | tf_op jit(solution)/shard_map/ppermute | solution.py:73
  151.9 8.2 %collective-permute-done.28.refs_3_ = bf16[256,768]{1,0:T(8,128)(2,1)S(1)} collective-permute-done((bf16[256,768]{1,0:T(8,128)(2,1)S(1)}, bf16[256,768]{1,0:T(8,128)(2,1)S(1)}, u32[]{:S(2)}, u32[]{:S(2)}) %collective-permute-start.28) | collective-permute-done | bytes 393248 | tf_op jit(solution)/shard_map/ppermute | solution.py:73
  163.3 3.7 %mid.1 = (bf16[256,2048]{1,0:T(8,128)(2,1)}, bf16[256,2048]{1,0:T(8,128)(2,1)}) custom-call(s32[1]{0:T(128)} %bitcast.1.me, bf16[256,2048]{1,0:T(8,128)(2,1)} %dynamic-slice_bitcast_fusion.tokens, bf16[1,256,2048]{2,1,0:T(8,128)(2,1)} %copy-done.72, bf16[1,256,2048]{2,1,0:T(8,128)(2,1)} %get-tuple-element.31.refs_1_, bf16[1,256,2048]{2,1,0:T(8,128)(2,1)} %copy-done.71, ...), custom_call_target="tpu_custom_call" | custom-call | flops 2000000000 | bytes 6291456 | tf_op jit(solution)/shard_map/mid/pallas_call | solution.py:328
  172.2 4.7 %collective-permute-done.48.refs_1_.refs_7_ = bf16[768,256]{1,0:T(8,128)(2,1)S(1)} collective-permute-done((bf16[768,256]{1,0:T(8,128)(2,1)S(1)}, bf16[768,256]{1,0:T(8,128)(2,1)S(1)}, u32[]{:S(2)}, u32[]{:S(2)}) %collective-permute-start.48) | collective-permute-done | bytes 393248 | tf_op jit(solution)/shard_map/ppermute | solution.py:73
  177.7 7.7 %collective-permute-done.49.refs_2_.refs_8_ = bf16[768,256]{1,0:T(8,128)(2,1)S(1)} collective-permute-done((bf16[768,256]{1,0:T(8,128)(2,1)S(1)}, bf16[768,256]{1,0:T(8,128)(2,1)S(1)}, u32[]{:S(2)}, u32[]{:S(2)}) %collective-permute-start.49) | collective-permute-done | bytes 393248 | tf_op jit(solution)/shard_map/ppermute | solution.py:73
  187.5 5.9 %collective-permute-done.30.refs_5_ = bf16[256,768]{1,0:T(8,128)(2,1)S(1)} collective-permute-done((bf16[256,768]{1,0:T(8,128)(2,1)}, bf16[256,768]{1,0:T(8,128)(2,1)S(1)}, u32[]{:S(2)}, u32[]{:S(2)}) %collective-permute-start.30) | collective-permute-done | bytes 393248 | tf_op jit(solution)/shard_map/ppermute | solution.py:73
  195.5 6.4 %collective-permute-done.37.refs_13_ = bf16[256,768]{1,0:T(8,128)(2,1)S(1)} collective-permute-done((bf16[256,768]{1,0:T(8,128)(2,1)}, bf16[256,768]{1,0:T(8,128)(2,1)S(1)}, u32[]{:S(2)}, u32[]{:S(2)}) %collective-permute-start.37) | collective-permute-done | bytes 393248 | tf_op jit(solution)/shard_map/ppermute | solution.py:73
  203.9 6.4 %collective-permute-done.54.refs_1_.refs_11_ = bf16[768,256]{1,0:T(8,128)(2,1)S(1)} collective-permute-done((bf16[768,256]{1,0:T(8,128)(2,1)S(1)}, bf16[768,256]{1,0:T(8,128)(2,1)S(1)}, u32[]{:S(2)}, u32[]{:S(2)}) %collective-permute-start.54) | collective-permute-done | bytes 393248 | tf_op jit(solution)/shard_map/ppermute | solution.py:73
  212.4 6.3 %collective-permute-done.32.refs_7_ = bf16[256,768]{1,0:T(8,128)(2,1)S(1)} collective-permute-done((bf16[256,768]{1,0:T(8,128)(2,1)S(1)}, bf16[256,768]{1,0:T(8,128)(2,1)S(1)}, u32[]{:S(2)}, u32[]{:S(2)}) %collective-permute-start.32) | collective-permute-done | bytes 393248 | tf_op jit(solution)/shard_map/ppermute | solution.py:73
  224.8 10.0 %up_project.3.refs_1_.refs_0_ = bf16[512,1536]{1,0:T(8,128)(2,1)} custom-call(s32[8]{0:T(128)} %copy-done.52, f32[1,1536]{1,0:T(1,128)} %broadcast_in_dim.33.scale, bf16[256,768]{1,0:T(8,128)(2,1)} %get-tuple-element.48.refs_0_, bf16[256,768]{1,0:T(8,128)(2,1)} %copy-done.75, bf16[256,768]{1,0:T(8,128)(2,1)} %copy-done.76, bf16[256,768]{1,0:T(8,128)(2,1)} %copy-done.82, ...), custom_call_target="tpu_custom_call" | custom-call | flops 3221225472 | bytes 9961472 | tf_op jit(solution)/shard_map/up_project/pallas_call | solution.py:366
  236.4 7.3 %down_project.9 = (bf16[1,256,1792]{2,1,0:T(8,128)(2,1)}, bf16[1,256,1792]{2,1,0:T(8,128)(2,1)}) custom-call(bf16[512,1536]{1,0:T(8,128)(2,1)} %up_project.3.refs_1_.refs_0_, bf16[768,256]{1,0:T(8,128)(2,1)} %copy-done.35, bf16[768,256]{1,0:T(8,128)(2,1)} %copy-done.34, bf16[768,256]{1,0:T(8,128)(2,1)} %copy-done.78, bf16[768,256]{1,0:T(8,128)(2,1)} %copy-done.80, ...), custom_call_target="tpu_custom_call" | custom-call | flops 2818572288 | bytes 8912896 | tf_op jit(solution)/shard_map/down_project/pallas_call | solution.py:411
  244.7 10.0 %up_project.2.refs_0_ = bf16[512,1536]{1,0:T(8,128)(2,1)} custom-call(s32[8]{0:T(128)} %copy-done.52, f32[1,1536]{1,0:T(1,128)} %broadcast_in_dim.33.scale, bf16[256,768]{1,0:T(8,128)(2,1)} %get-tuple-element.48.refs_0_, bf16[256,768]{1,0:T(8,128)(2,1)} %copy-done.75, bf16[256,768]{1,0:T(8,128)(2,1)} %copy-done.76, bf16[256,768]{1,0:T(8,128)(2,1)} %copy-done.82, ...), custom_call_target="tpu_custom_call" | custom-call | flops 3221225472 | bytes 9961472 | tf_op jit(solution)/shard_map/up_project/pallas_call | solution.py:366
  258.7 4.3 %down_project.5 = (bf16[1,256,768]{2,1,0:T(8,128)(2,1)}, bf16[1,256,768]{2,1,0:T(8,128)(2,1)}) custom-call(bf16[512,1536]{1,0:T(8,128)(2,1)} %up_project.2.refs_0_, bf16[768,256]{1,0:T(8,128)(2,1)} %copy-done.35, bf16[768,256]{1,0:T(8,128)(2,1)} %copy-done.34, bf16[768,256]{1,0:T(8,128)(2,1)} %copy-done.78, bf16[768,256]{1,0:T(8,128)(2,1)} %copy-done.80, ...), custom_call_target="tpu_custom_call" | custom-call | flops 1207959552 | bytes 4718592 | tf_op jit(solution)/shard_map/down_project/pallas_call | solution.py:411
  263.0 3.5 %down_project.7 = (bf16[1,256,512]{2,1,0:T(8,128)(2,1)}, bf16[1,256,512]{2,1,0:T(8,128)(2,1)}) custom-call(bf16[512,1536]{1,0:T(8,128)(2,1)} %up_project.2.refs_0_, bf16[768,256]{1,0:T(8,128)(2,1)} %copy-done.28, bf16[768,256]{1,0:T(8,128)(2,1)} %copy-done.29, bf16[768,256]{1,0:T(8,128)(2,1)} %copy-done.30, bf16[768,256]{1,0:T(8,128)(2,1)} %copy-done.27), custom_call_target="tpu_custom_call" | custom-call | flops 805306368 | bytes 3670016 | tf_op jit(solution)/shard_map/down_project/pallas_call | solution.py:411
  268.0 3.8 %down_project.8 = (bf16[2,256,256]{2,1,0:T(8,128)(2,1)}, bf16[2,256,256]{2,1,0:T(8,128)(2,1)}) custom-call(bf16[512,1536]{1,0:T(8,128)(2,1)} %up_project.2.refs_0_, bf16[512,1536]{1,0:T(8,128)(2,1)} %up_project.3.refs_1_.refs_0_, bf16[768,256]{1,0:T(8,128)(2,1)} %copy-done.37, bf16[768,256]{1,0:T(8,128)(2,1)} %copy-done.38), custom_call_target="tpu_custom_call" | custom-call | flops 805306368 | bytes 4456448 | tf_op jit(solution)/shard_map/down_project/pallas_call | solution.py:411
  277.0 20.6 %collective-permute-done.64.refs_3_ = bf16[1,256,256]{2,1,0:T(8,128)(2,1)S(1)} collective-permute-done((bf16[1,256,256]{2,1,0:T(8,128)(2,1)S(1)}, bf16[1,256,256]{2,1,0:T(8,128)(2,1)S(1)}, u32[]{:S(2)}, u32[]{:S(2)}) %collective-permute-start.64) | collective-permute-done | bytes 131104 | tf_op jit(solution)/shard_map/ppermute | solution.py:82
  298.6 4.5 %last.1 = bf16[256,2048]{1,0:T(8,128)(2,1)} custom-call(s32[9]{0:T(128)} %get-tuple-element.56.scalars, bf16[256,2048]{1,0:T(8,128)(2,1)} %get-tuple-element.33.hidden, bf16[1,256,768]{2,1,0:T(8,128)(2,1)} %copy-done.31, bf16[1,256,512]{2,1,0:T(8,128)(2,1)} %copy-done.41, bf16[1,256,512]{2,1,0:T(8,128)(2,1)} %copy-done.44, bf16[1,256,256]{2,1,0:T(8,128)(2,1)} %copy-done.46, ...), custom_call_target="tpu_custom_call" | custom-call | flops 1000000000 | bytes 5242880 | tf_op jit(solution)/shard_map/last/pallas_call | solution.py:456
  (329 shorter events, 95.8 us)
Async XLA Ops:
  2.5 26.4 %collective-permute-start = (bf16[256,2048]{1,0:T(8,128)(2,1)}, bf16[256,2048]{1,0:T(8,128)(2,1)}, u32[]{:S(2)}, u32[]{:S(2)}) collective-permute-start(bf16[256,2048]{1,0:T(8,128)(2,1)} %dynamic-slice_bitcast_fusion.tokens), channel_id=1, source_target_pairs={{16,0},{0,16},{17,1},{1,17},{18,2},{2,18},{19,3},{3,19},{20,4},{4,... | collective-permute-start | bytes 3145736 | tf_op jit(solution)/shard_map/ppermute | solution.py:82
  7.5 22.9 %collective-permute-start.3 = (bf16[256,768]{1,0:T(8,128)(2,1)S(1)}, bf16[256,768]{1,0:T(8,128)(2,1)S(1)}, u32[]{:S(2)}, u32[]{:S(2)}) collective-permute-start(bf16[256,768]{1,0:T(8,128)(2,1)S(1)} %pad_maximum_fusion.refs_0_), channel_id=1, source_target_pairs={{4,0},{8,4},{12,8},{14,12},{10,14},{6,10},{2,6},{0,2},{5,1},{9,5},... | collective-permute-start | bytes 1179656 | tf_op jit(solution)/shard_map/ppermute | solution.py:75
  8.0 24.1 %collective-permute-start.9 = (bf16[256,768]{1,0:T(8,128)(2,1)S(1)}, bf16[256,768]{1,0:T(8,128)(2,1)S(1)}, u32[]{:S(2)}, u32[]{:S(2)}) collective-permute-start(bf16[256,768]{1,0:T(8,128)(2,1)S(1)} %pad_maximum_fusion.1.refs_8_), channel_id=1, source_target_pairs={{0,4},{4,8},{8,12},{12,14},{14,10},{10,6},{6,2},{2,0},{1,5},{5,9},... | collective-permute-start | bytes 1179656 | tf_op jit(solution)/shard_map/ppermute | solution.py:73
  28.9 30.5 %collective-permute-start.1 = (bf16[256,2048]{1,0:T(8,128)(2,1)}, bf16[256,2048]{1,0:T(8,128)(2,1)}, u32[]{:S(2)}, u32[]{:S(2)}) collective-permute-start(bf16[256,2048]{1,0:T(8,128)(2,1)} %collective-permute-done.refs_0_), channel_id=1, source_target_pairs={{1,0},{0,1},{3,2},{2,3},{5,4},{4,5},{7,6},{6,7},{9,8},{8,9},{11,10... | collective-permute-start | bytes 3145736 | tf_op jit(solution)/shard_map/ppermute | solution.py:82
  33.3 19.2 %collective-permute-start.6 = (bf16[256,768]{1,0:T(8,128)(2,1)S(1)}, bf16[256,768]{1,0:T(8,128)(2,1)S(1)}, u32[]{:S(2)}, u32[]{:S(2)}) collective-permute-start(bf16[256,768]{1,0:T(8,128)(2,1)S(1)} %collective-permute-done.4.refs_3_), channel_id=1, source_target_pairs={{0,4},{4,8},{8,12},{12,14},{14,10},{10,6},{6,2},{2,0},{1,5},{5,9},... | collective-permute-start | bytes 1179656 | tf_op jit(solution)/shard_map/ppermute | solution.py:73
  38.0 16.9 %collective-permute-start.14 = (bf16[256,768]{1,0:T(8,128)(2,1)S(1)}, bf16[256,768]{1,0:T(8,128)(2,1)S(1)}, u32[]{:S(2)}, u32[]{:S(2)}) collective-permute-start(bf16[256,768]{1,0:T(8,128)(2,1)S(1)} %collective-permute-done.12.refs_12_), channel_id=1, source_target_pairs={{4,0},{8,4},{12,8},{14,12},{10,14},{6,10},{2,6},{0,2},{5,1},{9,5},... | collective-permute-start | bytes 1179656 | tf_op jit(solution)/shard_map/ppermute | solution.py:75
  46.4 21.0 %collective-permute-start.7 = (bf16[256,768]{1,0:T(8,128)(2,1)S(1)}, bf16[256,768]{1,0:T(8,128)(2,1)S(1)}, u32[]{:S(2)}, u32[]{:S(2)}) collective-permute-start(bf16[256,768]{1,0:T(8,128)(2,1)S(1)} %collective-permute-done.5.refs_4_), channel_id=1, source_target_pairs={{4,0},{8,4},{12,8},{14,12},{10,14},{6,10},{2,6},{0,2},{5,1},{9,5},... | collective-permute-start | bytes 1179656 | tf_op jit(solution)/shard_map/ppermute | solution.py:75
  46.4 21.0 %collective-permute-start.13 = (bf16[256,768]{1,0:T(8,128)(2,1)S(1)}, bf16[256,768]{1,0:T(8,128)(2,1)S(1)}, u32[]{:S(2)}, u32[]{:S(2)}) collective-permute-start(bf16[256,768]{1,0:T(8,128)(2,1)S(1)} %collective-permute-done.11.refs_11_), channel_id=1, source_target_pairs={{0,4},{4,8},{8,12},{12,14},{14,10},{10,6},{6,2},{2,0},{1,5},{5,9},... | collective-permute-start | bytes 1179656 | tf_op jit(solution)/shard_map/ppermute | solution.py:73
  59.5 43.1 %collective-permute-start.19 = (f32[2,256]{1,0:T(2,128)S(1)}, f32[2,256]{1,0:T(2,128)S(1)}, u32[]{:S(2)}, u32[]{:S(2)}) collective-permute-start(f32[2,256]{1,0:T(2,128)S(1)} %pad_maximum_fusion.4.refs_3_.refs_8_), channel_id=1, source_target_pairs={{2,0},{4,2},{6,4},{8,6},{10,8},{12,10},{14,12},{0,14},{3,1},{5,3},... | collective-permute-start | bytes 6152 | tf_op jit(solution)/shard_map/ppermute | solution.py:82
  67.4 42.3 %collective-permute-start.20 = (f32[2,256]{1,0:T(2,128)S(1)}, f32[2,256]{1,0:T(2,128)S(1)}, u32[]{:S(2)}, u32[]{:S(2)}) collective-permute-start(f32[2,256]{1,0:T(2,128)S(1)} %pad_maximum_fusion.4.refs_3_.refs_8_), channel_id=1, source_target_pairs={{4,0},{6,2},{8,4},{10,6},{12,8},{14,10},{0,12},{2,14},{5,1},{7,3},... | collective-permute-start | bytes 6152 | tf_op jit(solution)/shard_map/ppermute | solution.py:82
  67.4 42.7 %collective-permute-start.21 = (f32[2,256]{1,0:T(2,128)S(1)}, f32[2,256]{1,0:T(2,128)S(1)}, u32[]{:S(2)}, u32[]{:S(2)}) collective-permute-start(f32[2,256]{1,0:T(2,128)S(1)} %pad_maximum_fusion.4.refs_3_.refs_8_), channel_id=1, source_target_pairs={{6,0},{8,2},{10,4},{12,6},{14,8},{0,10},{2,12},{4,14},{7,1},{9,3},... | collective-permute-start | bytes 6152 | tf_op jit(solution)/shard_map/ppermute | solution.py:82
  68.7 43.4 %collective-permute-start.22 = (f32[2,256]{1,0:T(2,128)S(1)}, f32[2,256]{1,0:T(2,128)S(1)}, u32[]{:S(2)}, u32[]{:S(2)}) collective-permute-start(f32[2,256]{1,0:T(2,128)S(1)} %pad_maximum_fusion.4.refs_3_.refs_8_), channel_id=1, source_target_pairs={{8,0},{10,2},{12,4},{14,6},{0,8},{2,10},{4,12},{6,14},{9,1},{11,3}... | collective-permute-start | bytes 6152 | tf_op jit(solution)/shard_map/ppermute | solution.py:82
  89.7 24.4 %collective-permute-start.16 = (bf16[1,256,2048]{2,1,0:T(8,128)(2,1)}, bf16[1,256,2048]{2,1,0:T(8,128)(2,1)S(1)}, u32[]{:S(2)}, u32[]{:S(2)}) collective-permute-start(bf16[1,256,2048]{2,1,0:T(8,128)(2,1)} %get-tuple-element.28), channel_id=1, source_target_pairs={{1,0},{0,1},{3,2},{2,3},{5,4},{4,5},{7,6},{6,7},{9,8},{8,9},{11,10... | collective-permute-start | bytes 3145736 | tf_op jit(solution)/shard_map/ppermute | solution.py:82
  114.1 18.4 %collective-permute-start.33 = (bf16[256,768]{1,0:T(8,128)(2,1)S(1)}, bf16[256,768]{1,0:T(8,128)(2,1)S(1)}, u32[]{:S(2)}, u32[]{:S(2)}) collective-permute-start(bf16[256,768]{1,0:T(8,128)(2,1)S(1)} %get-tuple-element.47.refs_8_), channel_id=1, source_target_pairs={{0,4},{4,8},{8,12},{12,14},{14,10},{10,6},{6,2},{2,0},{1,5},{5,9},... | collective-permute-start | bytes 1179656 | tf_op jit(solution)/shard_map/ppermute | solution.py:73
  115.3 18.0 %collective-permute-start.34 = (bf16[256,768]{1,0:T(8,128)(2,1)S(1)}, bf16[256,768]{1,0:T(8,128)(2,1)S(1)}, u32[]{:S(2)}, u32[]{:S(2)}) collective-permute-start(bf16[256,768]{1,0:T(8,128)(2,1)S(1)} %get-tuple-element.47.refs_8_), channel_id=1, source_target_pairs={{4,0},{8,4},{12,8},{14,12},{10,14},{6,10},{2,6},{0,2},{5,1},{9,5},... | collective-permute-start | bytes 1179656 | tf_op jit(solution)/shard_map/ppermute | solution.py:75
  116.6 45.3 %collective-permute-start.18 = (bf16[1,256,2048]{2,1,0:T(8,128)(2,1)S(1)}, bf16[1,256,2048]{2,1,0:T(8,128)(2,1)S(1)}, u32[]{:S(2)}, u32[]{:S(2)}) collective-permute-start(bf16[1,256,2048]{2,1,0:T(8,128)(2,1)S(1)} %copy-done.70), channel_id=1, source_target_pairs={{1,0},{0,1},{3,2},{2,3},{5,4},{4,5},{7,6},{6,7},{9,8},{8,9},{11,10... | collective-permute-start | bytes 3145736 | tf_op jit(solution)/shard_map/ppermute | solution.py:82
  124.1 38.0 %collective-permute-start.17 = (bf16[1,256,2048]{2,1,0:T(8,128)(2,1)S(1)}, bf16[1,256,2048]{2,1,0:T(8,128)(2,1)S(1)}, u32[]{:S(2)}, u32[]{:S(2)}) collective-permute-start(bf16[1,256,2048]{2,1,0:T(8,128)(2,1)S(1)} %add_convert_fusion), channel_id=1, source_target_pairs={{16,0},{0,16},{17,1},{1,17},{18,2},{2,18},{19,3},{3,19},{20,4},{4,... | collective-permute-start | bytes 3145736 | tf_op jit(solution)/shard_map/ppermute | solution.py:82
  148.8 18.1 %collective-permute-start.29 = (bf16[256,768]{1,0:T(8,128)(2,1)S(1)}, bf16[256,768]{1,0:T(8,128)(2,1)S(1)}, u32[]{:S(2)}, u32[]{:S(2)}) collective-permute-start(bf16[256,768]{1,0:T(8,128)(2,1)S(1)} %collective-permute-done.27.refs_2_), channel_id=1, source_target_pairs={{4,0},{8,4},{12,8},{14,12},{10,14},{6,10},{2,6},{0,2},{5,1},{9,5},... | collective-permute-start | bytes 1179656 | tf_op jit(solution)/shard_map/ppermute | solution.py:75
  150.2 18.4 %collective-permute-start.35 = (bf16[256,768]{1,0:T(8,128)(2,1)S(1)}, bf16[256,768]{1,0:T(8,128)(2,1)}, u32[]{:S(2)}, u32[]{:S(2)}) collective-permute-start(bf16[256,768]{1,0:T(8,128)(2,1)S(1)} %collective-permute-done.33.refs_9_), channel_id=1, source_target_pairs={{0,4},{4,8},{8,12},{12,14},{14,10},{10,6},{6,2},{2,0},{1,5},{5,9},... | collective-permute-start | bytes 1179656 | tf_op jit(solution)/shard_map/ppermute | solution.py:73
  162.1 23.2 %collective-permute-start.49 = (bf16[768,256]{1,0:T(8,128)(2,1)S(1)}, bf16[768,256]{1,0:T(8,128)(2,1)S(1)}, u32[]{:S(2)}, u32[]{:S(2)}) collective-permute-start(bf16[768,256]{1,0:T(8,128)(2,1)S(1)} %collective-permute-done.43.refs_4_), channel_id=1, source_target_pairs={{0,4},{4,8},{8,12},{12,14},{14,10},{10,6},{6,2},{2,0},{1,5},{5,9},... | collective-permute-start | bytes 1179656 | tf_op jit(solution)/shard_map/ppermute | solution.py:73
  167.0 36.9 %collective-permute-start.40 = (bf16[256,2048]{1,0:T(8,128)(2,1)}, bf16[256,2048]{1,0:T(8,128)(2,1)S(1)}, u32[]{:S(2)}, u32[]{:S(2)}) collective-permute-start(bf16[256,2048]{1,0:T(8,128)(2,1)} %get-tuple-element.34.refs_16_), channel_id=1, source_target_pairs={{16,0},{0,16},{17,1},{1,17},{18,2},{2,18},{19,3},{3,19},{20,4},{4,... | collective-permute-start | bytes 3145736 | tf_op jit(solution)/shard_map/ppermute | solution.py:82
  168.6 18.6 %collective-permute-start.50 = (bf16[768,256]{1,0:T(8,128)(2,1)}, bf16[768,256]{1,0:T(8,128)(2,1)S(1)}, u32[]{:S(2)}, u32[]{:S(2)}) collective-permute-start(bf16[768,256]{1,0:T(8,128)(2,1)} %collective-permute-done.44.refs_5_), channel_id=1, source_target_pairs={{4,0},{8,4},{12,8},{14,12},{10,14},{6,10},{2,6},{0,2},{5,1},{9,5},... | collective-permute-start | bytes 1179656 | tf_op jit(solution)/shard_map/ppermute | solution.py:75
  187.2 35.0 %collective-permute-start.60 = (bf16[256,2048]{1,0:T(8,128)(2,1)}, bf16[256,2048]{1,0:T(8,128)(2,1)S(1)}, u32[]{:S(2)}, u32[]{:S(2)}) collective-permute-start(bf16[256,2048]{1,0:T(8,128)(2,1)} %get-tuple-element.34.refs_16_), channel_id=1, source_target_pairs={{1,0},{0,1},{3,2},{2,3},{5,4},{4,5},{7,6},{6,7},{9,8},{8,9},{11,10... | collective-permute-start | bytes 3145736 | tf_op jit(solution)/shard_map/ppermute | solution.py:82
  203.9 39.8 %collective-permute-start.41 = (bf16[256,2048]{1,0:T(8,128)(2,1)S(1)}, bf16[256,2048]{1,0:T(8,128)(2,1)S(1)}, u32[]{:S(2)}, u32[]{:S(2)}) collective-permute-start(bf16[256,2048]{1,0:T(8,128)(2,1)S(1)} %collective-permute-done.40.refs_16_), channel_id=1, source_target_pairs={{1,0},{0,1},{3,2},{2,3},{5,4},{4,5},{7,6},{6,7},{9,8},{8,9},{11,10... | collective-permute-start | bytes 3145736 | tf_op jit(solution)/shard_map/ppermute | solution.py:82
  212.1 22.9 %collective-permute-start.55 = (bf16[768,256]{1,0:T(8,128)(2,1)S(1)}, bf16[768,256]{1,0:T(8,128)(2,1)S(1)}, u32[]{:S(2)}, u32[]{:S(2)}) collective-permute-start(bf16[768,256]{1,0:T(8,128)(2,1)S(1)} %collective-permute-done.49.refs_2_.refs_8_), channel_id=1, source_target_pairs={{0,4},{4,8},{8,12},{12,14},{14,10},{10,6},{6,2},{2,0},{1,5},{5,9},... | collective-permute-start | bytes 1179656 | tf_op jit(solution)/shard_map/ppermute | solution.py:73
  221.9 44.6 %collective-permute-start.61 = (bf16[768,256]{1,0:T(8,128)(2,1)S(1)}, bf16[768,256]{1,0:T(8,128)(2,1)S(1)}, u32[]{:S(2)}, u32[]{:S(2)}) collective-permute-start(bf16[768,256]{1,0:T(8,128)(2,1)S(1)} %collective-permute-done.54.refs_1_.refs_11_), channel_id=1, source_target_pairs={{0,4},{4,8},{8,12},{12,14},{14,10},{10,6},{6,2},{2,0},{1,5},{5,9},... | collective-permute-start | bytes 1179656 | tf_op jit(solution)/shard_map/ppermute | solution.py:73
  222.7 44.5 %collective-permute-start.62 = (bf16[768,256]{1,0:T(8,128)(2,1)S(1)}, bf16[768,256]{1,0:T(8,128)(2,1)S(1)}, u32[]{:S(2)}, u32[]{:S(2)}) collective-permute-start(bf16[768,256]{1,0:T(8,128)(2,1)S(1)} %collective-permute-done.57.refs_4_.refs_14_), channel_id=1, source_target_pairs={{4,0},{8,4},{12,8},{14,12},{10,14},{6,10},{2,6},{0,2},{5,1},{9,5},... | collective-permute-start | bytes 1179656 | tf_op jit(solution)/shard_map/ppermute | solution.py:75
  243.7 33.3 %collective-permute-start.65 = (bf16[1,256,1792]{2,1,0:T(8,128)(2,1)}, bf16[1,256,1792]{2,1,0:T(8,128)(2,1)S(1)}, u32[]{:S(2)}, u32[]{:S(2)}) collective-permute-start(bf16[1,256,1792]{2,1,0:T(8,128)(2,1)} %get-tuple-element.44), channel_id=1, source_target_pairs={{1,0},{0,1},{3,2},{2,3},{5,4},{4,5},{7,6},{6,7},{9,8},{8,9},{11,10... | collective-permute-start | bytes 2752520 | tf_op jit(solution)/shard_map/ppermute | solution.py:82
  272.4 25.1 %collective-permute-start.53 = (bf16[1,256,512]{2,1,0:T(8,128)(2,1)S(1)}, bf16[1,256,512]{2,1,0:T(8,128)(2,1)S(1)}, u32[]{:S(2)}, u32[]{:S(2)}) collective-permute-start(bf16[1,256,512]{2,1,0:T(8,128)(2,1)S(1)} %add_convert_fusion.3), channel_id=1, source_target_pairs={{16,0},{0,16},{17,1},{1,17},{18,2},{2,18},{19,3},{3,19},{20,4},{4,... | collective-permute-start | bytes 786440 | tf_op jit(solution)/shard_map/ppermute | solution.py:82
  274.1 23.5 %collective-permute-start.47 = (bf16[1,256,768]{2,1,0:T(8,128)(2,1)S(1)}, bf16[1,256,768]{2,1,0:T(8,128)(2,1)S(1)}, u32[]{:S(2)}, u32[]{:S(2)}) collective-permute-start(bf16[1,256,768]{2,1,0:T(8,128)(2,1)S(1)} %add_convert_fusion.1), channel_id=1, source_target_pairs={{16,0},{0,16},{17,1},{1,17},{18,2},{2,18},{19,3},{3,19},{20,4},{4,... | collective-permute-start | bytes 1179656 | tf_op jit(solution)/shard_map/ppermute | solution.py:82
  274.7 22.8 %collective-permute-start.59 = (bf16[1,256,512]{2,1,0:T(8,128)(2,1)S(1)}, bf16[1,256,512]{2,1,0:T(8,128)(2,1)S(1)}, u32[]{:S(2)}, u32[]{:S(2)}) collective-permute-start(bf16[1,256,512]{2,1,0:T(8,128)(2,1)S(1)} %add_convert_fusion.2), channel_id=1, source_target_pairs={{16,0},{0,16},{17,1},{1,17},{18,2},{2,18},{19,3},{3,19},{20,4},{4,... | collective-permute-start | bytes 786440 | tf_op jit(solution)/shard_map/ppermute | solution.py:82
  276.4 21.2 %collective-permute-start.64 = (bf16[1,256,256]{2,1,0:T(8,128)(2,1)S(1)}, bf16[1,256,256]{2,1,0:T(8,128)(2,1)S(1)}, u32[]{:S(2)}, u32[]{:S(2)}) collective-permute-start(bf16[1,256,256]{2,1,0:T(8,128)(2,1)S(1)} %add_convert_fusion.4), channel_id=1, source_target_pairs={{16,0},{0,16},{17,1},{1,17},{18,2},{2,18},{19,3},{3,19},{20,4},{4,... | collective-permute-start | bytes 393224 | tf_op jit(solution)/shard_map/ppermute | solution.py:82
  (123 other events, 2240.6 us)
where the time goes:
time: 304 us; the launch traced here: 303 us
  waiting for transfers between devices  123 us (40%)
  Pallas kernels  93.3 us (31%)
  starting transfers between devices  67.2 us (22%)
  local copies, waits for them, and re-layouts  12.7 us (4%)
  other arithmetic  5.42 us (2%)
    ppermute x21, waiting for transfers between devices, ring_gather(): ahead[h] = lax.ppermute(ahead[h], 'fs', fwd)  83.2 us
    ppermute x21, starting transfers between devices, ring_gather(): behind[h] = lax.ppermute(behind[h], 'fs', bwd)  26.4 us
    ppermute x24, starting transfers between devices, shift(): lax.ppermute(value, axis, [((i + by) % count, i) for i in range(count)])  22.6 us
    pallas_call x5, Pallas kernels, down_project(): pl.pallas_call(functools.partial(down_kernel, len(held), len(acts)), in_s...  22.4 us
    ppermute x24, waiting for transfers between devices, shift(): lax.ppermute(value, axis, [((i + by) % count, i) for i in range(count)])  21.6 us
    pallas_call x2, Pallas kernels, up_project(): pl.pallas_call(functools.partial(up_kernel, steps, len(xs)), grid_spec=pl...  20 us
    ppermute x21, waiting for transfers between devices, ring_gather(): behind[h] = lax.ppermute(behind[h], 'fs', bwd)  18.6 us
    ppermute x21, starting transfers between devices, ring_gather(): ahead[h] = lax.ppermute(ahead[h], 'fs', fwd)  18.2 us
  transfers between devices with their start and end apart: 66, of which 23 were waited for; matrix products, arithmetic and copies ran while one was open for 3% of the time, Pallas kernels for 29%

commit v1 on v0

--- a/solution.py
+++ b/solution.py
@@ -16,7 +16,7 @@
 F32 = jnp.float32
 LANES = 128
 TIME_PAD = 8
-VMEM_LIMIT = 56 * 1024 * 1024
+VMEM_LIMIT = 24 * 1024 * 1024
 
 
 def rms_rows(values, gain_vector):
@@ -27,8 +27,8 @@
     )
 
 
-def params(**kw):
-    return pltpu.CompilerParams(vmem_limit_bytes=VMEM_LIMIT, **kw)
+def params(limit=VMEM_LIMIT):
+    return pltpu.CompilerParams(vmem_limit_bytes=limit)
 
 
 def cost(flops, bytes_accessed, transcendentals=0):
@@ -89,24 +89,58 @@
     return got
 
 
-def fetch(order, chunks, weights, first, cols, sems):
-    copies = []
-    for s, chunk in enumerate(chunks):
-        rows = chunk.shape[0]
-        at = pl.multiple_of(order[s] * rows, rows)
-        copies.append(
-            pltpu.make_async_copy(
-                chunk.at[:, 0:cols], weights.at[pl.ds(at, rows), first : first + cols], sems.at[s]
-            )
-        )
+def prepare_kernel(rep, x, gate, out, pre, scale, first, second, x_own, gate_own, out_own, sems):
+    rows, cols = x_own.shape
+    half = cols // 2
+    wide = pl.ds(pl.multiple_of(rep[0] * cols, cols), cols)
+    copies = [
+        pltpu.make_async_copy(x.at[:, wide], x_own, sems.at[0]),
+        pltpu.make_async_copy(gate.at[:, wide], gate_own, sems.at[1]),
+        pltpu.make_async_copy(out.at[wide, :], out_own, sems.at[2]),
+    ]
     for copy in copies:
         copy.start()
-    return copies
-
-
-def wait_all(copies):
-    for copy in copies:
+    gains = jnp.transpose(jnp.broadcast_to(pre[...], (LANES, rows)))
+    for copy, own, to in ((copies[0], x_own, first), (copies[1], gate_own, second)):
         copy.wait()
+        for at in range(0, cols, LANES):
+            to[:, at : at + LANES] = (own[:, at : at + LANES] * gains).astype(BF16)
+    copies[2].wait()
+    first[:, cols:] = (out_own[:half, :] * scale[...]).astype(BF16)
+    second[:, cols:] = (out_own[half:, :] * scale[...]).astype(BF16)
+
+
+def prepare(rep, reps, x, gate, out, pre, scale):
+    rows, cols = x.shape[0], x.shape[1] // reps
+    shape = (rows, cols + out.shape[1])
+    vmem = pl.BlockSpec(memory_space=pltpu.VMEM)
+    hbm = pl.BlockSpec(memory_space=pltpu.HBM)
+    return pl.pallas_call(
+        prepare_kernel,
+        grid_spec=pltpu.PrefetchScalarGridSpec(
+            num_scalar_prefetch=1,
+            grid=(),
+            in_specs=[hbm] * 3 + [vmem] * 2,
+            out_specs=[vmem] * 2,
+            scratch_shapes=[
+                pltpu.VMEM((rows, cols), F32),
+                pltpu.VMEM((rows, cols), F32),
+                pltpu.VMEM((cols, out.shape[1]), F32),
+                pltpu.SemaphoreType.DMA((3,)),
+            ],
+        ),
+        out_shape=[jax.ShapeDtypeStruct(shape, BF16)] * 2,
+        compiler_params=params(62 * 1024 * 1024),
+        cost_estimate=cost(1e6, 12 * rows * cols + 8 * rows * out.shape[1]),
+        name="prepare",
+    )(rep, x, gate, out, pre, scale)
+
+
+def in_order(x, order, rows):
+    steps = x.shape[1] // rows
+    return jnp.concatenate(
+        [x[:, pl.ds(pl.multiple_of(order[s] * rows, rows), rows)] for s in range(steps)], axis=1
+    )
 
 
 def norm_kernel(count, tp, *refs):
@@ -139,17 +173,13 @@
 
 
 def project_kernel(steps, order, normed, scale, *refs):
-    xs, gs = refs[:steps], refs[steps : 2 * steps]
-    x_out, gate_out, x_full, gate_full, sems = refs[2 * steps :]
-    cols = x_out.shape[1]
-    x_copies = fetch(order, xs, x_full, 0, cols, sems.at[0])
-    gate_copies = fetch(order, gs, gate_full, 0, cols, sems.at[1])
-    wait_all(x_copies)
-    total = jnp.dot(normed[...], x_full[...], preferred_element_type=F32)
-    x_out[...] = (total * scale[:, :cols]).astype(BF16)
-    wait_all(gate_copies)
-    total = jnp.dot(normed[...], gate_full[...], preferred_element_type=F32)
-    gate_out[...] = (total * scale[:, cols:]).astype(BF16)
+    outs = refs[2 * steps :]
+    rows, cols = refs[0].shape[0], outs[0].shape[1]
+    x = in_order(normed, order, rows)
+    for h, out in enumerate(outs):
+        full = jnp.concatenate([c[:, :cols] for c in refs[h * steps : (h + 1) * steps]], axis=0)
+        total = jnp.dot(x, full, preferred_element_type=F32)
+        out[...] = (total * scale[:, h * cols : (h + 1) * cols]).astype(BF16)
 
 
 def project(order, normed, scale, held):
@@ -158,19 +188,13 @@
     cols = scale.shape[1] // 2
     out = jax.ShapeDtypeStruct((length, cols), BF16)
     vmem = pl.BlockSpec(memory_space=pltpu.VMEM)
-    hbm = pl.BlockSpec(memory_space=pltpu.HBM)
     return pl.pallas_call(
         functools.partial(project_kernel, steps),
         grid_spec=pltpu.PrefetchScalarGridSpec(
             num_scalar_prefetch=1,
             grid=(),
-            in_specs=[vmem, vmem] + [hbm] * (2 * steps),
+            in_specs=[vmem] * (2 + 2 * steps),
             out_specs=[vmem, vmem],
-            scratch_shapes=[
-                pltpu.VMEM((width, cols), BF16),
-                pltpu.VMEM((width, cols), BF16),
-                pltpu.SemaphoreType.DMA((2, steps)),
-            ],
         ),
         out_shape=[out, out],
         compiler_params=params(),
@@ -249,11 +273,11 @@
     )(x_branch, gate_branch, conv_weight, maps, rate)
 
 
-def out_kernel(steps, order, mixed, *refs):
+def out_kernel(steps, cols, order, mixed, *refs):
     top, low = refs[:steps], refs[steps : 2 * steps]
     outs = refs[2 * steps :]
     tps, share = len(outs), outs[0].shape[1]
-    half, cols = top[0].shape
+    half = top[0].shape[0]
     pieces = []
     for j in range(tps):
         at = pl.multiple_of((order[steps] + j) % tps * share, share)
@@ -261,32 +285,31 @@
     m = jnp.concatenate(pieces, axis=0)
     for s in range(steps):
         at = pl.multiple_of(order[s] * cols, cols)
-        part = jnp.dot(m[:, :half], top[s][...], preferred_element_type=F32)
-        part = part + jnp.dot(m[:, half:], low[s][...], preferred_element_type=F32)
+        part = jnp.dot(m[:, :half], top[s][:, -cols:], preferred_element_type=F32)
+        part = part + jnp.dot(m[:, half:], low[s][:, -cols:], preferred_element_type=F32)
         for j, out in enumerate(outs):
             out[0, :, pl.ds(at, cols)] = part[j * share : (j + 1) * share].astype(BF16)
 
 
 def out_project(order, tp, tps, mixed, held, cols):
     steps = len(held)
-    seqs, length, width = mixed.shape
+    _, length, width = mixed.shape
     share = length // tps
-    scalars = jnp.concatenate([order, tp.astype(jnp.int32).reshape(1)])
-    chunk = pl.BlockSpec((width // 2, cols), lambda *_: (0, width // cols))
-    row = lambda rows, n: pl.BlockSpec((1, rows, n), lambda i, *_: (i, 0, 0))
-    return pl.pallas_call(
-        functools.partial(out_kernel, steps),
+    scalars = jnp.concatenate([order, tp])
+    vmem = pl.BlockSpec(memory_space=pltpu.VMEM)
+    return pl.pallas_call(
+        functools.partial(out_kernel, steps, cols),
         grid_spec=pltpu.PrefetchScalarGridSpec(
             num_scalar_prefetch=1,
-            grid=(seqs,),
-            in_specs=[row(length, width)] + [chunk] * (2 * steps),
-            out_specs=[row(share, steps * cols)] * tps,
-        ),
-        out_shape=[jax.ShapeDtypeStruct((seqs, share, steps * cols), BF16)] * tps,
+            grid=(),
+            in_specs=[vmem] * (1 + 2 * steps),
+            out_specs=[vmem] * tps,
+        ),
+        out_shape=[jax.ShapeDtypeStruct((1, share, steps * cols), BF16)] * tps,
         compiler_params=params(),
         cost_estimate=cost(
-            2 * seqs * length * width * steps * cols,
-            2 * (width * steps * cols + seqs * length * (width + steps * cols)),
+            2 * length * width * steps * cols,
+            2 * (width * steps * cols + length * (width + steps * cols)),
         ),
         name="out_project",
     )(scalars, mixed, *[h[0] for h in held], *[h[1] for h in held])
@@ -342,17 +365,14 @@
 
 
 def up_kernel(steps, blocks, order, scale, *refs):
-    first, second = refs[:steps], refs[steps : 2 * steps]
     xs = refs[2 * steps : 2 * steps + blocks]
-    out, first_full, second_full, sems = refs[2 * steps + blocks :]
-    cols = first[0].shape[1]
-    x = jnp.concatenate([ref[...] for ref in xs], axis=0)
-    ready = [fetch(order, first, first_full, 0, cols, sems.at[0])]
-    ready.append(fetch(order, second, second_full, 0, cols, sems.at[1]))
-    for w, full in enumerate((first_full, second_full)):
-        wait_all(ready[w])
-        span = slice(w * cols, (w + 1) * cols)
-        total = jnp.dot(x, full[...], preferred_element_type=F32)
+    out = refs[-1]
+    rows, cols = refs[0].shape
+    x = jnp.concatenate([in_order(ref, order, rows) for ref in xs], axis=0)
+    for h in range(2):
+        full = jnp.concatenate([c[...] for c in refs[h * steps : (h + 1) * steps]], axis=0)
+        span = slice(h * cols, (h + 1) * cols)
+        total = jnp.dot(x, full, preferred_element_type=F32)
         total = jnp.maximum(total * scale[:, span], 0.0)
         out[:, span] = (total * total).astype(BF16)
 
@@ -362,19 +382,13 @@
     rows, width = xs[0].shape
     cols = held[0][0].shape[1]
     vmem = pl.BlockSpec(memory_space=pltpu.VMEM)
-    hbm = pl.BlockSpec(memory_space=pltpu.HBM)
     return pl.pallas_call(
         functools.partial(up_kernel, steps, len(xs)),
         grid_spec=pltpu.PrefetchScalarGridSpec(
             num_scalar_prefetch=1,
             grid=(),
-            in_specs=[vmem] + [hbm] * (2 * steps) + [vmem] * len(xs),
+            in_specs=[vmem] * (1 + 2 * steps + len(xs)),
             out_specs=vmem,
-            scratch_shapes=[
-                pltpu.VMEM((width, cols), BF16),
-                pltpu.VMEM((width, cols), BF16),
-                pltpu.SemaphoreType.DMA((2, steps)),
-            ],
         ),
         out_shape=jax.ShapeDtypeStruct((len(xs) * rows, 2 * cols), BF16),
         compiler_params=params(),
@@ -507,17 +521,11 @@
     def rep_part(value, size, axis):
         return lax.dynamic_slice_in_dim(value, rep * size, size, axis)
 
-    pre = gain_mix_pre[:, None]
-    out_mine = rep_part(out_weight, chan, 0) * out_scale
-    mixer = ring_gather(
-        jnp.concatenate(
-            [rep_part(x_weight, chan, 1) * pre, out_mine[: chan // 2]], axis=1
-        ).astype(BF16),
-        jnp.concatenate(
-            [rep_part(gate_weight, chan, 1) * pre, out_mine[chan // 2 :]], axis=1
-        ).astype(BF16),
-        count,
-    )
+    rep_scalar, tp_scalar, me_scalar = (i.astype(jnp.int32).reshape(1) for i in (rep, tp, me))
+    halves = prepare(
+        rep_scalar, reps, x_weight, gate_weight, out_weight, gain_mix_pre[None], out_scale[None]
+    )
+    mixer = ring_gather(*halves, count)
     up_mine = (rep_part(up_weight, hid, 1) * gain_mlp_pre[:, None]).astype(BF16)
     ups = ring_gather(up_mine[:, : hid // 2], up_mine[:, hid // 2 :], count)
     down_mine = (rep_part(down_weight, hid, 0) * down_scale).astype(BF16)
@@ -530,7 +538,6 @@
         seqs.append([shift(mine, "rep", reps, dr)])
         for dt in range(1, tps):
             seqs[dr].append(shift(seqs[dr][0], "tp", tps, dt))
-    tp_scalar = tp.astype(jnp.int32).reshape(1)
     normed_in = []
     for dr, pieces in enumerate(seqs):
         normed_in.append(normalize(tp_scalar if dr else 0 * tp_scalar, pieces))
@@ -563,10 +570,10 @@
     for dr in far_first:
         x_branch, gate_branch = project(order, normed_in[dr], scales, mixer)
         mixed = recur(x_branch[None], gate_branch[None], taps, maps, rate)
-        parts = out_project(order, tp, tps, mixed, mixer, width // count)
+        parts = out_project(order, tp_scalar, tps, mixed, mixer, width // count)
         summands = over_tp(parts)
         pieces += [over_rep(summands, dr)] if dr else summands
-    hidden, normed = mid(me.astype(jnp.int32).reshape(1), mine, pieces, gains)
+    hidden, normed = mid(me_scalar, mine, pieces, gains)
 
     scale = rep_part(up_scale, hid, 0)[None]
     acts = []
@@ -601,7 +608,7 @@
         for i in range(len(rows_of[dr][0])):
             streams.append(group_sizes(count)[0 if dr else 1])
             arrays.append([group[i] for group in rows_of[dr]])
-    scalars = jnp.concatenate([order, me.astype(jnp.int32).reshape(1)])
+    scalars = jnp.concatenate([order, me_scalar])
     return last(scalars, hidden, tuple(streams), arrays, gains)[None]
 
 

time: 304 us -> 255 us (0.84)
  Pallas kernels: 93.3 us -> 40.8 us
  waiting for transfers between devices: 123 us -> 139 us
  local copies, waits for them, and re-layouts: 12.7 us -> 3.76 us
    pallas_call x5, Pallas kernels: 22.4 us -> 7.32 us  [down_project(): pl.pallas_call(functools.partial(down_kernel, len(held), len(acts)), in_s...]
    pallas_call x2, Pallas kernels: 20 us -> 7.97 us  [up_project(): pl.pallas_call(functools.partial(up_kernel, steps, len(xs)), grid_spec=pl...]
    ppermute x21, starting transfers between devices: 26.4 us -> 15.5 us  [ring_gather(): behind[h] = lax.ppermute(behind[h], 'fs', bwd)]
    ppermute x21, waiting for transfers between devices: 83.2 us -> 93.8 us  [ring_gather(): ahead[h] = lax.ppermute(ahead[h], 'fs', fwd)]
    pallas_call x2, Pallas kernels: 14.5 us -> 5.8 us  [project(): pl.pallas_call(functools.partial(project_kernel, steps), grid_spec=pltpu....]
    unnamed x179 -> x35, local copies, waits for them, and re-layouts: 6.96 us -> 0.09 us
    ppermute x21, starting transfers between devices: 18.2 us -> 24.6 us  [ring_gather(): ahead[h] = lax.ppermute(ahead[h], 'fs', fwd)]
    pallas_call x2, Pallas kernels: 7 us -> 1.39 us  [normalize(): pl.pallas_call(functools.partial(norm_kernel, count), grid_spec=pltpu.Pre...]
  transfers between devices with their start and end apart: 66 -> 66, of which waited for: 23 -> 28; matrix products, arithmetic and copies ran while one was open for 3% -> 2% of each run, Pallas kernels for 29% -> 15%
where the time goes in v1:
time: 255 us; the launch traced here: 254 us
  waiting for transfers between devices  139 us (55%)
  starting transfers between devices  66.2 us (26%)
  Pallas kernels  40.8 us (16%)
  other arithmetic  4.4 us (2%)
  local copies, waits for them, and re-layouts  3.76 us (1%)
    ppermute x21, waiting for transfers between devices, ring_gather(): ahead[h] = lax.ppermute(ahead[h], 'fs', fwd)  93.8 us
    ppermute x24, starting transfers between devices, shift(): lax.ppermute(value, axis, [((i + by) % count, i) for i in range(count)])  26.2 us
    ppermute x21, starting transfers between devices, ring_gather(): ahead[h] = lax.ppermute(ahead[h], 'fs', fwd)  24.6 us
    ppermute x21, waiting for transfers between devices, ring_gather(): behind[h] = lax.ppermute(behind[h], 'fs', bwd)  23.5 us
    ppermute x24, waiting for transfers between devices, shift(): lax.ppermute(value, axis, [((i + by) % count, i) for i in range(count)])  21.4 us
    ppermute x21, starting transfers between devices, ring_gather(): behind[h] = lax.ppermute(behind[h], 'fs', bwd)  15.5 us
    pallas_call x2, Pallas kernels, up_project(): pl.pallas_call(functools.partial(up_kernel, steps, len(xs)), grid_spec=pl...  7.97 us
    pallas_call x5, Pallas kernels, down_project(): pl.pallas_call(functools.partial(down_kernel, len(held), len(acts)), in_s...  7.32 us
  transfers between devices with their start and end apart: 66, of which 28 were waited for; matrix products, arithmetic and copies ran while one was open for 2% of the time, Pallas kernels for 15%

profile of v1, /device:TPU:0, one launch (start us, length us, event | category | flops | bytes accessed | tf_op | source)
XLA Modules:
  0.0 254.4 jit_solution(4144959917689045207)
XLA Ops:
  2.4 3.0 %collective-permute-start = (bf16[256,2048]{1,0:T(8,128)(2,1)}, bf16[256,2048]{1,0:T(8,128)(2,1)S(1)}, u32[]{:S(2)}, u32[]{:S(2)}) collective-permute-start(bf16[256,2048]{1,0:T(8,128)(2,1)} %dynamic-slice_bitcast_fusion.tokens), channel_id=1, source_target_pairs={{16,0},{0,16},{17,1},{1,17},{18,2},{2,18},{19,3},{3,19},{20,4},{4,... | collective-permute-start | bytes 3145736 | tf_op jit(solution)/shard_map/ppermute | solution.py:82
  5.4 3.0 %prepare.1 = (bf16[256,768]{1,0:T(8,128)(2,1)}, bf16[256,768]{1,0:T(8,128)(2,1)}) custom-call(s32[1]{0:T(128)} %bitcast.5.rep, f32[256,1024]{1,0:T(8,128)} %x.1, f32[256,1024]{1,0:T(8,128)} %gate.1, f32[1024,256]{1,0:T(8,128)} %out.1, f32[1,256]{1,0:T(1,128)} %bitcast.44, f32[1,256]{1,0:T(1,128)} %bitcast.45), custom_call_target="tpu_custom_call" | custom-call | flops 1000000 | bytes 2097152 | tf_op jit(solution)/shard_map/prepare/pallas_call | solution.py:118
  13.9 6.7 %collective-permute-done.2.refs_1_ = bf16[256,768]{1,0:T(8,128)(2,1)S(1)} collective-permute-done((bf16[256,768]{1,0:T(8,128)(2,1)}, bf16[256,768]{1,0:T(8,128)(2,1)S(1)}, u32[]{:S(2)}, u32[]{:S(2)}) %collective-permute-start.2) | collective-permute-done | bytes 393248 | tf_op jit(solution)/shard_map/ppermute | solution.py:73
  22.2 6.7 %collective-permute-done.10.refs_10_ = bf16[256,768]{1,0:T(8,128)(2,1)S(1)} collective-permute-done((bf16[256,768]{1,0:T(8,128)(2,1)}, bf16[256,768]{1,0:T(8,128)(2,1)S(1)}, u32[]{:S(2)}, u32[]{:S(2)}) %collective-permute-start.10) | collective-permute-done | bytes 393248 | tf_op jit(solution)/shard_map/ppermute | solution.py:75
  33.5 3.1 %collective-permute-done.4.refs_3_ = bf16[256,768]{1,0:T(8,128)(2,1)S(1)} collective-permute-done((bf16[256,768]{1,0:T(8,128)(2,1)S(1)}, bf16[256,768]{1,0:T(8,128)(2,1)S(1)}, u32[]{:S(2)}, u32[]{:S(2)}) %collective-permute-start.4) | collective-permute-done | bytes 393248 | tf_op jit(solution)/shard_map/ppermute | solution.py:73
  43.0 6.4 %collective-permute-done.5.refs_4_ = bf16[256,768]{1,0:T(8,128)(2,1)S(1)} collective-permute-done((bf16[256,768]{1,0:T(8,128)(2,1)S(1)}, bf16[256,768]{1,0:T(8,128)(2,1)S(1)}, u32[]{:S(2)}, u32[]{:S(2)}) %collective-permute-start.5) | collective-permute-done | bytes 393248 | tf_op jit(solution)/shard_map/ppermute | solution.py:75
  59.0 4.6 %collective-permute-start.19 = (f32[2,256]{1,0:T(2,128)S(1)}, f32[2,256]{1,0:T(2,128)S(1)}, u32[]{:S(2)}, u32[]{:S(2)}) collective-permute-start(f32[2,256]{1,0:T(2,128)S(1)} %pad_maximum_fusion.2.refs_3_.refs_8_), channel_id=1, source_target_pairs={{2,0},{4,2},{6,4},{8,6},{10,8},{12,10},{14,12},{0,14},{3,1},{5,3},... | collective-permute-start | bytes 6152 | tf_op jit(solution)/shard_map/ppermute | solution.py:82
  66.2 3.5 %collective-permute-start.20 = (f32[2,256]{1,0:T(2,128)S(1)}, f32[2,256]{1,0:T(2,128)S(1)}, u32[]{:S(2)}, u32[]{:S(2)}) collective-permute-start(f32[2,256]{1,0:T(2,128)S(1)} %pad_maximum_fusion.2.refs_3_.refs_8_), channel_id=1, source_target_pairs={{4,0},{6,2},{8,4},{10,6},{12,8},{14,10},{0,12},{2,14},{5,1},{7,3},... | collective-permute-start | bytes 6152 | tf_op jit(solution)/shard_map/ppermute | solution.py:82
  69.8 2.8 %collective-permute-start.22 = (f32[2,256]{1,0:T(2,128)S(1)}, f32[2,256]{1,0:T(2,128)S(1)}, u32[]{:S(2)}, u32[]{:S(2)}) collective-permute-start(f32[2,256]{1,0:T(2,128)S(1)} %pad_maximum_fusion.2.refs_3_.refs_8_), channel_id=1, source_target_pairs={{8,0},{10,2},{12,4},{14,6},{0,8},{2,10},{4,12},{6,14},{9,1},{11,3}... | collective-permute-start | bytes 6152 | tf_op jit(solution)/shard_map/ppermute | solution.py:82
  72.6 2.9 %project.2 = (bf16[512,512]{1,0:T(8,128)(2,1)S(1)}, bf16[512,512]{1,0:T(8,128)(2,1)S(1)}) custom-call(s32[8]{0:T(128)S(1)} %fusion.1.order, bf16[512,2048]{1,0:T(8,128)(2,1)S(1)} %normalize.2.normed, f32[1,1024]{1,0:T(1,128)S(1)} %bitcast.32, bf16[256,768]{1,0:T(8,128)(2,1)S(1)} %copy-done.2, bf16[256,768]{1,0:T(8,128)(2,1)S(1)} %collective-permute-done.2.refs_1_, ...), custom_call_target="tpu_custom_call" | custom-call | flops 2147483648 | bytes 6291456 | tf_op jit(solution)/shard_map/project/pallas_call | solution.py:191
  75.5 3.3 %recur.2.mixed = bf16[1,512,512]{2,1,0:T(8,128)(2,1)S(1)} custom-call(bf16[1,512,512]{2,1,0:T(8,128)(2,1)S(1)} %bitcast.38, bf16[1,512,512]{2,1,0:T(8,128)(2,1)S(1)} %bitcast.39, f32[4,512]{1,0:T(4,128)S(1)} %constant_dynamic-slice_fusion.conv_ref, bf16[4,128,256]{2,1,0:T(8,128)(2,1)S(1)} %pad_maximum_fusion.maps_ref, f32[1,512]{1,0:T(1,128)S(1)} %bitcast.34), custom_call_target="tpu_custom_call" | custom-call | flops 3000000000 | bytes 1572864 | tf_op jit(solution)/shard_map/recur/pallas_call | solution.py:260
  81.0 2.9 %project.3 = (bf16[512,512]{1,0:T(8,128)(2,1)S(1)}, bf16[512,512]{1,0:T(8,128)(2,1)S(1)}) custom-call(s32[8]{0:T(128)S(1)} %fusion.1.order, bf16[512,2048]{1,0:T(8,128)(2,1)S(1)} %normalize.3.normed, f32[1,1024]{1,0:T(1,128)S(1)} %bitcast.33, bf16[256,768]{1,0:T(8,128)(2,1)S(1)} %copy-done.2, bf16[256,768]{1,0:T(8,128)(2,1)S(1)} %collective-permute-done.2.refs_1_, ...), custom_call_target="tpu_custom_call" | custom-call | flops 2147483648 | bytes 6291456 | tf_op jit(solution)/shard_map/project/pallas_call | solution.py:191
  83.9 3.3 %recur.3.mixed = bf16[1,512,512]{2,1,0:T(8,128)(2,1)S(1)} custom-call(bf16[1,512,512]{2,1,0:T(8,128)(2,1)S(1)} %bitcast.36, bf16[1,512,512]{2,1,0:T(8,128)(2,1)S(1)} %bitcast.37, f32[4,512]{1,0:T(4,128)S(1)} %constant_dynamic-slice_fusion.conv_ref, bf16[4,128,256]{2,1,0:T(8,128)(2,1)S(1)} %pad_maximum_fusion.maps_ref, f32[1,512]{1,0:T(1,128)S(1)} %bitcast.35), custom_call_target="tpu_custom_call" | custom-call | flops 3000000000 | bytes 1572864 | tf_op jit(solution)/shard_map/recur/pallas_call | solution.py:260
  91.8 2.6 %collective-permute-start.25 = (f32[2,256]{1,0:T(2,128)S(1)}, f32[2,256]{1,0:T(2,128)S(1)}, u32[]{:S(2)}, u32[]{:S(2)}) collective-permute-start(f32[2,256]{1,0:T(2,128)S(1)} %pad_maximum_fusion.2.refs_3_.refs_8_), channel_id=1, source_target_pairs={{14,0},{0,2},{2,4},{4,6},{6,8},{8,10},{10,12},{12,14},{15,1},{1,3}... | collective-permute-start | bytes 6152 | tf_op jit(solution)/shard_map/ppermute | solution.py:82
  98.9 7.5 %collective-permute-done.26.refs_1_ = bf16[256,768]{1,0:T(8,128)(2,1)S(1)} collective-permute-done((bf16[256,768]{1,0:T(8,128)(2,1)S(1)}, bf16[256,768]{1,0:T(8,128)(2,1)S(1)}, u32[]{:S(2)}, u32[]{:S(2)}) %collective-permute-start.26) | collective-permute-done | bytes 393248 | tf_op jit(solution)/shard_map/ppermute | solution.py:73
  107.8 7.0 %collective-permute-done.33.refs_9_ = bf16[256,768]{1,0:T(8,128)(2,1)S(1)} collective-permute-done((bf16[256,768]{1,0:T(8,128)(2,1)S(1)}, bf16[256,768]{1,0:T(8,128)(2,1)S(1)}, u32[]{:S(2)}, u32[]{:S(2)}) %collective-permute-start.33) | collective-permute-done | bytes 393248 | tf_op jit(solution)/shard_map/ppermute | solution.py:73
  116.9 6.4 %collective-permute-done.42.refs_3_ = bf16[768,256]{1,0:T(8,128)(2,1)S(1)} collective-permute-done((bf16[768,256]{1,0:T(8,128)(2,1)S(1)}, bf16[768,256]{1,0:T(8,128)(2,1)S(1)}, u32[]{:S(2)}, u32[]{:S(2)}) %collective-permute-start.42) | collective-permute-done | bytes 393248 | tf_op jit(solution)/shard_map/ppermute | solution.py:73
  123.7 6.7 %collective-permute-done.43.refs_4_ = bf16[768,256]{1,0:T(8,128)(2,1)S(1)} collective-permute-done((bf16[768,256]{1,0:T(8,128)(2,1)S(1)}, bf16[768,256]{1,0:T(8,128)(2,1)S(1)}, u32[]{:S(2)}, u32[]{:S(2)}) %collective-permute-start.43) | collective-permute-done | bytes 393248 | tf_op jit(solution)/shard_map/ppermute | solution.py:73
  133.1 9.2 %collective-permute-done.28.refs_3_ = bf16[256,768]{1,0:T(8,128)(2,1)S(1)} collective-permute-done((bf16[256,768]{1,0:T(8,128)(2,1)S(1)}, bf16[256,768]{1,0:T(8,128)(2,1)S(1)}, u32[]{:S(2)}, u32[]{:S(2)}) %collective-permute-start.28) | collective-permute-done | bytes 393248 | tf_op jit(solution)/shard_map/ppermute | solution.py:73
  147.6 3.2 %collective-permute-done.35.refs_11_ = bf16[256,768]{1,0:T(8,128)(2,1)S(1)} collective-permute-done((bf16[256,768]{1,0:T(8,128)(2,1)S(1)}, bf16[256,768]{1,0:T(8,128)(2,1)S(1)}, u32[]{:S(2)}, u32[]{:S(2)}) %collective-permute-start.35) | collective-permute-done | bytes 393248 | tf_op jit(solution)/shard_map/ppermute | solution.py:73
  152.9 6.3 %collective-permute-done.48.refs_1_.refs_7_ = bf16[768,256]{1,0:T(8,128)(2,1)S(1)} collective-permute-done((bf16[768,256]{1,0:T(8,128)(2,1)S(1)}, bf16[768,256]{1,0:T(8,128)(2,1)S(1)}, u32[]{:S(2)}, u32[]{:S(2)}) %collective-permute-start.48) | collective-permute-done | bytes 393248 | tf_op jit(solution)/shard_map/ppermute | solution.py:73
  159.5 8.1 %collective-permute-done.49.refs_2_.refs_8_ = bf16[768,256]{1,0:T(8,128)(2,1)S(1)} collective-permute-done((bf16[768,256]{1,0:T(8,128)(2,1)S(1)}, bf16[768,256]{1,0:T(8,128)(2,1)S(1)}, u32[]{:S(2)}, u32[]{:S(2)}) %collective-permute-start.49) | collective-permute-done | bytes 393248 | tf_op jit(solution)/shard_map/ppermute | solution.py:73
  169.7 6.3 %collective-permute-done.30.refs_5_ = bf16[256,768]{1,0:T(8,128)(2,1)S(1)} collective-permute-done((bf16[256,768]{1,0:T(8,128)(2,1)S(1)}, bf16[256,768]{1,0:T(8,128)(2,1)S(1)}, u32[]{:S(2)}, u32[]{:S(2)}) %collective-permute-start.30) | collective-permute-done | bytes 393248 | tf_op jit(solution)/shard_map/ppermute | solution.py:73
  178.1 6.4 %collective-permute-done.37.refs_13_ = bf16[256,768]{1,0:T(8,128)(2,1)S(1)} collective-permute-done((bf16[256,768]{1,0:T(8,128)(2,1)S(1)}, bf16[256,768]{1,0:T(8,128)(2,1)S(1)}, u32[]{:S(2)}, u32[]{:S(2)}) %collective-permute-start.37) | collective-permute-done | bytes 393248 | tf_op jit(solution)/shard_map/ppermute | solution.py:73
  186.5 6.4 %collective-permute-done.54.refs_1_.refs_11_ = bf16[768,256]{1,0:T(8,128)(2,1)S(1)} collective-permute-done((bf16[768,256]{1,0:T(8,128)(2,1)S(1)}, bf16[768,256]{1,0:T(8,128)(2,1)S(1)}, u32[]{:S(2)}, u32[]{:S(2)}) %collective-permute-start.54) | collective-permute-done | bytes 393248 | tf_op jit(solution)/shard_map/ppermute | solution.py:73
  194.9 6.4 %collective-permute-done.32.refs_7_ = bf16[256,768]{1,0:T(8,128)(2,1)S(1)} collective-permute-done((bf16[256,768]{1,0:T(8,128)(2,1)S(1)}, bf16[256,768]{1,0:T(8,128)(2,1)S(1)}, u32[]{:S(2)}, u32[]{:S(2)}) %collective-permute-start.32) | collective-permute-done | bytes 393248 | tf_op jit(solution)/shard_map/ppermute | solution.py:73
  203.7 4.0 %up_project.3.refs_1_.refs_0_ = bf16[512,1536]{1,0:T(8,128)(2,1)S(1)} custom-call(s32[8]{0:T(128)S(1)} %fusion.1.order, f32[1,1536]{1,0:T(1,128)S(1)} %broadcast_in_dim.39.scale, bf16[256,768]{1,0:T(8,128)(2,1)S(1)} %get-tuple-element.52.refs_0_, bf16[256,768]{1,0:T(8,128)(2,1)S(1)} %collective-permute-done.26.refs_1_, ...), custom_call_target="tpu_custom_call" | custom-call | flops 3221225472 | bytes 9961472 | tf_op jit(solution)/shard_map/up_project/pallas_call | solution.py:385
  209.8 3.6 %collective-permute-done.56.refs_3_.refs_13_ = bf16[768,256]{1,0:T(8,128)(2,1)S(1)} collective-permute-done((bf16[768,256]{1,0:T(8,128)(2,1)S(1)}, bf16[768,256]{1,0:T(8,128)(2,1)S(1)}, u32[]{:S(2)}, u32[]{:S(2)}) %collective-permute-start.56) | collective-permute-done | bytes 393248 | tf_op jit(solution)/shard_map/ppermute | solution.py:75
  213.3 3.0 %down_project.9 = (bf16[1,256,1792]{2,1,0:T(8,128)(2,1)S(1)}, bf16[1,256,1792]{2,1,0:T(8,128)(2,1)S(1)}) custom-call(bf16[512,1536]{1,0:T(8,128)(2,1)S(1)} %up_project.3.refs_1_.refs_0_, bf16[768,256]{1,0:T(8,128)(2,1)S(1)} %get-tuple-element.50.refs_1_, bf16[768,256]{1,0:T(8,128)(2,1)S(1)} %get-tuple-element.49.refs_2_, ...), custom_call_target="tpu_custom_call" | custom-call | flops 2818572288 | bytes 8912896 | tf_op jit(solution)/shard_map/down_project/pallas_call | solution.py:425
  216.4 4.0 %up_project.2.refs_0_ = bf16[512,1536]{1,0:T(8,128)(2,1)S(1)} custom-call(s32[8]{0:T(128)S(1)} %fusion.1.order, f32[1,1536]{1,0:T(1,128)S(1)} %broadcast_in_dim.39.scale, bf16[256,768]{1,0:T(8,128)(2,1)S(1)} %get-tuple-element.52.refs_0_, bf16[256,768]{1,0:T(8,128)(2,1)S(1)} %collective-permute-done.26.refs_1_, ...), custom_call_target="tpu_custom_call" | custom-call | flops 3221225472 | bytes 9961472 | tf_op jit(solution)/shard_map/up_project/pallas_call | solution.py:385
  230.7 21.1 %collective-permute-done.64.refs_3_ = bf16[1,256,256]{2,1,0:T(8,128)(2,1)S(1)} collective-permute-done((bf16[1,256,256]{2,1,0:T(8,128)(2,1)S(1)}, bf16[1,256,256]{2,1,0:T(8,128)(2,1)S(1)}, u32[]{:S(2)}, u32[]{:S(2)}) %collective-permute-start.64) | collective-permute-done | bytes 131104 | tf_op jit(solution)/shard_map/ppermute | solution.py:82
  251.8 2.6 %last.1 = bf16[256,2048]{1,0:T(8,128)(2,1)} custom-call(s32[9]{0:T(128)S(1)} %get-tuple-element.56.scalars, bf16[256,2048]{1,0:T(8,128)(2,1)S(1)} %get-tuple-element.37.hidden, bf16[1,256,768]{2,1,0:T(8,128)(2,1)S(1)} %collective-permute-done.47.refs_0_, bf16[1,256,512]{2,1,0:T(8,128)(2,1)S(1)} %collective-permute-done.53.refs_1_, ...), custom_call_target="tpu_custom_call" | custom-call | flops 1000000000 | bytes 5242880 | tf_op jit(solution)/shard_map/last/pallas_call | solution.py:470
  (181 shorter events, 80.9 us)
Async XLA Ops:
  2.4 27.8 %collective-permute-start = (bf16[256,2048]{1,0:T(8,128)(2,1)}, bf16[256,2048]{1,0:T(8,128)(2,1)S(1)}, u32[]{:S(2)}, u32[]{:S(2)}) collective-permute-start(bf16[256,2048]{1,0:T(8,128)(2,1)} %dynamic-slice_bitcast_fusion.tokens), channel_id=1, source_target_pairs={{16,0},{0,16},{17,1},{1,17},{18,2},{2,18},{19,3},{3,19},{20,4},{4,... | collective-permute-start | bytes 3145736 | tf_op jit(solution)/shard_map/ppermute | solution.py:82
  10.0 21.4 %collective-permute-start.3 = (bf16[256,768]{1,0:T(8,128)(2,1)}, bf16[256,768]{1,0:T(8,128)(2,1)S(1)}, u32[]{:S(2)}, u32[]{:S(2)}) collective-permute-start(bf16[256,768]{1,0:T(8,128)(2,1)} %get-tuple-element.27.refs_0_), channel_id=1, source_target_pairs={{4,0},{8,4},{12,8},{14,12},{10,14},{6,10},{2,6},{0,2},{5,1},{9,5},... | collective-permute-start | bytes 1179656 | tf_op jit(solution)/shard_map/ppermute | solution.py:75
  10.5 22.5 %collective-permute-start.9 = (bf16[256,768]{1,0:T(8,128)(2,1)}, bf16[256,768]{1,0:T(8,128)(2,1)S(1)}, u32[]{:S(2)}, u32[]{:S(2)}) collective-permute-start(bf16[256,768]{1,0:T(8,128)(2,1)} %get-tuple-element.28.refs_8_), channel_id=1, source_target_pairs={{0,4},{4,8},{8,12},{12,14},{14,10},{10,6},{6,2},{2,0},{1,5},{5,9},... | collective-permute-start | bytes 1179656 | tf_op jit(solution)/shard_map/ppermute | solution.py:73
  12.1 16.9 %collective-permute-start.10 = (bf16[256,768]{1,0:T(8,128)(2,1)}, bf16[256,768]{1,0:T(8,128)(2,1)S(1)}, u32[]{:S(2)}, u32[]{:S(2)}) collective-permute-start(bf16[256,768]{1,0:T(8,128)(2,1)} %get-tuple-element.28.refs_8_), channel_id=1, source_target_pairs={{4,0},{8,4},{12,8},{14,12},{10,14},{6,10},{2,6},{0,2},{5,1},{9,5},... | collective-permute-start | bytes 1179656 | tf_op jit(solution)/shard_map/ppermute | solution.py:75
  30.1 28.9 %collective-permute-start.1 = (bf16[256,2048]{1,0:T(8,128)(2,1)S(1)}, bf16[256,2048]{1,0:T(8,128)(2,1)S(1)}, u32[]{:S(2)}, u32[]{:S(2)}) collective-permute-start(bf16[256,2048]{1,0:T(8,128)(2,1)S(1)} %collective-permute-done.refs_0_), channel_id=1, source_target_pairs={{1,0},{0,1},{3,2},{2,3},{5,4},{4,5},{7,6},{6,7},{9,8},{8,9},{11,10... | collective-permute-start | bytes 3145736 | tf_op jit(solution)/shard_map/ppermute | solution.py:82
  31.4 18.0 %collective-permute-start.5 = (bf16[256,768]{1,0:T(8,128)(2,1)S(1)}, bf16[256,768]{1,0:T(8,128)(2,1)S(1)}, u32[]{:S(2)}, u32[]{:S(2)}) collective-permute-start(bf16[256,768]{1,0:T(8,128)(2,1)S(1)} %collective-permute-done.3.refs_2_), channel_id=1, source_target_pairs={{4,0},{8,4},{12,8},{14,12},{10,14},{6,10},{2,6},{0,2},{5,1},{9,5},... | collective-permute-start | bytes 1179656 | tf_op jit(solution)/shard_map/ppermute | solution.py:75
  36.6 16.9 %collective-permute-start.6 = (bf16[256,768]{1,0:T(8,128)(2,1)S(1)}, bf16[256,768]{1,0:T(8,128)(2,1)S(1)}, u32[]{:S(2)}, u32[]{:S(2)}) collective-permute-start(bf16[256,768]{1,0:T(8,128)(2,1)S(1)} %collective-permute-done.4.refs_3_), channel_id=1, source_target_pairs={{0,4},{4,8},{8,12},{12,14},{14,10},{10,6},{6,2},{2,0},{1,5},{5,9},... | collective-permute-start | bytes 1179656 | tf_op jit(solution)/shard_map/ppermute | solution.py:73
  41.0 16.9 %collective-permute-start.14 = (bf16[256,768]{1,0:T(8,128)(2,1)S(1)}, bf16[256,768]{1,0:T(8,128)(2,1)S(1)}, u32[]{:S(2)}, u32[]{:S(2)}) collective-permute-start(bf16[256,768]{1,0:T(8,128)(2,1)S(1)} %collective-permute-done.12.refs_12_), channel_id=1, source_target_pairs={{4,0},{8,4},{12,8},{14,12},{10,14},{6,10},{2,6},{0,2},{5,1},{9,5},... | collective-permute-start | bytes 1179656 | tf_op jit(solution)/shard_map/ppermute | solution.py:75
  49.4 16.9 %collective-permute-start.7 = (bf16[256,768]{1,0:T(8,128)(2,1)S(1)}, bf16[256,768]{1,0:T(8,128)(2,1)S(1)}, u32[]{:S(2)}, u32[]{:S(2)}) collective-permute-start(bf16[256,768]{1,0:T(8,128)(2,1)S(1)} %collective-permute-done.5.refs_4_), channel_id=1, source_target_pairs={{4,0},{8,4},{12,8},{14,12},{10,14},{6,10},{2,6},{0,2},{5,1},{9,5},... | collective-permute-start | bytes 1179656 | tf_op jit(solution)/shard_map/ppermute | solution.py:75
  49.8 19.9 %collective-permute-start.13 = (bf16[256,768]{1,0:T(8,128)(2,1)S(1)}, bf16[256,768]{1,0:T(8,128)(2,1)S(1)}, u32[]{:S(2)}, u32[]{:S(2)}) collective-permute-start(bf16[256,768]{1,0:T(8,128)(2,1)S(1)} %collective-permute-done.11.refs_11_), channel_id=1, source_target_pairs={{0,4},{4,8},{8,12},{12,14},{14,10},{10,6},{6,2},{2,0},{1,5},{5,9},... | collective-permute-start | bytes 1179656 | tf_op jit(solution)/shard_map/ppermute | solution.py:73
  59.0 28.2 %collective-permute-start.19 = (f32[2,256]{1,0:T(2,128)S(1)}, f32[2,256]{1,0:T(2,128)S(1)}, u32[]{:S(2)}, u32[]{:S(2)}) collective-permute-start(f32[2,256]{1,0:T(2,128)S(1)} %pad_maximum_fusion.2.refs_3_.refs_8_), channel_id=1, source_target_pairs={{2,0},{4,2},{6,4},{8,6},{10,8},{12,10},{14,12},{0,14},{3,1},{5,3},... | collective-permute-start | bytes 6152 | tf_op jit(solution)/shard_map/ppermute | solution.py:82
  66.2 25.4 %collective-permute-start.20 = (f32[2,256]{1,0:T(2,128)S(1)}, f32[2,256]{1,0:T(2,128)S(1)}, u32[]{:S(2)}, u32[]{:S(2)}) collective-permute-start(f32[2,256]{1,0:T(2,128)S(1)} %pad_maximum_fusion.2.refs_3_.refs_8_), channel_id=1, source_target_pairs={{4,0},{6,2},{8,4},{10,6},{12,8},{14,10},{0,12},{2,14},{5,1},{7,3},... | collective-permute-start | bytes 6152 | tf_op jit(solution)/shard_map/ppermute | solution.py:82
  69.8 22.0 %collective-permute-start.21 = (f32[2,256]{1,0:T(2,128)S(1)}, f32[2,256]{1,0:T(2,128)S(1)}, u32[]{:S(2)}, u32[]{:S(2)}) collective-permute-start(f32[2,256]{1,0:T(2,128)S(1)} %pad_maximum_fusion.2.refs_3_.refs_8_), channel_id=1, source_target_pairs={{6,0},{8,2},{10,4},{12,6},{14,8},{0,10},{2,12},{4,14},{7,1},{9,3},... | collective-permute-start | bytes 6152 | tf_op jit(solution)/shard_map/ppermute | solution.py:82
  69.8 24.6 %collective-permute-start.22 = (f32[2,256]{1,0:T(2,128)S(1)}, f32[2,256]{1,0:T(2,128)S(1)}, u32[]{:S(2)}, u32[]{:S(2)}) collective-permute-start(f32[2,256]{1,0:T(2,128)S(1)} %pad_maximum_fusion.2.refs_3_.refs_8_), channel_id=1, source_target_pairs={{8,0},{10,2},{12,4},{14,6},{0,8},{2,10},{4,12},{6,14},{9,1},{11,3}... | collective-permute-start | bytes 6152 | tf_op jit(solution)/shard_map/ppermute | solution.py:82
  96.4 18.4 %collective-permute-start.33 = (bf16[256,768]{1,0:T(8,128)(2,1)S(1)}, bf16[256,768]{1,0:T(8,128)(2,1)S(1)}, u32[]{:S(2)}, u32[]{:S(2)}) collective-permute-start(bf16[256,768]{1,0:T(8,128)(2,1)S(1)} %get-tuple-element.51.refs_8_), channel_id=1, source_target_pairs={{0,4},{4,8},{8,12},{12,14},{14,10},{10,6},{6,2},{2,0},{1,5},{5,9},... | collective-permute-start | bytes 1179656 | tf_op jit(solution)/shard_map/ppermute | solution.py:73
  97.1 17.7 %collective-permute-start.34 = (bf16[256,768]{1,0:T(8,128)(2,1)S(1)}, bf16[256,768]{1,0:T(8,128)(2,1)S(1)}, u32[]{:S(2)}, u32[]{:S(2)}) collective-permute-start(bf16[256,768]{1,0:T(8,128)(2,1)S(1)} %get-tuple-element.51.refs_8_), channel_id=1, source_target_pairs={{4,0},{8,4},{12,8},{14,12},{10,14},{6,10},{2,6},{0,2},{5,1},{9,5},... | collective-permute-start | bytes 1179656 | tf_op jit(solution)/shard_map/ppermute | solution.py:75
  98.9 44.0 %collective-permute-start.18 = (bf16[1,256,2048]{2,1,0:T(8,128)(2,1)S(1)}, bf16[1,256,2048]{2,1,0:T(8,128)(2,1)S(1)}, u32[]{:S(2)}, u32[]{:S(2)}) collective-permute-start(bf16[1,256,2048]{2,1,0:T(8,128)(2,1)S(1)} %get-tuple-element.36), channel_id=1, source_target_pairs={{1,0},{0,1},{3,2},{2,3},{5,4},{4,5},{7,6},{6,7},{9,8},{8,9},{11,10... | collective-permute-start | bytes 3145736 | tf_op jit(solution)/shard_map/ppermute | solution.py:82
  106.4 38.0 %collective-permute-start.17 = (bf16[1,256,2048]{2,1,0:T(8,128)(2,1)S(1)}, bf16[1,256,2048]{2,1,0:T(8,128)(2,1)S(1)}, u32[]{:S(2)}, u32[]{:S(2)}) collective-permute-start(bf16[1,256,2048]{2,1,0:T(8,128)(2,1)S(1)} %add_convert_fusion), channel_id=1, source_target_pairs={{16,0},{0,16},{17,1},{1,17},{18,2},{2,18},{19,3},{3,19},{20,4},{4,... | collective-permute-start | bytes 3145736 | tf_op jit(solution)/shard_map/ppermute | solution.py:82
  132.4 18.4 %collective-permute-start.35 = (bf16[256,768]{1,0:T(8,128)(2,1)S(1)}, bf16[256,768]{1,0:T(8,128)(2,1)S(1)}, u32[]{:S(2)}, u32[]{:S(2)}) collective-permute-start(bf16[256,768]{1,0:T(8,128)(2,1)S(1)} %collective-permute-done.33.refs_9_), channel_id=1, source_target_pairs={{0,4},{4,8},{8,12},{12,14},{14,10},{10,6},{6,2},{2,0},{1,5},{5,9},... | collective-permute-start | bytes 1179656 | tf_op jit(solution)/shard_map/ppermute | solution.py:73
  144.4 23.2 %collective-permute-start.49 = (bf16[768,256]{1,0:T(8,128)(2,1)S(1)}, bf16[768,256]{1,0:T(8,128)(2,1)S(1)}, u32[]{:S(2)}, u32[]{:S(2)}) collective-permute-start(bf16[768,256]{1,0:T(8,128)(2,1)S(1)} %collective-permute-done.43.refs_4_), channel_id=1, source_target_pairs={{0,4},{4,8},{8,12},{12,14},{14,10},{10,6},{6,2},{2,0},{1,5},{5,9},... | collective-permute-start | bytes 1179656 | tf_op jit(solution)/shard_map/ppermute | solution.py:73
  147.0 39.5 %collective-permute-start.40 = (bf16[256,2048]{1,0:T(8,128)(2,1)S(1)}, bf16[256,2048]{1,0:T(8,128)(2,1)S(1)}, u32[]{:S(2)}, u32[]{:S(2)}) collective-permute-start(bf16[256,2048]{1,0:T(8,128)(2,1)S(1)} %get-tuple-element.38.refs_16_), channel_id=1, source_target_pairs={{16,0},{0,16},{17,1},{1,17},{18,2},{2,18},{19,3},{3,19},{20,4},{4,... | collective-permute-start | bytes 3145736 | tf_op jit(solution)/shard_map/ppermute | solution.py:82
  150.8 17.4 %collective-permute-start.50 = (bf16[768,256]{1,0:T(8,128)(2,1)S(1)}, bf16[768,256]{1,0:T(8,128)(2,1)S(1)}, u32[]{:S(2)}, u32[]{:S(2)}) collective-permute-start(bf16[768,256]{1,0:T(8,128)(2,1)S(1)} %collective-permute-done.44.refs_5_), channel_id=1, source_target_pairs={{4,0},{8,4},{12,8},{14,12},{10,14},{6,10},{2,6},{0,2},{5,1},{9,5},... | collective-permute-start | bytes 1179656 | tf_op jit(solution)/shard_map/ppermute | solution.py:75
  151.3 16.9 %collective-permute-start.51 = (bf16[768,256]{1,0:T(8,128)(2,1)S(1)}, bf16[768,256]{1,0:T(8,128)(2,1)S(1)}, u32[]{:S(2)}, u32[]{:S(2)}) collective-permute-start(bf16[768,256]{1,0:T(8,128)(2,1)S(1)} %collective-permute-done.45.refs_6_), channel_id=1, source_target_pairs={{4,0},{8,4},{12,8},{14,12},{10,14},{6,10},{2,6},{0,2},{5,1},{9,5},... | collective-permute-start | bytes 1179656 | tf_op jit(solution)/shard_map/ppermute | solution.py:75
  159.2 16.9 %collective-permute-start.30 = (bf16[256,768]{1,0:T(8,128)(2,1)S(1)}, bf16[256,768]{1,0:T(8,128)(2,1)S(1)}, u32[]{:S(2)}, u32[]{:S(2)}) collective-permute-start(bf16[256,768]{1,0:T(8,128)(2,1)S(1)} %collective-permute-done.28.refs_3_), channel_id=1, source_target_pairs={{0,4},{4,8},{8,12},{12,14},{14,10},{10,6},{6,2},{2,0},{1,5},{5,9},... | collective-permute-start | bytes 1179656 | tf_op jit(solution)/shard_map/ppermute | solution.py:73
  168.1 35.4 %collective-permute-start.60 = (bf16[256,2048]{1,0:T(8,128)(2,1)S(1)}, bf16[256,2048]{1,0:T(8,128)(2,1)S(1)}, u32[]{:S(2)}, u32[]{:S(2)}) collective-permute-start(bf16[256,2048]{1,0:T(8,128)(2,1)S(1)} %get-tuple-element.38.refs_16_), channel_id=1, source_target_pairs={{1,0},{0,1},{3,2},{2,3},{5,4},{4,5},{7,6},{6,7},{9,8},{8,9},{11,10... | collective-permute-start | bytes 3145736 | tf_op jit(solution)/shard_map/ppermute | solution.py:82
  186.5 29.9 %collective-permute-start.41 = (bf16[256,2048]{1,0:T(8,128)(2,1)S(1)}, bf16[256,2048]{1,0:T(8,128)(2,1)S(1)}, u32[]{:S(2)}, u32[]{:S(2)}) collective-permute-start(bf16[256,2048]{1,0:T(8,128)(2,1)S(1)} %collective-permute-done.40.refs_16_), channel_id=1, source_target_pairs={{1,0},{0,1},{3,2},{2,3},{5,4},{4,5},{7,6},{6,7},{9,8},{8,9},{11,10... | collective-permute-start | bytes 3145736 | tf_op jit(solution)/shard_map/ppermute | solution.py:82
  201.7 22.8 %collective-permute-start.61 = (bf16[768,256]{1,0:T(8,128)(2,1)S(1)}, bf16[768,256]{1,0:T(8,128)(2,1)S(1)}, u32[]{:S(2)}, u32[]{:S(2)}) collective-permute-start(bf16[768,256]{1,0:T(8,128)(2,1)S(1)} %collective-permute-done.54.refs_1_.refs_11_), channel_id=1, source_target_pairs={{0,4},{4,8},{8,12},{12,14},{14,10},{10,6},{6,2},{2,0},{1,5},{5,9},... | collective-permute-start | bytes 1179656 | tf_op jit(solution)/shard_map/ppermute | solution.py:73
  203.5 21.5 %collective-permute-start.62 = (bf16[768,256]{1,0:T(8,128)(2,1)S(1)}, bf16[768,256]{1,0:T(8,128)(2,1)S(1)}, u32[]{:S(2)}, u32[]{:S(2)}) collective-permute-start(bf16[768,256]{1,0:T(8,128)(2,1)S(1)} %collective-permute-done.57.refs_4_.refs_14_), channel_id=1, source_target_pairs={{4,0},{8,4},{12,8},{14,12},{10,14},{6,10},{2,6},{0,2},{5,1},{9,5},... | collective-permute-start | bytes 1179656 | tf_op jit(solution)/shard_map/ppermute | solution.py:75
  226.1 25.6 %collective-permute-start.53 = (bf16[1,256,512]{2,1,0:T(8,128)(2,1)S(1)}, bf16[1,256,512]{2,1,0:T(8,128)(2,1)S(1)}, u32[]{:S(2)}, u32[]{:S(2)}) collective-permute-start(bf16[1,256,512]{2,1,0:T(8,128)(2,1)S(1)} %add_convert_fusion.3), channel_id=1, source_target_pairs={{16,0},{0,16},{17,1},{1,17},{18,2},{2,18},{19,3},{3,19},{20,4},{4,... | collective-permute-start | bytes 786440 | tf_op jit(solution)/shard_map/ppermute | solution.py:82
  226.8 24.9 %collective-permute-start.47 = (bf16[1,256,768]{2,1,0:T(8,128)(2,1)S(1)}, bf16[1,256,768]{2,1,0:T(8,128)(2,1)S(1)}, u32[]{:S(2)}, u32[]{:S(2)}) collective-permute-start(bf16[1,256,768]{2,1,0:T(8,128)(2,1)S(1)} %add_convert_fusion.1), channel_id=1, source_target_pairs={{16,0},{0,16},{17,1},{1,17},{18,2},{2,18},{19,3},{3,19},{20,4},{4,... | collective-permute-start | bytes 1179656 | tf_op jit(solution)/shard_map/ppermute | solution.py:82
  228.5 23.3 %collective-permute-start.59 = (bf16[1,256,512]{2,1,0:T(8,128)(2,1)S(1)}, bf16[1,256,512]{2,1,0:T(8,128)(2,1)S(1)}, u32[]{:S(2)}, u32[]{:S(2)}) collective-permute-start(bf16[1,256,512]{2,1,0:T(8,128)(2,1)S(1)} %add_convert_fusion.2), channel_id=1, source_target_pairs={{16,0},{0,16},{17,1},{1,17},{18,2},{2,18},{19,3},{3,19},{20,4},{4,... | collective-permute-start | bytes 786440 | tf_op jit(solution)/shard_map/ppermute | solution.py:82
  229.1 22.6 %collective-permute-start.64 = (bf16[1,256,256]{2,1,0:T(8,128)(2,1)S(1)}, bf16[1,256,256]{2,1,0:T(8,128)(2,1)S(1)}, u32[]{:S(2)}, u32[]{:S(2)}) collective-permute-start(bf16[1,256,256]{2,1,0:T(8,128)(2,1)S(1)} %add_convert_fusion.4), channel_id=1, source_target_pairs={{16,0},{0,16},{17,1},{1,17},{18,2},{2,18},{19,3},{3,19},{20,4},{4,... | collective-permute-start | bytes 393224 | tf_op jit(solution)/shard_map/ppermute | solution.py:82
  (51 other events, 665.7 us)

commit v2 on v1

--- a/solution.py
+++ b/solution.py
@@ -89,7 +89,8 @@
     return got
 
 
-def prepare_kernel(rep, x, gate, out, pre, scale, first, second, x_own, gate_own, out_own, sems):
+def prepare_kernel(rep, x, gate, out, pre_all, scale_all, first, second, *scratch):
+    x_own, gate_own, out_own, pre, scale, sems = scratch
     rows, cols = x_own.shape
     half = cols // 2
     wide = pl.ds(pl.multiple_of(rep[0] * cols, cols), cols)
@@ -97,15 +98,19 @@
         pltpu.make_async_copy(x.at[:, wide], x_own, sems.at[0]),
         pltpu.make_async_copy(gate.at[:, wide], gate_own, sems.at[1]),
         pltpu.make_async_copy(out.at[wide, :], out_own, sems.at[2]),
+        pltpu.make_async_copy(pre_all, pre, sems.at[3]),
+        pltpu.make_async_copy(scale_all, scale, sems.at[4]),
     ]
     for copy in copies:
         copy.start()
+    copies[3].wait()
     gains = jnp.transpose(jnp.broadcast_to(pre[...], (LANES, rows)))
     for copy, own, to in ((copies[0], x_own, first), (copies[1], gate_own, second)):
         copy.wait()
         for at in range(0, cols, LANES):
             to[:, at : at + LANES] = (own[:, at : at + LANES] * gains).astype(BF16)
     copies[2].wait()
+    copies[4].wait()
     first[:, cols:] = (out_own[:half, :] * scale[...]).astype(BF16)
     second[:, cols:] = (out_own[half:, :] * scale[...]).astype(BF16)
 
@@ -120,13 +125,15 @@
         grid_spec=pltpu.PrefetchScalarGridSpec(
             num_scalar_prefetch=1,
             grid=(),
-            in_specs=[hbm] * 3 + [vmem] * 2,
+            in_specs=[hbm] * 5,
             out_specs=[vmem] * 2,
             scratch_shapes=[
                 pltpu.VMEM((rows, cols), F32),
                 pltpu.VMEM((rows, cols), F32),
                 pltpu.VMEM((cols, out.shape[1]), F32),
-                pltpu.SemaphoreType.DMA((3,)),
+                pltpu.VMEM(pre.shape, F32),
+                pltpu.VMEM(scale.shape, F32),
+                pltpu.SemaphoreType.DMA((5,)),
             ],
         ),
         out_shape=[jax.ShapeDtypeStruct(shape, BF16)] * 2,
@@ -436,56 +443,98 @@
     )(*acts, *flat)
 
 
-def last_kernel(streams, count, scalars, hidden, *refs):
-    pieces = refs[-3 - count : -3]
-    out, total, gains = refs[-3:]
-    place_gains(scalars[count], pieces, gains)
-    cols = hidden.shape[1] // count
+def sum_kernel(streams, count, order, *refs):
+    total, squares = refs[-2:]
     where = []
     first = 0
     for groups in streams:
         where.append([(first + g, s) for g, steps in enumerate(groups) for s in range(steps)])
         first += len(groups)
-    for step in range(count):
+    cols = total.shape[1] // count
+    power = jnp.zeros(squares.shape, F32)
+    for step in range(count - 1):
         value = None
         for places in where:
             g, s = places[step]
             part = refs[g][0, :, s * cols : (s + 1) * cols].astype(F32)
             value = part if value is None else value + part
-        to = pl.multiple_of(scalars[step] * cols, cols)
+        to = pl.multiple_of(order[step] * cols, cols)
         total[:, pl.ds(to, cols)] = value
-    v = total[...]
-    out[...] = (
-        hidden[...].astype(F32)
-        + v * lax.rsqrt(jnp.mean(v * v, axis=-1, keepdims=True) + EPSILON) * gains[1:2, :]
-    ).astype(BF16)
-
-
-def last(scalars, hidden, streams, parts, gains):
-    rows, width = hidden.shape
+        power = power + sum(
+            value[:, at : at + LANES] * value[:, at : at + LANES] for at in range(0, cols, LANES)
+        )
+    to = pl.multiple_of(order[count - 1] * cols, cols)
+    total[:, pl.ds(to, cols)] = jnp.zeros((total.shape[0], cols), F32)
+    squares[...] = power
+
+
+def sum_blocks(order, streams, parts, rows, width):
     tile = rows // 2
     flat = [p for stream in parts for p in stream]
-    row = pl.BlockSpec((tile, width), lambda i, *_: (i, 0))
-    part = lambda p: pl.BlockSpec((1, tile, p.shape[2]), lambda i, *_: (p.shape[0] - 1, i, 0))
-    return pl.pallas_call(
-        functools.partial(last_kernel, streams, len(gains)),
+    row = lambda n: pl.BlockSpec((tile, n), lambda i, *_: (i, 0))
+    return pl.pallas_call(
+        functools.partial(sum_kernel, streams, order.shape[0]),
         grid_spec=pltpu.PrefetchScalarGridSpec(
             num_scalar_prefetch=1,
             grid=(rows // tile,),
-            in_specs=[row] + [part(p) for p in flat] + [whole_spec(g.shape) for g in gains],
-            out_specs=row,
-            scratch_shapes=[pltpu.VMEM((tile, width), F32), pltpu.VMEM((2, width), F32)],
+            in_specs=[
+                pl.BlockSpec((1, tile, p.shape[2]), lambda i, *_: (0, i, 0)) for p in flat
+            ],
+            out_specs=[row(width), row(LANES)],
+        ),
+        out_shape=[
+            jax.ShapeDtypeStruct((rows, width), F32),
+            jax.ShapeDtypeStruct((rows, LANES), F32),
+        ],
+        compiler_params=params(),
+        cost_estimate=cost(1e9, 2 * rows * width * (2 + len(streams))),
+        name="sum_blocks",
+    )(order, *flat)
+
+
+def last_kernel(count, scalars, hidden, total, squares, *refs):
+    ends, pieces = refs[: -2 - count], refs[-2 - count : -2]
+    out, gains = refs[-2:]
+    place_gains(scalars[count], pieces, gains)
+    width = hidden.shape[1]
+    cols = width // count
+    end = ends[0][0].astype(F32)
+    for ref in ends[1:]:
+        end = end + ref[0].astype(F32)
+    power = jnp.sum(squares[...], axis=-1, keepdims=True)
+    power = power + jnp.sum(end * end, axis=-1, keepdims=True)
+    scale = lax.rsqrt(power * (1.0 / width) + EPSILON)
+    out[...] = (hidden[...].astype(F32) + total[...] * scale * gains[1:2, :]).astype(BF16)
+    at = pl.ds(pl.multiple_of(scalars[count - 1] * cols, cols), cols)
+    out[:, at] = (hidden[:, at].astype(F32) + end * scale * gains[1:2, at]).astype(BF16)
+
+
+def last(scalars, hidden, total, squares, ends, gains):
+    rows, width = hidden.shape
+    tile = rows // 2
+    row = lambda n: pl.BlockSpec((tile, n), lambda i, *_: (i, 0))
+    part = lambda p: pl.BlockSpec((1, tile, p.shape[2]), lambda i, *_: (p.shape[0] - 1, i, 0))
+    return pl.pallas_call(
+        functools.partial(last_kernel, len(gains)),
+        grid_spec=pltpu.PrefetchScalarGridSpec(
+            num_scalar_prefetch=1,
+            grid=(rows // tile,),
+            in_specs=[row(width), row(width), row(LANES)]
+            + [part(p) for p in ends]
+            + [whole_spec(g.shape) for g in gains],
+            out_specs=row(width),
+            scratch_shapes=[pltpu.VMEM((2, width), F32)],
         ),
         out_shape=jax.ShapeDtypeStruct((rows, width), BF16),
         compiler_params=params(),
-        cost_estimate=cost(1e9, 2 * rows * width * (2 + len(streams))),
+        cost_estimate=cost(1e9, 8 * rows * width),
         name="last",
-    )(scalars, hidden, *flat, *gains)
+    )(scalars, hidden, total, squares, *ends, *gains)
 
 
 def group_sizes(count):
     far = (3,) + (2,) * (count // 2 - 2) + (1,) if count > 2 else (1, 1)
-    return far, (count - 1, 1)
+    return far, (count - 3, 2, 1)
 
 
 def ring_device(
@@ -595,21 +644,20 @@
             at += steps
             summands = over_tp(parts)
             rows_of[dr].append([over_rep(summands, dr)] if dr else summands)
-    parts = down_project(tps, [acts[dr] for dr in far_first], downs[-1:])
-    summands = over_tp(parts)
-    for i, dr in enumerate(far_first):
-        if dr:
-            own = [x[i : i + 1] for x in summands]
-            rows_of[dr].append([over_rep(own, dr)])
-        else:
-            rows_of[dr].append(summands)
     streams, arrays = [], []
     for dr in far_first:
         for i in range(len(rows_of[dr][0])):
-            streams.append(group_sizes(count)[0 if dr else 1])
+            streams.append(group_sizes(count)[0 if dr else 1][:-1])
             arrays.append([group[i] for group in rows_of[dr]])
+    total, squares = sum_blocks(order, tuple(streams), arrays, share, width)
+    parts = down_project(tps, [acts[dr] for dr in far_first], downs[-1:])
+    summands = over_tp(parts)
+    ends = list(summands)
+    for i, dr in enumerate(far_first):
+        if dr:
+            ends.append(over_rep([x[i : i + 1] for x in summands], dr))
     scalars = jnp.concatenate([order, me_scalar])
-    return last(scalars, hidden, tuple(streams), arrays, gains)[None]
+    return last(scalars, hidden, total, squares, ends, gains)[None]
 
 
 def link_states(earlier, later):
@@ -733,6 +781,7 @@
         chan, hid = x_weight.shape[1] // reps, up_weight.shape[1] // reps
         fits = (
             count % 2 == 0
+            and count >= 4
             and rows % (2 * LANES) == 0
             and chan % (2 * LANES) == 0
             and chan == 2 * rows

time: 255 us -> 254 us (level)
  waiting for transfers between devices: 139 us -> 132 us
  starting transfers between devices: 66.2 us -> 72.3 us
    ppermute x21, waiting for transfers between devices: 93.8 us -> 68.5 us  [ring_gather(): ahead[h] = lax.ppermute(ahead[h], 'fs', fwd)]
    ppermute x21, waiting for transfers between devices: 23.5 us -> 42.6 us  [ring_gather(): behind[h] = lax.ppermute(behind[h], 'fs', bwd)]
    ppermute x21, starting transfers between devices: 15.5 us -> 24.2 us  [ring_gather(): behind[h] = lax.ppermute(behind[h], 'fs', bwd)]
    ppermute x24 -> x25, starting transfers between devices: 26.2 us -> 25.2 us  [shift(): lax.ppermute(value, axis, [((i + by) % count, i) for i in range(count)])]
    pallas_call x5 -> x6, Pallas kernels: 7.32 us -> 7.48 us  [down_project(): pl.pallas_call(functools.partial(down_kernel, len(held), len(acts)), in_s...]
    ppermute x24 -> x25, waiting for transfers between devices: 21.4 us -> 21.4 us  [shift(): lax.ppermute(value, axis, [((i + by) % count, i) for i in range(count)])]
  transfers between devices with their start and end apart: 66 -> 67, of which waited for: 28 -> 32; matrix products, arithmetic and copies ran while one was open for 2% -> 2% of each run, Pallas kernels for 15% -> 15%
where the time goes in v2:
time: 254 us
  waiting for transfers between devices  132 us (52%)
  starting transfers between devices  72.3 us (28%)
  Pallas kernels  40.7 us (16%)
  other arithmetic  4.39 us (2%)
  local copies, waits for them, and re-layouts  3.76 us (1%)
    ppermute x21, waiting for transfers between devices, ring_gather(): ahead[h] = lax.ppermute(ahead[h], 'fs', fwd)  68.5 us
    ppermute x21, waiting for transfers between devices, ring_gather(): behind[h] = lax.ppermute(behind[h], 'fs', bwd)  42.6 us
    ppermute x25, starting transfers between devices, shift(): lax.ppermute(value, axis, [((i + by) % count, i) for i in range(count)])  25.2 us
    ppermute x21, starting transfers between devices, ring_gather(): behind[h] = lax.ppermute(behind[h], 'fs', bwd)  24.2 us
    ppermute x21, starting transfers between devices, ring_gather(): ahead[h] = lax.ppermute(ahead[h], 'fs', fwd)  22.9 us
    ppermute x25, waiting for transfers between devices, shift(): lax.ppermute(value, axis, [((i + by) % count, i) for i in range(count)])  21.4 us
    pallas_call x2, Pallas kernels, up_project(): pl.pallas_call(functools.partial(up_kernel, steps, len(xs)), grid_spec=pl...  7.96 us
    pallas_call x6, Pallas kernels, down_project(): pl.pallas_call(functools.partial(down_kernel, len(held), len(acts)), in_s...  7.48 us
  transfers between devices with their start and end apart: 67, of which 32 were waited for; matrix products, arithmetic and copies ran while one was open for 2% of the time, Pallas kernels for 15%

profile of v2, /device:TPU:0, one launch (start us, length us, event | category | flops | bytes accessed | tf_op | source)
XLA Modules:
  0.0 254.2 jit_solution(2928600404428671195)
XLA Ops:
  2.4 3.0 %collective-permute-start = (bf16[256,2048]{1,0:T(8,128)(2,1)}, bf16[256,2048]{1,0:T(8,128)(2,1)S(1)}, u32[]{:S(2)}, u32[]{:S(2)}) collective-permute-start(bf16[256,2048]{1,0:T(8,128)(2,1)} %dynamic-slice_bitcast_fusion.tokens), channel_id=1, source_target_pairs={{16,0},{0,16},{17,1},{1,17},{18,2},{2,18},{19,3},{3,19},{20,4},{4,... | collective-permute-start | bytes 3145736 | tf_op jit(solution)/shard_map/ppermute | solution.py:82
  13.3 6.7 %collective-permute-done.10.refs_10_ = bf16[256,768]{1,0:T(8,128)(2,1)S(1)} collective-permute-done((bf16[256,768]{1,0:T(8,128)(2,1)}, bf16[256,768]{1,0:T(8,128)(2,1)S(1)}, u32[]{:S(2)}, u32[]{:S(2)}) %collective-permute-start.10) | collective-permute-done | bytes 393248 | tf_op jit(solution)/shard_map/ppermute | solution.py:75
  21.5 6.7 %collective-permute-done.2.refs_1_ = bf16[256,768]{1,0:T(8,128)(2,1)S(1)} collective-permute-done((bf16[256,768]{1,0:T(8,128)(2,1)}, bf16[256,768]{1,0:T(8,128)(2,1)S(1)}, u32[]{:S(2)}, u32[]{:S(2)}) %collective-permute-start.2) | collective-permute-done | bytes 393248 | tf_op jit(solution)/shard_map/ppermute | solution.py:73
  32.8 3.0 %collective-permute-done.12.refs_12_ = bf16[256,768]{1,0:T(8,128)(2,1)S(1)} collective-permute-done((bf16[256,768]{1,0:T(8,128)(2,1)S(1)}, bf16[256,768]{1,0:T(8,128)(2,1)S(1)}, u32[]{:S(2)}, u32[]{:S(2)}) %collective-permute-start.12) | collective-permute-done | bytes 393248 | tf_op jit(solution)/shard_map/ppermute | solution.py:75
  35.9 2.5 collective-permute-start.14
  42.3 6.4 %collective-permute-done.11.refs_11_ = bf16[256,768]{1,0:T(8,128)(2,1)S(1)} collective-permute-done((bf16[256,768]{1,0:T(8,128)(2,1)S(1)}, bf16[256,768]{1,0:T(8,128)(2,1)S(1)}, u32[]{:S(2)}, u32[]{:S(2)}) %collective-permute-start.11) | collective-permute-done | bytes 393248 | tf_op jit(solution)/shard_map/ppermute | solution.py:73
  52.8 2.4 collective-permute-start.15
  58.4 4.6 %collective-permute-start.19 = (f32[2,256]{1,0:T(2,128)S(1)}, f32[2,256]{1,0:T(2,128)S(1)}, u32[]{:S(2)}, u32[]{:S(2)}) collective-permute-start(f32[2,256]{1,0:T(2,128)S(1)} %pad_maximum_fusion.2.refs_3_), channel_id=1, source_target_pairs={{2,0},{4,2},{6,4},{8,6},{10,8},{12,10},{14,12},{0,14},{3,1},{5,3},... | collective-permute-start | bytes 6152 | tf_op jit(solution)/shard_map/ppermute | solution.py:82
  65.5 2.5 collective-permute-start.20
  69.6 2.4 collective-permute-start.22
  72.0 2.9 %project.2 = (bf16[512,512]{1,0:T(8,128)(2,1)S(1)}, bf16[512,512]{1,0:T(8,128)(2,1)S(1)}) custom-call(s32[8]{0:T(128)S(1)} %fusion.1.order, bf16[512,2048]{1,0:T(8,128)(2,1)S(1)} %normalize.2.normed, f32[1,1024]{1,0:T(1,128)S(1)} %bitcast.32, bf16[256,768]{1,0:T(8,128)(2,1)S(1)} %copy-done.2, bf16[256,768]{1,0:T(8,128)(2,1)S(1)} %collective-permute-done.2.refs_1_, ...), custom_call_target="tpu_custom_call" | custom-call | flops 2147483648 | bytes 6291456 | tf_op jit(solution)/shard_map/project/pallas_call | solution.py:198
  74.9 3.3 %recur.2.mixed = bf16[1,512,512]{2,1,0:T(8,128)(2,1)S(1)} custom-call(bf16[1,512,512]{2,1,0:T(8,128)(2,1)S(1)} %bitcast.38, bf16[1,512,512]{2,1,0:T(8,128)(2,1)S(1)} %bitcast.39, f32[4,512]{1,0:T(4,128)S(1)} %constant_dynamic-slice_fusion.conv_ref, bf16[4,128,256]{2,1,0:T(8,128)(2,1)S(1)} %pad_maximum_fusion.maps_ref, f32[1,512]{1,0:T(1,128)S(1)} %bitcast.34), custom_call_target="tpu_custom_call" | custom-call | flops 3000000000 | bytes 1572864 | tf_op jit(solution)/shard_map/recur/pallas_call | solution.py:267
  80.4 2.9 %project.3 = (bf16[512,512]{1,0:T(8,128)(2,1)S(1)}, bf16[512,512]{1,0:T(8,128)(2,1)S(1)}) custom-call(s32[8]{0:T(128)S(1)} %fusion.1.order, bf16[512,2048]{1,0:T(8,128)(2,1)S(1)} %normalize.3.normed, f32[1,1024]{1,0:T(1,128)S(1)} %bitcast.33, bf16[256,768]{1,0:T(8,128)(2,1)S(1)} %copy-done.2, bf16[256,768]{1,0:T(8,128)(2,1)S(1)} %collective-permute-done.2.refs_1_, ...), custom_call_target="tpu_custom_call" | custom-call | flops 2147483648 | bytes 6291456 | tf_op jit(solution)/shard_map/project/pallas_call | solution.py:198
  83.3 3.3 %recur.3.mixed = bf16[1,512,512]{2,1,0:T(8,128)(2,1)S(1)} custom-call(bf16[1,512,512]{2,1,0:T(8,128)(2,1)S(1)} %bitcast.36, bf16[1,512,512]{2,1,0:T(8,128)(2,1)S(1)} %bitcast.37, f32[4,512]{1,0:T(4,128)S(1)} %constant_dynamic-slice_fusion.conv_ref, bf16[4,128,256]{2,1,0:T(8,128)(2,1)S(1)} %pad_maximum_fusion.maps_ref, f32[1,512]{1,0:T(1,128)S(1)} %bitcast.35), custom_call_target="tpu_custom_call" | custom-call | flops 3000000000 | bytes 1572864 | tf_op jit(solution)/shard_map/recur/pallas_call | solution.py:267
  98.6 6.2 %collective-permute-done.26.refs_1_ = bf16[256,768]{1,0:T(8,128)(2,1)S(1)} collective-permute-done((bf16[256,768]{1,0:T(8,128)(2,1)S(1)}, bf16[256,768]{1,0:T(8,128)(2,1)S(1)}, u32[]{:S(2)}, u32[]{:S(2)}) %collective-permute-start.26) | collective-permute-done | bytes 393248 | tf_op jit(solution)/shard_map/ppermute | solution.py:73
  105.3 7.1 %collective-permute-done.34.refs_10_ = bf16[256,768]{1,0:T(8,128)(2,1)S(1)} collective-permute-done((bf16[256,768]{1,0:T(8,128)(2,1)S(1)}, bf16[256,768]{1,0:T(8,128)(2,1)S(1)}, u32[]{:S(2)}, u32[]{:S(2)}) %collective-permute-start.34) | collective-permute-done | bytes 393248 | tf_op jit(solution)/shard_map/ppermute | solution.py:75
  115.8 8.6 %collective-permute-done.42.refs_3_ = bf16[768,256]{1,0:T(8,128)(2,1)S(1)} collective-permute-done((bf16[768,256]{1,0:T(8,128)(2,1)S(1)}, bf16[768,256]{1,0:T(8,128)(2,1)S(1)}, u32[]{:S(2)}, u32[]{:S(2)}) %collective-permute-start.42) | collective-permute-done | bytes 393248 | tf_op jit(solution)/shard_map/ppermute | solution.py:73
  126.5 6.4 %collective-permute-done.43.refs_4_ = bf16[768,256]{1,0:T(8,128)(2,1)S(1)} collective-permute-done((bf16[768,256]{1,0:T(8,128)(2,1)S(1)}, bf16[768,256]{1,0:T(8,128)(2,1)S(1)}, u32[]{:S(2)}, u32[]{:S(2)}) %collective-permute-start.43) | collective-permute-done | bytes 393248 | tf_op jit(solution)/shard_map/ppermute | solution.py:73
  135.5 3.4 %collective-permute-done.28.refs_3_ = bf16[256,768]{1,0:T(8,128)(2,1)S(1)} collective-permute-done((bf16[256,768]{1,0:T(8,128)(2,1)S(1)}, bf16[256,768]{1,0:T(8,128)(2,1)S(1)}, u32[]{:S(2)}, u32[]{:S(2)}) %collective-permute-start.28) | collective-permute-done | bytes 393248 | tf_op jit(solution)/shard_map/ppermute | solution.py:73
  145.3 7.9 %collective-permute-done.29.refs_4_ = bf16[256,768]{1,0:T(8,128)(2,1)S(1)} collective-permute-done((bf16[256,768]{1,0:T(8,128)(2,1)S(1)}, bf16[256,768]{1,0:T(8,128)(2,1)S(1)}, u32[]{:S(2)}, u32[]{:S(2)}) %collective-permute-start.29) | collective-permute-done | bytes 393248 | tf_op jit(solution)/shard_map/ppermute | solution.py:75
  155.3 3.9 %collective-permute-done.48.refs_1_.refs_7_ = bf16[768,256]{1,0:T(8,128)(2,1)S(1)} collective-permute-done((bf16[768,256]{1,0:T(8,128)(2,1)S(1)}, bf16[768,256]{1,0:T(8,128)(2,1)S(1)}, u32[]{:S(2)}, u32[]{:S(2)}) %collective-permute-start.48) | collective-permute-done | bytes 393248 | tf_op jit(solution)/shard_map/ppermute | solution.py:73
  162.8 4.9 %collective-permute-done.49.refs_2_.refs_8_ = bf16[768,256]{1,0:T(8,128)(2,1)S(1)} collective-permute-done((bf16[768,256]{1,0:T(8,128)(2,1)S(1)}, bf16[768,256]{1,0:T(8,128)(2,1)S(1)}, u32[]{:S(2)}, u32[]{:S(2)}) %collective-permute-start.49) | collective-permute-done | bytes 393248 | tf_op jit(solution)/shard_map/ppermute | solution.py:73
  167.7 2.4 collective-permute-done.50.refs_3_.refs_9_
  174.5 3.4 %collective-permute-done.38.refs_14_ = bf16[256,768]{1,0:T(8,128)(2,1)S(1)} collective-permute-done((bf16[256,768]{1,0:T(8,128)(2,1)S(1)}, bf16[256,768]{1,0:T(8,128)(2,1)S(1)}, u32[]{:S(2)}, u32[]{:S(2)}) %collective-permute-start.38) | collective-permute-done | bytes 393248 | tf_op jit(solution)/shard_map/ppermute | solution.py:75
  179.1 4.5 %collective-permute-done.31.refs_6_ = bf16[256,768]{1,0:T(8,128)(2,1)S(1)} collective-permute-done((bf16[256,768]{1,0:T(8,128)(2,1)S(1)}, bf16[256,768]{1,0:T(8,128)(2,1)S(1)}, u32[]{:S(2)}, u32[]{:S(2)}) %collective-permute-start.31) | collective-permute-done | bytes 393248 | tf_op jit(solution)/shard_map/ppermute | solution.py:75
  186.5 7.3 %collective-permute-done.54.refs_1_ = bf16[768,256]{1,0:T(8,128)(2,1)S(1)} collective-permute-done((bf16[768,256]{1,0:T(8,128)(2,1)S(1)}, bf16[768,256]{1,0:T(8,128)(2,1)S(1)}, u32[]{:S(2)}, u32[]{:S(2)}) %collective-permute-start.54) | collective-permute-done | bytes 393248 | tf_op jit(solution)/shard_map/ppermute | solution.py:73
  195.8 6.4 %collective-permute-done.32.refs_7_ = bf16[256,768]{1,0:T(8,128)(2,1)S(1)} collective-permute-done((bf16[256,768]{1,0:T(8,128)(2,1)S(1)}, bf16[256,768]{1,0:T(8,128)(2,1)S(1)}, u32[]{:S(2)}, u32[]{:S(2)}) %collective-permute-start.32) | collective-permute-done | bytes 393248 | tf_op jit(solution)/shard_map/ppermute | solution.py:73
  203.4 2.4 collective-permute-done.39.refs_15_
  207.8 4.0 %up_project.3.refs_0_.refs_1_ = bf16[512,1536]{1,0:T(8,128)(2,1)S(1)} custom-call(s32[8]{0:T(128)S(1)} %fusion.1.order, f32[1,1536]{1,0:T(1,128)S(1)} %broadcast_in_dim.39.scale, bf16[256,768]{1,0:T(8,128)(2,1)S(1)} %get-tuple-element.60.refs_0_, bf16[256,768]{1,0:T(8,128)(2,1)S(1)} %collective-permute-done.26.refs_1_, ...), custom_call_target="tpu_custom_call" | custom-call | flops 3221225472 | bytes 9961472 | tf_op jit(solution)/shard_map/up_project/pallas_call | solution.py:392
  217.3 4.0 %up_project.2.refs_0_ = bf16[512,1536]{1,0:T(8,128)(2,1)S(1)} custom-call(s32[8]{0:T(128)S(1)} %fusion.1.order, f32[1,1536]{1,0:T(1,128)S(1)} %broadcast_in_dim.39.scale, bf16[256,768]{1,0:T(8,128)(2,1)S(1)} %get-tuple-element.60.refs_0_, bf16[256,768]{1,0:T(8,128)(2,1)S(1)} %collective-permute-done.26.refs_1_, ...), custom_call_target="tpu_custom_call" | custom-call | flops 3221225472 | bytes 9961472 | tf_op jit(solution)/shard_map/up_project/pallas_call | solution.py:392
  231.6 4.7 %collective-permute-done.59.refs_2_ = bf16[1,256,512]{2,1,0:T(8,128)(2,1)S(1)} collective-permute-done((bf16[1,256,512]{2,1,0:T(8,128)(2,1)S(1)}, bf16[1,256,512]{2,1,0:T(8,128)(2,1)S(1)}, u32[]{:S(2)}, u32[]{:S(2)}) %collective-permute-start.59) | collective-permute-done | bytes 262176 | tf_op jit(solution)/shard_map/ppermute | solution.py:82
  236.3 14.0 %collective-permute-done.53.refs_1_ = bf16[1,256,512]{2,1,0:T(8,128)(2,1)S(1)} collective-permute-done((bf16[1,256,512]{2,1,0:T(8,128)(2,1)S(1)}, bf16[1,256,512]{2,1,0:T(8,128)(2,1)S(1)}, u32[]{:S(2)}, u32[]{:S(2)}) %collective-permute-start.53) | collective-permute-done | bytes 262176 | tf_op jit(solution)/shard_map/ppermute | solution.py:82
  (185 shorter events, 99.4 us)
Async XLA Ops:
  2.4 27.1 %collective-permute-start = (bf16[256,2048]{1,0:T(8,128)(2,1)}, bf16[256,2048]{1,0:T(8,128)(2,1)S(1)}, u32[]{:S(2)}, u32[]{:S(2)}) collective-permute-start(bf16[256,2048]{1,0:T(8,128)(2,1)} %dynamic-slice_bitcast_fusion.tokens), channel_id=1, source_target_pairs={{16,0},{0,16},{17,1},{1,17},{18,2},{2,18},{19,3},{3,19},{20,4},{4,... | collective-permute-start | bytes 3145736 | tf_op jit(solution)/shard_map/ppermute | solution.py:82
  9.3 21.4 %collective-permute-start.9 = (bf16[256,768]{1,0:T(8,128)(2,1)}, bf16[256,768]{1,0:T(8,128)(2,1)S(1)}, u32[]{:S(2)}, u32[]{:S(2)}) collective-permute-start(bf16[256,768]{1,0:T(8,128)(2,1)} %get-tuple-element.32.refs_8_), channel_id=1, source_target_pairs={{0,4},{4,8},{8,12},{12,14},{14,10},{10,6},{6,2},{2,0},{1,5},{5,9},... | collective-permute-start | bytes 1179656 | tf_op jit(solution)/shard_map/ppermute | solution.py:73
  9.8 18.4 %collective-permute-start.2 = (bf16[256,768]{1,0:T(8,128)(2,1)}, bf16[256,768]{1,0:T(8,128)(2,1)S(1)}, u32[]{:S(2)}, u32[]{:S(2)}) collective-permute-start(bf16[256,768]{1,0:T(8,128)(2,1)} %get-tuple-element.31.refs_0_), channel_id=1, source_target_pairs={{0,4},{4,8},{8,12},{12,14},{14,10},{10,6},{6,2},{2,0},{1,5},{5,9},... | collective-permute-start | bytes 1179656 | tf_op jit(solution)/shard_map/ppermute | solution.py:73
  11.4 21.0 %collective-permute-start.3 = (bf16[256,768]{1,0:T(8,128)(2,1)}, bf16[256,768]{1,0:T(8,128)(2,1)S(1)}, u32[]{:S(2)}, u32[]{:S(2)}) collective-permute-start(bf16[256,768]{1,0:T(8,128)(2,1)} %get-tuple-element.31.refs_0_), channel_id=1, source_target_pairs={{4,0},{8,4},{12,8},{14,12},{10,14},{6,10},{2,6},{0,2},{5,1},{9,5},... | collective-permute-start | bytes 1179656 | tf_op jit(solution)/shard_map/ppermute | solution.py:75
  29.5 28.9 %collective-permute-start.1 = (bf16[256,2048]{1,0:T(8,128)(2,1)S(1)}, bf16[256,2048]{1,0:T(8,128)(2,1)S(1)}, u32[]{:S(2)}, u32[]{:S(2)}) collective-permute-start(bf16[256,2048]{1,0:T(8,128)(2,1)S(1)} %collective-permute-done.refs_0_), channel_id=1, source_target_pairs={{1,0},{0,1},{3,2},{2,3},{5,4},{4,5},{7,6},{6,7},{9,8},{8,9},{11,10... | collective-permute-start | bytes 3145736 | tf_op jit(solution)/shard_map/ppermute | solution.py:82
  30.7 17.9 %collective-permute-start.11 = (bf16[256,768]{1,0:T(8,128)(2,1)S(1)}, bf16[256,768]{1,0:T(8,128)(2,1)S(1)}, u32[]{:S(2)}, u32[]{:S(2)}) collective-permute-start(bf16[256,768]{1,0:T(8,128)(2,1)S(1)} %collective-permute-done.9.refs_9_), channel_id=1, source_target_pairs={{0,4},{4,8},{8,12},{12,14},{14,10},{10,6},{6,2},{2,0},{1,5},{5,9},... | collective-permute-start | bytes 1179656 | tf_op jit(solution)/shard_map/ppermute | solution.py:73
  35.9 16.9 %collective-permute-start.14 = (bf16[256,768]{1,0:T(8,128)(2,1)S(1)}, bf16[256,768]{1,0:T(8,128)(2,1)S(1)}, u32[]{:S(2)}, u32[]{:S(2)}) collective-permute-start(bf16[256,768]{1,0:T(8,128)(2,1)S(1)} %collective-permute-done.12.refs_12_), channel_id=1, source_target_pairs={{4,0},{8,4},{12,8},{14,12},{10,14},{6,10},{2,6},{0,2},{5,1},{9,5},... | collective-permute-start | bytes 1179656 | tf_op jit(solution)/shard_map/ppermute | solution.py:75
  40.2 16.9 %collective-permute-start.6 = (bf16[256,768]{1,0:T(8,128)(2,1)S(1)}, bf16[256,768]{1,0:T(8,128)(2,1)S(1)}, u32[]{:S(2)}, u32[]{:S(2)}) collective-permute-start(bf16[256,768]{1,0:T(8,128)(2,1)S(1)} %collective-permute-done.4.refs_3_), channel_id=1, source_target_pairs={{0,4},{4,8},{8,12},{12,14},{14,10},{10,6},{6,2},{2,0},{1,5},{5,9},... | collective-permute-start | bytes 1179656 | tf_op jit(solution)/shard_map/ppermute | solution.py:73
  48.7 16.9 %collective-permute-start.13 = (bf16[256,768]{1,0:T(8,128)(2,1)S(1)}, bf16[256,768]{1,0:T(8,128)(2,1)S(1)}, u32[]{:S(2)}, u32[]{:S(2)}) collective-permute-start(bf16[256,768]{1,0:T(8,128)(2,1)S(1)} %collective-permute-done.11.refs_11_), channel_id=1, source_target_pairs={{0,4},{4,8},{8,12},{12,14},{14,10},{10,6},{6,2},{2,0},{1,5},{5,9},... | collective-permute-start | bytes 1179656 | tf_op jit(solution)/shard_map/ppermute | solution.py:73
  49.2 18.9 %collective-permute-start.7 = (bf16[256,768]{1,0:T(8,128)(2,1)S(1)}, bf16[256,768]{1,0:T(8,128)(2,1)S(1)}, u32[]{:S(2)}, u32[]{:S(2)}) collective-permute-start(bf16[256,768]{1,0:T(8,128)(2,1)S(1)} %collective-permute-done.5.refs_4_), channel_id=1, source_target_pairs={{4,0},{8,4},{12,8},{14,12},{10,14},{6,10},{2,6},{0,2},{5,1},{9,5},... | collective-permute-start | bytes 1179656 | tf_op jit(solution)/shard_map/ppermute | solution.py:75
  58.4 28.3 %collective-permute-start.19 = (f32[2,256]{1,0:T(2,128)S(1)}, f32[2,256]{1,0:T(2,128)S(1)}, u32[]{:S(2)}, u32[]{:S(2)}) collective-permute-start(f32[2,256]{1,0:T(2,128)S(1)} %pad_maximum_fusion.2.refs_3_), channel_id=1, source_target_pairs={{2,0},{4,2},{6,4},{8,6},{10,8},{12,10},{14,12},{0,14},{3,1},{5,3},... | collective-permute-start | bytes 6152 | tf_op jit(solution)/shard_map/ppermute | solution.py:82
  65.5 25.4 %collective-permute-start.20 = (f32[2,256]{1,0:T(2,128)S(1)}, f32[2,256]{1,0:T(2,128)S(1)}, u32[]{:S(2)}, u32[]{:S(2)}) collective-permute-start(f32[2,256]{1,0:T(2,128)S(1)} %pad_maximum_fusion.2.refs_3_), channel_id=1, source_target_pairs={{4,0},{6,2},{8,4},{10,6},{12,8},{14,10},{0,12},{2,14},{5,1},{7,3},... | collective-permute-start | bytes 6152 | tf_op jit(solution)/shard_map/ppermute | solution.py:82
  68.0 24.2 %collective-permute-start.21 = (f32[2,256]{1,0:T(2,128)S(1)}, f32[2,256]{1,0:T(2,128)S(1)}, u32[]{:S(2)}, u32[]{:S(2)}) collective-permute-start(f32[2,256]{1,0:T(2,128)S(1)} %pad_maximum_fusion.2.refs_3_), channel_id=1, source_target_pairs={{6,0},{8,2},{10,4},{12,6},{14,8},{0,10},{2,12},{4,14},{7,1},{9,3},... | collective-permute-start | bytes 6152 | tf_op jit(solution)/shard_map/ppermute | solution.py:82
  69.6 23.1 %collective-permute-start.22 = (f32[2,256]{1,0:T(2,128)S(1)}, f32[2,256]{1,0:T(2,128)S(1)}, u32[]{:S(2)}, u32[]{:S(2)}) collective-permute-start(f32[2,256]{1,0:T(2,128)S(1)} %pad_maximum_fusion.2.refs_3_), channel_id=1, source_target_pairs={{8,0},{10,2},{12,4},{14,6},{0,8},{2,10},{4,12},{6,14},{9,1},{11,3}... | collective-permute-start | bytes 6152 | tf_op jit(solution)/shard_map/ppermute | solution.py:82
  93.6 20.2 %collective-permute-start.27 = (bf16[256,768]{1,0:T(8,128)(2,1)S(1)}, bf16[256,768]{1,0:T(8,128)(2,1)S(1)}, u32[]{:S(2)}, u32[]{:S(2)}) collective-permute-start(bf16[256,768]{1,0:T(8,128)(2,1)S(1)} %get-tuple-element.60.refs_0_), channel_id=1, source_target_pairs={{4,0},{8,4},{12,8},{14,12},{10,14},{6,10},{2,6},{0,2},{5,1},{9,5},... | collective-permute-start | bytes 1179656 | tf_op jit(solution)/shard_map/ppermute | solution.py:75
  94.8 17.7 %collective-permute-start.34 = (bf16[256,768]{1,0:T(8,128)(2,1)S(1)}, bf16[256,768]{1,0:T(8,128)(2,1)S(1)}, u32[]{:S(2)}, u32[]{:S(2)}) collective-permute-start(bf16[256,768]{1,0:T(8,128)(2,1)S(1)} %get-tuple-element.59.refs_8_), channel_id=1, source_target_pairs={{4,0},{8,4},{12,8},{14,12},{10,14},{6,10},{2,6},{0,2},{5,1},{9,5},... | collective-permute-start | bytes 1179656 | tf_op jit(solution)/shard_map/ppermute | solution.py:75
  96.7 17.8 %collective-permute-start.33 = (bf16[256,768]{1,0:T(8,128)(2,1)S(1)}, bf16[256,768]{1,0:T(8,128)(2,1)S(1)}, u32[]{:S(2)}, u32[]{:S(2)}) collective-permute-start(bf16[256,768]{1,0:T(8,128)(2,1)S(1)} %get-tuple-element.59.refs_8_), channel_id=1, source_target_pairs={{0,4},{4,8},{8,12},{12,14},{14,10},{10,6},{6,2},{2,0},{1,5},{5,9},... | collective-permute-start | bytes 1179656 | tf_op jit(solution)/shard_map/ppermute | solution.py:73
  98.6 41.6 %collective-permute-start.18 = (bf16[1,256,2048]{2,1,0:T(8,128)(2,1)S(1)}, bf16[1,256,2048]{2,1,0:T(8,128)(2,1)S(1)}, u32[]{:S(2)}, u32[]{:S(2)}) collective-permute-start(bf16[1,256,2048]{2,1,0:T(8,128)(2,1)S(1)} %get-tuple-element.40), channel_id=1, source_target_pairs={{1,0},{0,1},{3,2},{2,3},{5,4},{4,5},{7,6},{6,7},{9,8},{8,9},{11,10... | collective-permute-start | bytes 3145736 | tf_op jit(solution)/shard_map/ppermute | solution.py:82
  104.7 37.7 %collective-permute-start.17 = (bf16[1,256,2048]{2,1,0:T(8,128)(2,1)S(1)}, bf16[1,256,2048]{2,1,0:T(8,128)(2,1)S(1)}, u32[]{:S(2)}, u32[]{:S(2)}) collective-permute-start(bf16[1,256,2048]{2,1,0:T(8,128)(2,1)S(1)} %add_convert_fusion), channel_id=1, source_target_pairs={{16,0},{0,16},{17,1},{1,17},{18,2},{2,18},{19,3},{3,19},{20,4},{4,... | collective-permute-start | bytes 3145736 | tf_op jit(solution)/shard_map/ppermute | solution.py:82
  114.5 18.4 %collective-permute-start.43 = (bf16[768,256]{1,0:T(8,128)(2,1)S(1)}, bf16[768,256]{1,0:T(8,128)(2,1)S(1)}, u32[]{:S(2)}, u32[]{:S(2)}) collective-permute-start(bf16[768,256]{1,0:T(8,128)(2,1)S(1)} %get-tuple-element.57.refs_2_), channel_id=1, source_target_pairs={{0,4},{4,8},{8,12},{12,14},{14,10},{10,6},{6,2},{2,0},{1,5},{5,9},... | collective-permute-start | bytes 1179656 | tf_op jit(solution)/shard_map/ppermute | solution.py:73
  134.0 19.3 %collective-permute-start.29 = (bf16[256,768]{1,0:T(8,128)(2,1)S(1)}, bf16[256,768]{1,0:T(8,128)(2,1)S(1)}, u32[]{:S(2)}, u32[]{:S(2)}) collective-permute-start(bf16[256,768]{1,0:T(8,128)(2,1)S(1)} %collective-permute-done.27.refs_2_), channel_id=1, source_target_pairs={{4,0},{8,4},{12,8},{14,12},{10,14},{6,10},{2,6},{0,2},{5,1},{9,5},... | collective-permute-start | bytes 1179656 | tf_op jit(solution)/shard_map/ppermute | solution.py:75
  140.2 19.1 %collective-permute-start.48 = (bf16[768,256]{1,0:T(8,128)(2,1)S(1)}, bf16[768,256]{1,0:T(8,128)(2,1)S(1)}, u32[]{:S(2)}, u32[]{:S(2)}) collective-permute-start(bf16[768,256]{1,0:T(8,128)(2,1)S(1)} %collective-permute-done.42.refs_3_), channel_id=1, source_target_pairs={{0,4},{4,8},{8,12},{12,14},{14,10},{10,6},{6,2},{2,0},{1,5},{5,9},... | collective-permute-start | bytes 1179656 | tf_op jit(solution)/shard_map/ppermute | solution.py:73
  142.4 19.3 %collective-permute-start.51 = (bf16[768,256]{1,0:T(8,128)(2,1)S(1)}, bf16[768,256]{1,0:T(8,128)(2,1)S(1)}, u32[]{:S(2)}, u32[]{:S(2)}) collective-permute-start(bf16[768,256]{1,0:T(8,128)(2,1)S(1)} %collective-permute-done.45.refs_6_), channel_id=1, source_target_pairs={{4,0},{8,4},{12,8},{14,12},{10,14},{6,10},{2,6},{0,2},{5,1},{9,5},... | collective-permute-start | bytes 1179656 | tf_op jit(solution)/shard_map/ppermute | solution.py:75
  144.8 41.6 %collective-permute-start.40 = (bf16[256,2048]{1,0:T(8,128)(2,1)S(1)}, bf16[256,2048]{1,0:T(8,128)(2,1)S(1)}, u32[]{:S(2)}, u32[]{:S(2)}) collective-permute-start(bf16[256,2048]{1,0:T(8,128)(2,1)S(1)} %get-tuple-element.42.refs_16_), channel_id=1, source_target_pairs={{16,0},{0,16},{17,1},{1,17},{18,2},{2,18},{19,3},{3,19},{20,4},{4,... | collective-permute-start | bytes 3145736 | tf_op jit(solution)/shard_map/ppermute | solution.py:82
  167.7 39.6 %collective-permute-start.60 = (bf16[256,2048]{1,0:T(8,128)(2,1)S(1)}, bf16[256,2048]{1,0:T(8,128)(2,1)S(1)}, u32[]{:S(2)}, u32[]{:S(2)}) collective-permute-start(bf16[256,2048]{1,0:T(8,128)(2,1)S(1)} %get-tuple-element.42.refs_16_), channel_id=1, source_target_pairs={{1,0},{0,1},{3,2},{2,3},{5,4},{4,5},{7,6},{6,7},{9,8},{8,9},{11,10... | collective-permute-start | bytes 3145736 | tf_op jit(solution)/shard_map/ppermute | solution.py:82
  186.5 30.8 %collective-permute-start.41 = (bf16[256,2048]{1,0:T(8,128)(2,1)S(1)}, bf16[256,2048]{1,0:T(8,128)(2,1)S(1)}, u32[]{:S(2)}, u32[]{:S(2)}) collective-permute-start(bf16[256,2048]{1,0:T(8,128)(2,1)S(1)} %collective-permute-done.40.refs_16_), channel_id=1, source_target_pairs={{1,0},{0,1},{3,2},{2,3},{5,4},{4,5},{7,6},{6,7},{9,8},{8,9},{11,10... | collective-permute-start | bytes 3145736 | tf_op jit(solution)/shard_map/ppermute | solution.py:82
  194.9 16.9 %collective-permute-start.55 = (bf16[768,256]{1,0:T(8,128)(2,1)S(1)}, bf16[768,256]{1,0:T(8,128)(2,1)S(1)}, u32[]{:S(2)}, u32[]{:S(2)}) collective-permute-start(bf16[768,256]{1,0:T(8,128)(2,1)S(1)} %collective-permute-done.49.refs_2_.refs_8_), channel_id=1, source_target_pairs={{0,4},{4,8},{8,12},{12,14},{14,10},{10,6},{6,2},{2,0},{1,5},{5,9},... | collective-permute-start | bytes 1179656 | tf_op jit(solution)/shard_map/ppermute | solution.py:73
  205.8 18.0 %collective-permute-start.63 = (bf16[768,256]{1,0:T(8,128)(2,1)S(1)}, bf16[768,256]{1,0:T(8,128)(2,1)S(1)}, u32[]{:S(2)}, u32[]{:S(2)}) collective-permute-start(bf16[768,256]{1,0:T(8,128)(2,1)S(1)} %collective-permute-done.54.refs_1_), channel_id=1, source_target_pairs={{0,4},{4,8},{8,12},{12,14},{14,10},{10,6},{6,2},{2,0},{1,5},{5,9},... | collective-permute-start | bytes 1179656 | tf_op jit(solution)/shard_map/ppermute | solution.py:73
  207.3 17.0 %collective-permute-start.64 = (bf16[768,256]{1,0:T(8,128)(2,1)S(1)}, bf16[768,256]{1,0:T(8,128)(2,1)S(1)}, u32[]{:S(2)}, u32[]{:S(2)}) collective-permute-start(bf16[768,256]{1,0:T(8,128)(2,1)S(1)} %collective-permute-done.57.refs_4_), channel_id=1, source_target_pairs={{4,0},{8,4},{12,8},{14,12},{10,14},{6,10},{2,6},{0,2},{5,1},{9,5},... | collective-permute-start | bytes 1179656 | tf_op jit(solution)/shard_map/ppermute | solution.py:75
  228.1 22.2 %collective-permute-start.47 = (bf16[1,256,768]{2,1,0:T(8,128)(2,1)S(1)}, bf16[1,256,768]{2,1,0:T(8,128)(2,1)S(1)}, u32[]{:S(2)}, u32[]{:S(2)}) collective-permute-start(bf16[1,256,768]{2,1,0:T(8,128)(2,1)S(1)} %add_convert_fusion.1), channel_id=1, source_target_pairs={{16,0},{0,16},{17,1},{1,17},{18,2},{2,18},{19,3},{3,19},{20,4},{4,... | collective-permute-start | bytes 1179656 | tf_op jit(solution)/shard_map/ppermute | solution.py:82
  229.4 20.9 %collective-permute-start.53 = (bf16[1,256,512]{2,1,0:T(8,128)(2,1)S(1)}, bf16[1,256,512]{2,1,0:T(8,128)(2,1)S(1)}, u32[]{:S(2)}, u32[]{:S(2)}) collective-permute-start(bf16[1,256,512]{2,1,0:T(8,128)(2,1)S(1)} %add_convert_fusion.3), channel_id=1, source_target_pairs={{16,0},{0,16},{17,1},{1,17},{18,2},{2,18},{19,3},{3,19},{20,4},{4,... | collective-permute-start | bytes 786440 | tf_op jit(solution)/shard_map/ppermute | solution.py:82
  230.3 21.9 %collective-permute-start.66 = (bf16[1,256,256]{2,1,0:T(8,128)(2,1)S(1)}, bf16[1,256,256]{2,1,0:T(8,128)(2,1)S(1)}, u32[]{:S(2)}, u32[]{:S(2)}) collective-permute-start(bf16[1,256,256]{2,1,0:T(8,128)(2,1)S(1)} %add_convert_fusion.4), channel_id=1, source_target_pairs={{16,0},{0,16},{17,1},{1,17},{18,2},{2,18},{19,3},{3,19},{20,4},{4,... | collective-permute-start | bytes 393224 | tf_op jit(solution)/shard_map/ppermute | solution.py:82
  (52 other events, 676.4 us)

commit v3 on v2

--- a/solution.py
+++ b/solution.py
@@ -60,22 +60,24 @@
     return np.asarray(rows, np.int32)
 
 
-def ring_gather(first, second, count):
+def ring_gather(first, second, count, cuts=1):
     ring = ring_order(count)
     fwd = [(ring[i], ring[(i + 1) % count]) for i in range(count)]
     bwd = [(b, a) for a, b in fwd]
     far = count // 2
     ahead, behind = [first, second], [first, second]
     held = [(first, second)]
-    for k in range(1, far + 1):
+    for _ in range(1, far):
         for h in range(2):
-            if k < far or h == 0:
-                ahead[h] = lax.ppermute(ahead[h], "fs", fwd)
-            if k < far or h == 1:
-                behind[h] = lax.ppermute(behind[h], "fs", bwd)
-        if k < far:
-            held += [tuple(ahead), tuple(behind)]
-    return held + [(ahead[0], behind[1])]
+            ahead[h] = lax.ppermute(ahead[h], "fs", fwd)
+            behind[h] = lax.ppermute(behind[h], "fs", bwd)
+        held += [tuple(ahead), tuple(behind)]
+    for i in range(cuts):
+        cols = slice(i * first.shape[1] // cuts, (i + 1) * first.shape[1] // cuts)
+        one = lax.ppermute(ahead[0][:, cols], "fs", fwd)
+        two = lax.ppermute(behind[1][:, cols], "fs", bwd)
+        held.append((one, two))
+    return held
 
 
 def shift(value, axis, count, by):
@@ -492,30 +494,35 @@
     )(order, *flat)
 
 
-def last_kernel(count, scalars, hidden, total, squares, *refs):
+def last_kernel(count, cuts, scalars, hidden, total, squares, *refs):
     ends, pieces = refs[: -2 - count], refs[-2 - count : -2]
     out, gains = refs[-2:]
     place_gains(scalars[count], pieces, gains)
     width = hidden.shape[1]
-    cols = width // count
-    end = ends[0][0].astype(F32)
-    for ref in ends[1:]:
-        end = end + ref[0].astype(F32)
+    cols = width // count // cuts
+    each = len(ends) // cuts
     power = jnp.sum(squares[...], axis=-1, keepdims=True)
-    power = power + jnp.sum(end * end, axis=-1, keepdims=True)
+    sums = []
+    for i in range(cuts):
+        end = ends[i * each][0].astype(F32)
+        for ref in ends[i * each + 1 : (i + 1) * each]:
+            end = end + ref[0].astype(F32)
+        sums.append(end)
+        power = power + jnp.sum(end * end, axis=-1, keepdims=True)
     scale = lax.rsqrt(power * (1.0 / width) + EPSILON)
     out[...] = (hidden[...].astype(F32) + total[...] * scale * gains[1:2, :]).astype(BF16)
-    at = pl.ds(pl.multiple_of(scalars[count - 1] * cols, cols), cols)
-    out[:, at] = (hidden[:, at].astype(F32) + end * scale * gains[1:2, at]).astype(BF16)
-
-
-def last(scalars, hidden, total, squares, ends, gains):
+    for i, end in enumerate(sums):
+        at = pl.ds(pl.multiple_of((scalars[count - 1] * cuts + i) * cols, cols), cols)
+        out[:, at] = (hidden[:, at].astype(F32) + end * scale * gains[1:2, at]).astype(BF16)
+
+
+def last(scalars, hidden, total, squares, ends, gains, cuts):
     rows, width = hidden.shape
     tile = rows // 2
     row = lambda n: pl.BlockSpec((tile, n), lambda i, *_: (i, 0))
     part = lambda p: pl.BlockSpec((1, tile, p.shape[2]), lambda i, *_: (p.shape[0] - 1, i, 0))
     return pl.pallas_call(
-        functools.partial(last_kernel, len(gains)),
+        functools.partial(last_kernel, len(gains), cuts),
         grid_spec=pltpu.PrefetchScalarGridSpec(
             num_scalar_prefetch=1,
             grid=(rows // tile,),
@@ -530,6 +537,9 @@
         cost_estimate=cost(1e9, 8 * rows * width),
         name="last",
     )(scalars, hidden, total, squares, *ends, *gains)
+
+
+FAR_CUTS = 2
 
 
 def group_sizes(count):
@@ -578,7 +588,7 @@
     up_mine = (rep_part(up_weight, hid, 1) * gain_mlp_pre[:, None]).astype(BF16)
     ups = ring_gather(up_mine[:, : hid // 2], up_mine[:, hid // 2 :], count)
     down_mine = (rep_part(down_weight, hid, 0) * down_scale).astype(BF16)
-    downs = ring_gather(down_mine[: hid // 2], down_mine[hid // 2 :], count)
+    downs = ring_gather(down_mine[: hid // 2], down_mine[hid // 2 :], count, FAR_CUTS)
     order = lax.dynamic_slice_in_dim(jnp.asarray(order_table(count)), me, 1, 0)[0]
 
     mine = lax.dynamic_slice_in_dim(tokens[0], tp * share, share, 0)
@@ -650,14 +660,18 @@
             streams.append(group_sizes(count)[0 if dr else 1][:-1])
             arrays.append([group[i] for group in rows_of[dr]])
     total, squares = sum_blocks(order, tuple(streams), arrays, share, width)
-    parts = down_project(tps, [acts[dr] for dr in far_first], downs[-1:])
-    summands = over_tp(parts)
-    ends = list(summands)
-    for i, dr in enumerate(far_first):
-        if dr:
-            ends.append(over_rep([x[i : i + 1] for x in summands], dr))
+    ends = []
+    for cut in range(FAR_CUTS):
+        parts = down_project(
+            tps, [acts[dr] for dr in far_first], downs[count - 1 + cut : count + cut]
+        )
+        summands = over_tp(parts)
+        ends += summands
+        for i, dr in enumerate(far_first):
+            if dr:
+                ends.append(over_rep([x[i : i + 1] for x in summands], dr))
     scalars = jnp.concatenate([order, me_scalar])
-    return last(scalars, hidden, total, squares, ends, gains)[None]
+    return last(scalars, hidden, total, squares, ends, gains, FAR_CUTS)[None]
 
 
 def link_states(earlier, later):
@@ -787,6 +801,7 @@
             and chan == 2 * rows
             and chan % (width // count) == 0
             and hid % (2 * LANES) == 0
+            and width // count % (FAR_CUTS * LANES) == 0
             and length % (32 * tps) == 0
             and reps * (chan // LANES) <= 8
         )

time: 254 us -> 258 us (1.016)
  starting transfers between devices: 72.3 us -> 75.5 us
    ppermute x0 -> x8, starting transfers between devices: none -> 9.66 us  [the longest x4 5.07 us: ring_gather(): two = lax.ppermute(behind[1][:, cols], 'fs', bwd)]
    ppermute x0 -> x8, waiting for transfers between devices: none -> 8.78 us  [the longest x4 6.31 us: ring_gather(): one = lax.ppermute(ahead[0][:, cols], 'fs', fwd)]
    ppermute x21 -> x18, waiting for transfers between devices: 68.5 us -> 62.2 us  [ring_gather(): ahead[h] = lax.ppermute(ahead[h], 'fs', fwd)]
    ppermute x21 -> x18, starting transfers between devices: 24.2 us -> 20.2 us  [ring_gather(): behind[h] = lax.ppermute(behind[h], 'fs', bwd)]
    ppermute x21 -> x18, waiting for transfers between devices: 42.6 us -> 38.8 us  [ring_gather(): behind[h] = lax.ppermute(behind[h], 'fs', bwd)]
    ppermute x21 -> x18, starting transfers between devices: 22.9 us -> 19.6 us  [ring_gather(): ahead[h] = lax.ppermute(ahead[h], 'fs', fwd)]
    pallas_call x6 -> x7, Pallas kernels: 7.48 us -> 8.45 us  [down_project(): pl.pallas_call(functools.partial(down_kernel, len(held), len(acts)), in_s...]
    ppermute x25 -> x27, starting transfers between devices: 25.2 us -> 26 us  [shift(): lax.ppermute(value, axis, [((i + by) % count, i) for i in range(count)])]
  transfers between devices with their start and end apart: 67 -> 71, of which waited for: 32 -> 34; matrix products, arithmetic and copies ran while one was open for 2% -> 2% of each run, Pallas kernels for 15% -> 15%
where the time goes in v3:
time: 258 us
  waiting for transfers between devices  132 us (51%)
  starting transfers between devices  75.5 us (29%)
  Pallas kernels  41.7 us (16%)
  other arithmetic  4.39 us (2%)
  local copies, waits for them, and re-layouts  3.81 us (1%)
    ppermute x18, waiting for transfers between devices, ring_gather(): ahead[h] = lax.ppermute(ahead[h], 'fs', fwd)  62.2 us
    ppermute x18, waiting for transfers between devices, ring_gather(): behind[h] = lax.ppermute(behind[h], 'fs', bwd)  38.8 us
    ppermute x27, starting transfers between devices, shift(): lax.ppermute(value, axis, [((i + by) % count, i) for i in range(count)])  26 us
    ppermute x27, waiting for transfers between devices, shift(): lax.ppermute(value, axis, [((i + by) % count, i) for i in range(count)])  22 us
    ppermute x18, starting transfers between devices, ring_gather(): behind[h] = lax.ppermute(behind[h], 'fs', bwd)  20.2 us
    ppermute x18, starting transfers between devices, ring_gather(): ahead[h] = lax.ppermute(ahead[h], 'fs', fwd)  19.6 us
    pallas_call x7, Pallas kernels, down_project(): pl.pallas_call(functools.partial(down_kernel, len(held), len(acts)), in_s...  8.45 us
    pallas_call x2, Pallas kernels, up_project(): pl.pallas_call(functools.partial(up_kernel, steps, len(xs)), grid_spec=pl...  8 us
  transfers between devices with their start and end apart: 71, of which 34 were waited for; matrix products, arithmetic and copies ran while one was open for 2% of the time, Pallas kernels for 15%

profile of v3, /device:TPU:0, one launch (start us, length us, event | category | flops | bytes accessed | tf_op | source)
XLA Modules:
  0.0 257.7 jit_solution(6927197729323788888)
XLA Ops:
  2.4 3.0 %collective-permute-start = (bf16[256,2048]{1,0:T(8,128)(2,1)}, bf16[256,2048]{1,0:T(8,128)(2,1)S(1)}, u32[]{:S(2)}, u32[]{:S(2)}) collective-permute-start(bf16[256,2048]{1,0:T(8,128)(2,1)} %dynamic-slice_bitcast_fusion.tokens), channel_id=1, source_target_pairs={{16,0},{0,16},{17,1},{1,17},{18,2},{2,18},{19,3},{3,19},{20,4},{4,... | collective-permute-start | bytes 3145736 | tf_op jit(solution)/shard_map/ppermute | solution.py:84
  13.2 6.7 %collective-permute-done.10.refs_10_ = bf16[256,768]{1,0:T(8,128)(2,1)S(1)} collective-permute-done((bf16[256,768]{1,0:T(8,128)(2,1)}, bf16[256,768]{1,0:T(8,128)(2,1)S(1)}, u32[]{:S(2)}, u32[]{:S(2)}) %collective-permute-start.10) | collective-permute-done | bytes 393248 | tf_op jit(solution)/shard_map/ppermute | solution.py:73
  21.5 6.7 %collective-permute-done.2.refs_1_ = bf16[256,768]{1,0:T(8,128)(2,1)S(1)} collective-permute-done((bf16[256,768]{1,0:T(8,128)(2,1)}, bf16[256,768]{1,0:T(8,128)(2,1)S(1)}, u32[]{:S(2)}, u32[]{:S(2)}) %collective-permute-start.2) | collective-permute-done | bytes 393248 | tf_op jit(solution)/shard_map/ppermute | solution.py:72
  32.8 3.0 %collective-permute-done.12.refs_12_ = bf16[256,768]{1,0:T(8,128)(2,1)S(1)} collective-permute-done((bf16[256,768]{1,0:T(8,128)(2,1)S(1)}, bf16[256,768]{1,0:T(8,128)(2,1)S(1)}, u32[]{:S(2)}, u32[]{:S(2)}) %collective-permute-start.12) | collective-permute-done | bytes 393248 | tf_op jit(solution)/shard_map/ppermute | solution.py:73
  35.9 2.5 collective-permute-start.14
  42.3 6.4 %collective-permute-done.11.refs_11_ = bf16[256,768]{1,0:T(8,128)(2,1)S(1)} collective-permute-done((bf16[256,768]{1,0:T(8,128)(2,1)S(1)}, bf16[256,768]{1,0:T(8,128)(2,1)S(1)}, u32[]{:S(2)}, u32[]{:S(2)}) %collective-permute-start.11) | collective-permute-done | bytes 393248 | tf_op jit(solution)/shard_map/ppermute | solution.py:72
  58.3 4.6 %collective-permute-start.19 = (f32[2,256]{1,0:T(2,128)S(1)}, f32[2,256]{1,0:T(2,128)S(1)}, u32[]{:S(2)}, u32[]{:S(2)}) collective-permute-start(f32[2,256]{1,0:T(2,128)S(1)} %pad_maximum_fusion.2.refs_3_.refs_6_), channel_id=1, source_target_pairs={{2,0},{4,2},{6,4},{8,6},{10,8},{12,10},{14,12},{0,14},{3,1},{5,3},... | collective-permute-start | bytes 6152 | tf_op jit(solution)/shard_map/ppermute | solution.py:84
  65.5 2.5 collective-permute-start.20
  69.5 2.4 collective-permute-start.22
  72.0 2.9 %project.2 = (bf16[512,512]{1,0:T(8,128)(2,1)S(1)}, bf16[512,512]{1,0:T(8,128)(2,1)S(1)}) custom-call(s32[8]{0:T(128)S(1)} %fusion.1.order, bf16[512,2048]{1,0:T(8,128)(2,1)S(1)} %normalize.2.normed, f32[1,1024]{1,0:T(1,128)S(1)} %bitcast.32, bf16[256,768]{1,0:T(8,128)(2,1)S(1)} %copy-done.2, bf16[256,768]{1,0:T(8,128)(2,1)S(1)} %collective-permute-done.2.refs_1_, ...), custom_call_target="tpu_custom_call" | custom-call | flops 2147483648 | bytes 6291456 | tf_op jit(solution)/shard_map/project/pallas_call | solution.py:200
  74.9 3.3 %recur.2.mixed = bf16[1,512,512]{2,1,0:T(8,128)(2,1)S(1)} custom-call(bf16[1,512,512]{2,1,0:T(8,128)(2,1)S(1)} %bitcast.38, bf16[1,512,512]{2,1,0:T(8,128)(2,1)S(1)} %bitcast.39, f32[4,512]{1,0:T(4,128)S(1)} %constant_dynamic-slice_fusion.conv_ref, bf16[4,128,256]{2,1,0:T(8,128)(2,1)S(1)} %pad_maximum_fusion.maps_ref, f32[1,512]{1,0:T(1,128)S(1)} %bitcast.34), custom_call_target="tpu_custom_call" | custom-call | flops 3000000000 | bytes 1572864 | tf_op jit(solution)/shard_map/recur/pallas_call | solution.py:269
  80.4 2.9 %project.3 = (bf16[512,512]{1,0:T(8,128)(2,1)S(1)}, bf16[512,512]{1,0:T(8,128)(2,1)S(1)}) custom-call(s32[8]{0:T(128)S(1)} %fusion.1.order, bf16[512,2048]{1,0:T(8,128)(2,1)S(1)} %normalize.3.normed, f32[1,1024]{1,0:T(1,128)S(1)} %bitcast.33, bf16[256,768]{1,0:T(8,128)(2,1)S(1)} %copy-done.2, bf16[256,768]{1,0:T(8,128)(2,1)S(1)} %collective-permute-done.2.refs_1_, ...), custom_call_target="tpu_custom_call" | custom-call | flops 2147483648 | bytes 6291456 | tf_op jit(solution)/shard_map/project/pallas_call | solution.py:200
  83.3 3.3 %recur.3.mixed = bf16[1,512,512]{2,1,0:T(8,128)(2,1)S(1)} custom-call(bf16[1,512,512]{2,1,0:T(8,128)(2,1)S(1)} %bitcast.36, bf16[1,512,512]{2,1,0:T(8,128)(2,1)S(1)} %bitcast.37, f32[4,512]{1,0:T(4,128)S(1)} %constant_dynamic-slice_fusion.conv_ref, bf16[4,128,256]{2,1,0:T(8,128)(2,1)S(1)} %pad_maximum_fusion.maps_ref, f32[1,512]{1,0:T(1,128)S(1)} %bitcast.35), custom_call_target="tpu_custom_call" | custom-call | flops 3000000000 | bytes 1572864 | tf_op jit(solution)/shard_map/recur/pallas_call | solution.py:269
  98.5 6.2 %collective-permute-done.26.refs_1_ = bf16[256,768]{1,0:T(8,128)(2,1)S(1)} collective-permute-done((bf16[256,768]{1,0:T(8,128)(2,1)S(1)}, bf16[256,768]{1,0:T(8,128)(2,1)S(1)}, u32[]{:S(2)}, u32[]{:S(2)}) %collective-permute-start.26) | collective-permute-done | bytes 393248 | tf_op jit(solution)/shard_map/ppermute | solution.py:72
  105.3 7.1 %collective-permute-done.34.refs_10_ = bf16[256,768]{1,0:T(8,128)(2,1)S(1)} collective-permute-done((bf16[256,768]{1,0:T(8,128)(2,1)S(1)}, bf16[256,768]{1,0:T(8,128)(2,1)S(1)}, u32[]{:S(2)}, u32[]{:S(2)}) %collective-permute-start.34) | collective-permute-done | bytes 393248 | tf_op jit(solution)/shard_map/ppermute | solution.py:73
  115.8 8.6 %collective-permute-done.42.refs_3_ = bf16[768,256]{1,0:T(8,128)(2,1)S(1)} collective-permute-done((bf16[768,256]{1,0:T(8,128)(2,1)S(1)}, bf16[768,256]{1,0:T(8,128)(2,1)S(1)}, u32[]{:S(2)}, u32[]{:S(2)}) %collective-permute-start.42) | collective-permute-done | bytes 393248 | tf_op jit(solution)/shard_map/ppermute | solution.py:72
  126.4 6.4 %collective-permute-done.43.refs_4_ = bf16[768,256]{1,0:T(8,128)(2,1)S(1)} collective-permute-done((bf16[768,256]{1,0:T(8,128)(2,1)S(1)}, bf16[768,256]{1,0:T(8,128)(2,1)S(1)}, u32[]{:S(2)}, u32[]{:S(2)}) %collective-permute-start.43) | collective-permute-done | bytes 393248 | tf_op jit(solution)/shard_map/ppermute | solution.py:72
  135.4 3.4 %collective-permute-done.28.refs_3_ = bf16[256,768]{1,0:T(8,128)(2,1)S(1)} collective-permute-done((bf16[256,768]{1,0:T(8,128)(2,1)S(1)}, bf16[256,768]{1,0:T(8,128)(2,1)S(1)}, u32[]{:S(2)}, u32[]{:S(2)}) %collective-permute-start.28) | collective-permute-done | bytes 393248 | tf_op jit(solution)/shard_map/ppermute | solution.py:72
  145.3 8.0 %collective-permute-done.29.refs_4_ = bf16[256,768]{1,0:T(8,128)(2,1)S(1)} collective-permute-done((bf16[256,768]{1,0:T(8,128)(2,1)S(1)}, bf16[256,768]{1,0:T(8,128)(2,1)S(1)}, u32[]{:S(2)}, u32[]{:S(2)}) %collective-permute-start.29) | collective-permute-done | bytes 393248 | tf_op jit(solution)/shard_map/ppermute | solution.py:73
  155.3 4.0 %collective-permute-done.48.refs_1_.refs_7_ = bf16[768,256]{1,0:T(8,128)(2,1)S(1)} collective-permute-done((bf16[768,256]{1,0:T(8,128)(2,1)S(1)}, bf16[768,256]{1,0:T(8,128)(2,1)S(1)}, u32[]{:S(2)}, u32[]{:S(2)}) %collective-permute-start.48) | collective-permute-done | bytes 393248 | tf_op jit(solution)/shard_map/ppermute | solution.py:72
  162.8 4.9 %collective-permute-done.49.refs_2_.refs_8_ = bf16[768,256]{1,0:T(8,128)(2,1)S(1)} collective-permute-done((bf16[768,256]{1,0:T(8,128)(2,1)S(1)}, bf16[768,256]{1,0:T(8,128)(2,1)S(1)}, u32[]{:S(2)}, u32[]{:S(2)}) %collective-permute-start.49) | collective-permute-done | bytes 393248 | tf_op jit(solution)/shard_map/ppermute | solution.py:72
  167.6 2.4 collective-permute-done.50.refs_3_.refs_9_
  174.4 3.4 %collective-permute-done.38.refs_14_ = bf16[256,768]{1,0:T(8,128)(2,1)S(1)} collective-permute-done((bf16[256,768]{1,0:T(8,128)(2,1)S(1)}, bf16[256,768]{1,0:T(8,128)(2,1)S(1)}, u32[]{:S(2)}, u32[]{:S(2)}) %collective-permute-start.38) | collective-permute-done | bytes 393248 | tf_op jit(solution)/shard_map/ppermute | solution.py:73
  179.0 4.5 %collective-permute-done.31.refs_6_ = bf16[256,768]{1,0:T(8,128)(2,1)S(1)} collective-permute-done((bf16[256,768]{1,0:T(8,128)(2,1)S(1)}, bf16[256,768]{1,0:T(8,128)(2,1)S(1)}, u32[]{:S(2)}, u32[]{:S(2)}) %collective-permute-start.31) | collective-permute-done | bytes 393248 | tf_op jit(solution)/shard_map/ppermute | solution.py:73
  186.5 7.3 %collective-permute-done.54.refs_1_ = bf16[768,256]{1,0:T(8,128)(2,1)S(1)} collective-permute-done((bf16[768,256]{1,0:T(8,128)(2,1)S(1)}, bf16[768,256]{1,0:T(8,128)(2,1)S(1)}, u32[]{:S(2)}, u32[]{:S(2)}) %collective-permute-start.54) | collective-permute-done | bytes 393248 | tf_op jit(solution)/shard_map/ppermute | solution.py:72
  195.9 6.3 %collective-permute-done.32.refs_7_ = bf16[256,768]{1,0:T(8,128)(2,1)S(1)} collective-permute-done((bf16[256,768]{1,0:T(8,128)(2,1)S(1)}, bf16[256,768]{1,0:T(8,128)(2,1)S(1)}, u32[]{:S(2)}, u32[]{:S(2)}) %collective-permute-start.32) | collective-permute-done | bytes 393248 | tf_op jit(solution)/shard_map/ppermute | solution.py:77
  203.3 2.5 collective-permute-done.39.refs_15_
  207.8 4.0 %up_project.3.refs_0_.refs_1_ = bf16[512,1536]{1,0:T(8,128)(2,1)S(1)} custom-call(s32[8]{0:T(128)S(1)} %fusion.1.order, f32[1,1536]{1,0:T(1,128)S(1)} %broadcast_in_dim.39.scale, bf16[256,768]{1,0:T(8,128)(2,1)S(1)} %get-tuple-element.64.refs_0_, bf16[256,768]{1,0:T(8,128)(2,1)S(1)} %collective-permute-done.26.refs_1_, ...), custom_call_target="tpu_custom_call" | custom-call | flops 3221225472 | bytes 9961472 | tf_op jit(solution)/shard_map/up_project/pallas_call | solution.py:394
  217.8 4.0 %up_project.2.refs_0_ = bf16[512,1536]{1,0:T(8,128)(2,1)S(1)} custom-call(s32[8]{0:T(128)S(1)} %fusion.1.order, f32[1,1536]{1,0:T(1,128)S(1)} %broadcast_in_dim.39.scale, bf16[256,768]{1,0:T(8,128)(2,1)S(1)} %get-tuple-element.64.refs_0_, bf16[256,768]{1,0:T(8,128)(2,1)S(1)} %collective-permute-done.26.refs_1_, ...), custom_call_target="tpu_custom_call" | custom-call | flops 3221225472 | bytes 9961472 | tf_op jit(solution)/shard_map/up_project/pallas_call | solution.py:394
  235.0 4.3 %collective-permute-done.59.refs_2_ = bf16[1,256,512]{2,1,0:T(8,128)(2,1)S(1)} collective-permute-done((bf16[1,256,512]{2,1,0:T(8,128)(2,1)S(1)}, bf16[1,256,512]{2,1,0:T(8,128)(2,1)S(1)}, u32[]{:S(2)}, u32[]{:S(2)}) %collective-permute-start.59) | collective-permute-done | bytes 262176 | tf_op jit(solution)/shard_map/ppermute | solution.py:84
  239.4 5.6 %collective-permute-done.53.refs_1_ = bf16[1,256,512]{2,1,0:T(8,128)(2,1)S(1)} collective-permute-done((bf16[1,256,512]{2,1,0:T(8,128)(2,1)S(1)}, bf16[1,256,512]{2,1,0:T(8,128)(2,1)S(1)}, u32[]{:S(2)}, u32[]{:S(2)}) %collective-permute-start.53) | collective-permute-done | bytes 262176 | tf_op jit(solution)/shard_map/ppermute | solution.py:84
  245.0 8.4 %collective-permute-done.47.refs_0_ = bf16[1,256,768]{2,1,0:T(8,128)(2,1)S(1)} collective-permute-done((bf16[1,256,768]{2,1,0:T(8,128)(2,1)S(1)}, bf16[1,256,768]{2,1,0:T(8,128)(2,1)S(1)}, u32[]{:S(2)}, u32[]{:S(2)}) %collective-permute-start.47) | collective-permute-done | bytes 393248 | tf_op jit(solution)/shard_map/ppermute | solution.py:84
  (197 shorter events, 105.5 us)
Async XLA Ops:
  2.4 27.1 %collective-permute-start = (bf16[256,2048]{1,0:T(8,128)(2,1)}, bf16[256,2048]{1,0:T(8,128)(2,1)S(1)}, u32[]{:S(2)}, u32[]{:S(2)}) collective-permute-start(bf16[256,2048]{1,0:T(8,128)(2,1)} %dynamic-slice_bitcast_fusion.tokens), channel_id=1, source_target_pairs={{16,0},{0,16},{17,1},{1,17},{18,2},{2,18},{19,3},{3,19},{20,4},{4,... | collective-permute-start | bytes 3145736 | tf_op jit(solution)/shard_map/ppermute | solution.py:84
  9.3 21.4 %collective-permute-start.9 = (bf16[256,768]{1,0:T(8,128)(2,1)}, bf16[256,768]{1,0:T(8,128)(2,1)S(1)}, u32[]{:S(2)}, u32[]{:S(2)}) collective-permute-start(bf16[256,768]{1,0:T(8,128)(2,1)} %get-tuple-element.34.refs_8_), channel_id=1, source_target_pairs={{0,4},{4,8},{8,12},{12,14},{14,10},{10,6},{6,2},{2,0},{1,5},{5,9},... | collective-permute-start | bytes 1179656 | tf_op jit(solution)/shard_map/ppermute | solution.py:72
  9.8 18.4 %collective-permute-start.2 = (bf16[256,768]{1,0:T(8,128)(2,1)}, bf16[256,768]{1,0:T(8,128)(2,1)S(1)}, u32[]{:S(2)}, u32[]{:S(2)}) collective-permute-start(bf16[256,768]{1,0:T(8,128)(2,1)} %get-tuple-element.33.refs_0_), channel_id=1, source_target_pairs={{0,4},{4,8},{8,12},{12,14},{14,10},{10,6},{6,2},{2,0},{1,5},{5,9},... | collective-permute-start | bytes 1179656 | tf_op jit(solution)/shard_map/ppermute | solution.py:72
  11.4 21.0 %collective-permute-start.3 = (bf16[256,768]{1,0:T(8,128)(2,1)}, bf16[256,768]{1,0:T(8,128)(2,1)S(1)}, u32[]{:S(2)}, u32[]{:S(2)}) collective-permute-start(bf16[256,768]{1,0:T(8,128)(2,1)} %get-tuple-element.33.refs_0_), channel_id=1, source_target_pairs={{4,0},{8,4},{12,8},{14,12},{10,14},{6,10},{2,6},{0,2},{5,1},{9,5},... | collective-permute-start | bytes 1179656 | tf_op jit(solution)/shard_map/ppermute | solution.py:73
  29.4 28.9 %collective-permute-start.1 = (bf16[256,2048]{1,0:T(8,128)(2,1)S(1)}, bf16[256,2048]{1,0:T(8,128)(2,1)S(1)}, u32[]{:S(2)}, u32[]{:S(2)}) collective-permute-start(bf16[256,2048]{1,0:T(8,128)(2,1)S(1)} %collective-permute-done.refs_0_), channel_id=1, source_target_pairs={{1,0},{0,1},{3,2},{2,3},{5,4},{4,5},{7,6},{6,7},{9,8},{8,9},{11,10... | collective-permute-start | bytes 3145736 | tf_op jit(solution)/shard_map/ppermute | solution.py:84
  30.7 17.9 %collective-permute-start.11 = (bf16[256,768]{1,0:T(8,128)(2,1)S(1)}, bf16[256,768]{1,0:T(8,128)(2,1)S(1)}, u32[]{:S(2)}, u32[]{:S(2)}) collective-permute-start(bf16[256,768]{1,0:T(8,128)(2,1)S(1)} %collective-permute-done.9.refs_9_), channel_id=1, source_target_pairs={{0,4},{4,8},{8,12},{12,14},{14,10},{10,6},{6,2},{2,0},{1,5},{5,9},... | collective-permute-start | bytes 1179656 | tf_op jit(solution)/shard_map/ppermute | solution.py:72
  35.9 16.9 %collective-permute-start.14 = (bf16[256,768]{1,0:T(8,128)(2,1)S(1)}, bf16[256,768]{1,0:T(8,128)(2,1)S(1)}, u32[]{:S(2)}, u32[]{:S(2)}) collective-permute-start(bf16[256,768]{1,0:T(8,128)(2,1)S(1)} %collective-permute-done.12.refs_12_), channel_id=1, source_target_pairs={{4,0},{8,4},{12,8},{14,12},{10,14},{6,10},{2,6},{0,2},{5,1},{9,5},... | collective-permute-start | bytes 1179656 | tf_op jit(solution)/shard_map/ppermute | solution.py:73
  40.2 16.9 %collective-permute-start.6 = (bf16[256,768]{1,0:T(8,128)(2,1)S(1)}, bf16[256,768]{1,0:T(8,128)(2,1)S(1)}, u32[]{:S(2)}, u32[]{:S(2)}) collective-permute-start(bf16[256,768]{1,0:T(8,128)(2,1)S(1)} %collective-permute-done.4.refs_3_), channel_id=1, source_target_pairs={{0,4},{4,8},{8,12},{12,14},{14,10},{10,6},{6,2},{2,0},{1,5},{5,9},... | collective-permute-start | bytes 1179656 | tf_op jit(solution)/shard_map/ppermute | solution.py:72
  48.6 16.9 %collective-permute-start.13 = (bf16[256,768]{1,0:T(8,128)(2,1)S(1)}, bf16[256,768]{1,0:T(8,128)(2,1)S(1)}, u32[]{:S(2)}, u32[]{:S(2)}) collective-permute-start(bf16[256,768]{1,0:T(8,128)(2,1)S(1)} %collective-permute-done.11.refs_11_), channel_id=1, source_target_pairs={{0,4},{4,8},{8,12},{12,14},{14,10},{10,6},{6,2},{2,0},{1,5},{5,9},... | collective-permute-start | bytes 1179656 | tf_op jit(solution)/shard_map/ppermute | solution.py:72
  49.1 18.9 %collective-permute-start.7 = (bf16[256,768]{1,0:T(8,128)(2,1)S(1)}, bf16[256,768]{1,0:T(8,128)(2,1)S(1)}, u32[]{:S(2)}, u32[]{:S(2)}) collective-permute-start(bf16[256,768]{1,0:T(8,128)(2,1)S(1)} %collective-permute-done.5.refs_4_), channel_id=1, source_target_pairs={{4,0},{8,4},{12,8},{14,12},{10,14},{6,10},{2,6},{0,2},{5,1},{9,5},... | collective-permute-start | bytes 1179656 | tf_op jit(solution)/shard_map/ppermute | solution.py:73
  58.3 28.2 %collective-permute-start.19 = (f32[2,256]{1,0:T(2,128)S(1)}, f32[2,256]{1,0:T(2,128)S(1)}, u32[]{:S(2)}, u32[]{:S(2)}) collective-permute-start(f32[2,256]{1,0:T(2,128)S(1)} %pad_maximum_fusion.2.refs_3_.refs_6_), channel_id=1, source_target_pairs={{2,0},{4,2},{6,4},{8,6},{10,8},{12,10},{14,12},{0,14},{3,1},{5,3},... | collective-permute-start | bytes 6152 | tf_op jit(solution)/shard_map/ppermute | solution.py:84
  65.5 25.4 %collective-permute-start.20 = (f32[2,256]{1,0:T(2,128)S(1)}, f32[2,256]{1,0:T(2,128)S(1)}, u32[]{:S(2)}, u32[]{:S(2)}) collective-permute-start(f32[2,256]{1,0:T(2,128)S(1)} %pad_maximum_fusion.2.refs_3_.refs_6_), channel_id=1, source_target_pairs={{4,0},{6,2},{8,4},{10,6},{12,8},{14,10},{0,12},{2,14},{5,1},{7,3},... | collective-permute-start | bytes 6152 | tf_op jit(solution)/shard_map/ppermute | solution.py:84
  68.0 24.2 %collective-permute-start.21 = (f32[2,256]{1,0:T(2,128)S(1)}, f32[2,256]{1,0:T(2,128)S(1)}, u32[]{:S(2)}, u32[]{:S(2)}) collective-permute-start(f32[2,256]{1,0:T(2,128)S(1)} %pad_maximum_fusion.2.refs_3_.refs_6_), channel_id=1, source_target_pairs={{6,0},{8,2},{10,4},{12,6},{14,8},{0,10},{2,12},{4,14},{7,1},{9,3},... | collective-permute-start | bytes 6152 | tf_op jit(solution)/shard_map/ppermute | solution.py:84
  69.5 23.1 %collective-permute-start.22 = (f32[2,256]{1,0:T(2,128)S(1)}, f32[2,256]{1,0:T(2,128)S(1)}, u32[]{:S(2)}, u32[]{:S(2)}) collective-permute-start(f32[2,256]{1,0:T(2,128)S(1)} %pad_maximum_fusion.2.refs_3_.refs_6_), channel_id=1, source_target_pairs={{8,0},{10,2},{12,4},{14,6},{0,8},{2,10},{4,12},{6,14},{9,1},{11,3}... | collective-permute-start | bytes 6152 | tf_op jit(solution)/shard_map/ppermute | solution.py:84
  93.6 20.2 %collective-permute-start.27 = (bf16[256,768]{1,0:T(8,128)(2,1)S(1)}, bf16[256,768]{1,0:T(8,128)(2,1)S(1)}, u32[]{:S(2)}, u32[]{:S(2)}) collective-permute-start(bf16[256,768]{1,0:T(8,128)(2,1)S(1)} %get-tuple-element.64.refs_0_), channel_id=1, source_target_pairs={{4,0},{8,4},{12,8},{14,12},{10,14},{6,10},{2,6},{0,2},{5,1},{9,5},... | collective-permute-start | bytes 1179656 | tf_op jit(solution)/shard_map/ppermute | solution.py:73
  94.7 17.7 %collective-permute-start.34 = (bf16[256,768]{1,0:T(8,128)(2,1)S(1)}, bf16[256,768]{1,0:T(8,128)(2,1)S(1)}, u32[]{:S(2)}, u32[]{:S(2)}) collective-permute-start(bf16[256,768]{1,0:T(8,128)(2,1)S(1)} %get-tuple-element.63.refs_8_), channel_id=1, source_target_pairs={{4,0},{8,4},{12,8},{14,12},{10,14},{6,10},{2,6},{0,2},{5,1},{9,5},... | collective-permute-start | bytes 1179656 | tf_op jit(solution)/shard_map/ppermute | solution.py:73
  96.6 17.8 %collective-permute-start.33 = (bf16[256,768]{1,0:T(8,128)(2,1)S(1)}, bf16[256,768]{1,0:T(8,128)(2,1)S(1)}, u32[]{:S(2)}, u32[]{:S(2)}) collective-permute-start(bf16[256,768]{1,0:T(8,128)(2,1)S(1)} %get-tuple-element.63.refs_8_), channel_id=1, source_target_pairs={{0,4},{4,8},{8,12},{12,14},{14,10},{10,6},{6,2},{2,0},{1,5},{5,9},... | collective-permute-start | bytes 1179656 | tf_op jit(solution)/shard_map/ppermute | solution.py:72
  98.5 41.6 %collective-permute-start.18 = (bf16[1,256,2048]{2,1,0:T(8,128)(2,1)S(1)}, bf16[1,256,2048]{2,1,0:T(8,128)(2,1)S(1)}, u32[]{:S(2)}, u32[]{:S(2)}) collective-permute-start(bf16[1,256,2048]{2,1,0:T(8,128)(2,1)S(1)} %get-tuple-element.42), channel_id=1, source_target_pairs={{1,0},{0,1},{3,2},{2,3},{5,4},{4,5},{7,6},{6,7},{9,8},{8,9},{11,10... | collective-permute-start | bytes 3145736 | tf_op jit(solution)/shard_map/ppermute | solution.py:84
  104.7 37.6 %collective-permute-start.17 = (bf16[1,256,2048]{2,1,0:T(8,128)(2,1)S(1)}, bf16[1,256,2048]{2,1,0:T(8,128)(2,1)S(1)}, u32[]{:S(2)}, u32[]{:S(2)}) collective-permute-start(bf16[1,256,2048]{2,1,0:T(8,128)(2,1)S(1)} %add_convert_fusion), channel_id=1, source_target_pairs={{16,0},{0,16},{17,1},{1,17},{18,2},{2,18},{19,3},{3,19},{20,4},{4,... | collective-permute-start | bytes 3145736 | tf_op jit(solution)/shard_map/ppermute | solution.py:84
  114.4 18.4 %collective-permute-start.43 = (bf16[768,256]{1,0:T(8,128)(2,1)S(1)}, bf16[768,256]{1,0:T(8,128)(2,1)S(1)}, u32[]{:S(2)}, u32[]{:S(2)}) collective-permute-start(bf16[768,256]{1,0:T(8,128)(2,1)S(1)} %get-tuple-element.61.refs_2_), channel_id=1, source_target_pairs={{0,4},{4,8},{8,12},{12,14},{14,10},{10,6},{6,2},{2,0},{1,5},{5,9},... | collective-permute-start | bytes 1179656 | tf_op jit(solution)/shard_map/ppermute | solution.py:72
  133.9 19.3 %collective-permute-start.29 = (bf16[256,768]{1,0:T(8,128)(2,1)S(1)}, bf16[256,768]{1,0:T(8,128)(2,1)S(1)}, u32[]{:S(2)}, u32[]{:S(2)}) collective-permute-start(bf16[256,768]{1,0:T(8,128)(2,1)S(1)} %collective-permute-done.27.refs_2_), channel_id=1, source_target_pairs={{4,0},{8,4},{12,8},{14,12},{10,14},{6,10},{2,6},{0,2},{5,1},{9,5},... | collective-permute-start | bytes 1179656 | tf_op jit(solution)/shard_map/ppermute | solution.py:73
  140.1 19.1 %collective-permute-start.48 = (bf16[768,256]{1,0:T(8,128)(2,1)S(1)}, bf16[768,256]{1,0:T(8,128)(2,1)S(1)}, u32[]{:S(2)}, u32[]{:S(2)}) collective-permute-start(bf16[768,256]{1,0:T(8,128)(2,1)S(1)} %collective-permute-done.42.refs_3_), channel_id=1, source_target_pairs={{0,4},{4,8},{8,12},{12,14},{14,10},{10,6},{6,2},{2,0},{1,5},{5,9},... | collective-permute-start | bytes 1179656 | tf_op jit(solution)/shard_map/ppermute | solution.py:72
  142.3 19.3 %collective-permute-start.51 = (bf16[768,256]{1,0:T(8,128)(2,1)S(1)}, bf16[768,256]{1,0:T(8,128)(2,1)S(1)}, u32[]{:S(2)}, u32[]{:S(2)}) collective-permute-start(bf16[768,256]{1,0:T(8,128)(2,1)S(1)} %collective-permute-done.45.refs_6_), channel_id=1, source_target_pairs={{4,0},{8,4},{12,8},{14,12},{10,14},{6,10},{2,6},{0,2},{5,1},{9,5},... | collective-permute-start | bytes 1179656 | tf_op jit(solution)/shard_map/ppermute | solution.py:73
  144.8 41.6 %collective-permute-start.40 = (bf16[256,2048]{1,0:T(8,128)(2,1)S(1)}, bf16[256,2048]{1,0:T(8,128)(2,1)S(1)}, u32[]{:S(2)}, u32[]{:S(2)}) collective-permute-start(bf16[256,2048]{1,0:T(8,128)(2,1)S(1)} %get-tuple-element.44.refs_16_), channel_id=1, source_target_pairs={{16,0},{0,16},{17,1},{1,17},{18,2},{2,18},{19,3},{3,19},{20,4},{4,... | collective-permute-start | bytes 3145736 | tf_op jit(solution)/shard_map/ppermute | solution.py:84
  167.6 39.6 %collective-permute-start.60 = (bf16[256,2048]{1,0:T(8,128)(2,1)S(1)}, bf16[256,2048]{1,0:T(8,128)(2,1)S(1)}, u32[]{:S(2)}, u32[]{:S(2)}) collective-permute-start(bf16[256,2048]{1,0:T(8,128)(2,1)S(1)} %get-tuple-element.44.refs_16_), channel_id=1, source_target_pairs={{1,0},{0,1},{3,2},{2,3},{5,4},{4,5},{7,6},{6,7},{9,8},{8,9},{11,10... | collective-permute-start | bytes 3145736 | tf_op jit(solution)/shard_map/ppermute | solution.py:84
  185.4 16.9 %collective-permute-start.32 = (bf16[256,768]{1,0:T(8,128)(2,1)S(1)}, bf16[256,768]{1,0:T(8,128)(2,1)S(1)}, u32[]{:S(2)}, u32[]{:S(2)}) collective-permute-start(bf16[256,768]{1,0:T(8,128)(2,1)S(1)} %collective-permute-done.30.refs_5_), channel_id=1, source_target_pairs={{0,4},{4,8},{8,12},{12,14},{14,10},{10,6},{6,2},{2,0},{1,5},{5,9},... | collective-permute-start | bytes 1179656 | tf_op jit(solution)/shard_map/ppermute | solution.py:77
  186.4 31.3 %collective-permute-start.41 = (bf16[256,2048]{1,0:T(8,128)(2,1)S(1)}, bf16[256,2048]{1,0:T(8,128)(2,1)S(1)}, u32[]{:S(2)}, u32[]{:S(2)}) collective-permute-start(bf16[256,2048]{1,0:T(8,128)(2,1)S(1)} %collective-permute-done.40.refs_16_), channel_id=1, source_target_pairs={{1,0},{0,1},{3,2},{2,3},{5,4},{4,5},{7,6},{6,7},{9,8},{8,9},{11,10... | collective-permute-start | bytes 3145736 | tf_op jit(solution)/shard_map/ppermute | solution.py:84
  194.9 16.9 %collective-permute-start.55 = (bf16[768,256]{1,0:T(8,128)(2,1)S(1)}, bf16[768,256]{1,0:T(8,128)(2,1)S(1)}, u32[]{:S(2)}, u32[]{:S(2)}) collective-permute-start(bf16[768,256]{1,0:T(8,128)(2,1)S(1)} %collective-permute-done.49.refs_2_.refs_8_), channel_id=1, source_target_pairs={{0,4},{4,8},{8,12},{12,14},{14,10},{10,6},{6,2},{2,0},{1,5},{5,9},... | collective-permute-start | bytes 1179656 | tf_op jit(solution)/shard_map/ppermute | solution.py:72
  205.8 17.0 %collective-permute-start.67 = (bf16[768,128]{1,0:T(8,128)(2,1)S(1)}, bf16[768,128]{1,0:T(8,128)(2,1)S(1)}, u32[]{:S(2)}, u32[]{:S(2)}) collective-permute-start(bf16[768,128]{1,0:T(8,128)(2,1)S(1)} %get-tuple-element.67), channel_id=1, source_target_pairs={{0,4},{4,8},{8,12},{12,14},{14,10},{10,6},{6,2},{2,0},{1,5},{5,9},... | collective-permute-start | bytes 589832 | tf_op jit(solution)/shard_map/ppermute | solution.py:77
  232.4 21.0 %collective-permute-start.47 = (bf16[1,256,768]{2,1,0:T(8,128)(2,1)S(1)}, bf16[1,256,768]{2,1,0:T(8,128)(2,1)S(1)}, u32[]{:S(2)}, u32[]{:S(2)}) collective-permute-start(bf16[1,256,768]{2,1,0:T(8,128)(2,1)S(1)} %add_convert_fusion.1), channel_id=1, source_target_pairs={{16,0},{0,16},{17,1},{1,17},{18,2},{2,18},{19,3},{3,19},{20,4},{4,... | collective-permute-start | bytes 1179656 | tf_op jit(solution)/shard_map/ppermute | solution.py:84
  233.0 21.9 %collective-permute-start.70 = (bf16[1,256,128]{2,1,0:T(8,128)(2,1)S(1)}, bf16[1,256,128]{2,1,0:T(8,128)(2,1)S(1)}, u32[]{:S(2)}, u32[]{:S(2)}) collective-permute-start(bf16[1,256,128]{2,1,0:T(8,128)(2,1)S(1)} %add_convert_fusion.4), channel_id=1, source_target_pairs={{16,0},{0,16},{17,1},{1,17},{18,2},{2,18},{19,3},{3,19},{20,4},{4,... | collective-permute-start | bytes 196616 | tf_op jit(solution)/shard_map/ppermute | solution.py:84
  234.5 21.1 %collective-permute-start.66 = (bf16[1,256,128]{2,1,0:T(8,128)(2,1)S(1)}, bf16[1,256,128]{2,1,0:T(8,128)(2,1)S(1)}, u32[]{:S(2)}, u32[]{:S(2)}) collective-permute-start(bf16[1,256,128]{2,1,0:T(8,128)(2,1)S(1)} %add_convert_fusion.5), channel_id=1, source_target_pairs={{16,0},{0,16},{17,1},{1,17},{18,2},{2,18},{19,3},{3,19},{20,4},{4,... | collective-permute-start | bytes 196616 | tf_op jit(solution)/shard_map/ppermute | solution.py:84
  (56 other events, 700.8 us)
